TPU v7x, 32 devices: a whole 2x2x4 slice. The times are simulated.
32 devices in a mesh: ep: 16 (over z, x, core), tp: 2 (over y).
Axes of the slice: x: 2, y: 2, z: 4, core: 2. Of those that a mesh axis runs over, the one named last changes fastest.
Arguments:
- tokens: bfloat16 [2048, 2048], P('ep'), may hold values from -6 to 6
- cotangent: bfloat16 [2048, 2048], P('ep'), may hold values from -1.796875 to 1.796875
- group_weight: float32 [2048], P('ep'), may hold values from 0.2 to 1
- expert_weight: float32 [2048, 2], P('ep'), may hold values from 0.1 to 0.9
- group_choice: int32 [2048], P('ep'), may hold values from 0 to 3, as said below
- local_choice: int32 [2048, 2], P('ep'), may hold values from 0 to 3, as said below
- w_gate: bfloat16 [16, 2048, 512], P('ep', None, 'tp'), may hold values from -0.125 to 0.125
- w_up: bfloat16 [16, 2048, 512], P('ep', None, 'tp'), may hold values from -0.125 to 0.125
- w_down: bfloat16 [16, 512, 2048], P('ep', 'tp'), may hold values from -0.25 to 0.25
Outputs:
- token_grad: float32 [2048, 2048], P('ep', 'tp')
- group_weight_grad: float32 [2048], P('ep')
- expert_weight_grad: float32 [2048, 2], P('ep')
- w_gate_grad: float32 [16, 2048, 512], P('ep', None, 'tp')
- w_up_grad: float32 [16, 2048, 512], P('ep', None, 'tp')
- w_down_grad: float32 [16, 512, 2048], P('ep', 'tp')
Inputs may be any that keep to these rules, and one draw needn't show every extreme that they name: Among the 128 tokens of each device (aligned blocks of tokens), no expert 4 * group_choice + local_choice is named by more than 24 slots, and some expert is named by exactly 24 slots of every device. `local_choice`: the 2 local choices of a token differ.
All inputs are finite; a program needn't handle non-finite values.
Results may differ from a plain program's by a relative error of at most 0.006.
Values may be sent and summed in bfloat16 or wider, within the bound.
No kernel may reach another device: no remote copies, remote signals or barrier semaphores. Data moves between devices by JAX's collectives and lax.ppermute only.
A program may use at most 64 MiB of HBM per device.

v0:
```python
import functools

import jax
import jax.numpy as jnp
from jax import lax
from jax.experimental import pallas as pl
from jax.experimental.pallas import tpu as pltpu
from jax.sharding import PartitionSpec as P


EPG = 4
LANES = 128
F32 = jnp.float32
BF16 = jnp.bfloat16

ROWS_COLS = (((1,), (1,)), ((), ()))
COLS_ROWS = (((1,), (0,)), ((), ()))
ROWS_ROWS = (((0,), (0,)), ((), ()))


def dot(a, b, dims):
    return lax.dot_general(a, b, dims, preferred_element_type=F32)


def call(body, outs, flops=0, space=pltpu.VMEM, scratch=()):
    def run(*args):
        return pl.pallas_call(
            body,
            out_shape=outs,
            in_specs=[pl.BlockSpec(memory_space=space)] * len(args),
            out_specs=jax.tree.map(lambda _: pl.BlockSpec(memory_space=pltpu.VMEM), outs),
            scratch_shapes=scratch,
            compiler_params=pltpu.CompilerParams(vmem_limit_bytes=40 * 2**20),
            cost_estimate=pl.CostEstimate(flops=flops, bytes_accessed=0, transcendentals=0),
        )(*args)

    return run


def route_body(groups, cap, width, *refs):
    sources = refs[:6]
    own_out = refs[6]
    tok_out = refs[7 : 6 + groups]
    cot_out = refs[6 + groups : 5 + 2 * groups]
    choice_ref, local_ref, weight_ref, expert_ref, tok_ref, cot_ref, sems = refs[5 + 2 * groups :]
    count = tok_ref.shape[0]
    own = lax.axis_index("ep") // EPG
    start = pl.multiple_of(lax.axis_index("tp") * width, width)
    copies = []
    for k, (src, dst) in enumerate(
        zip(sources, (choice_ref, local_ref, weight_ref, expert_ref, tok_ref, cot_ref))
    ):
        if k >= 4:
            src = src.at[:, pl.ds(start, width)]
        copies.append(pltpu.make_async_copy(src, dst, sems.at[k]))
    for copy in copies:
        copy.start()
    for copy in copies[:4]:
        copy.wait()
    choice = choice_ref[...]
    padded = -(-groups // 8) * 8
    member = lax.broadcasted_iota(jnp.int32, (padded, count), 0) == choice
    before = (
        lax.broadcasted_iota(jnp.int32, (count, count), 0)
        < lax.broadcasted_iota(jnp.int32, (count, count), 1)
    ).astype(BF16)
    member = member.astype(F32)
    ahead = dot(member.astype(BF16), before, COLS_ROWS)
    place = jnp.sum(ahead * member, axis=0, keepdims=True).astype(jnp.int32)
    lane = lax.broadcasted_iota(jnp.int32, (LANES, count), 0)
    gates = jnp.zeros((LANES, count), F32)
    for k in range(local_ref.shape[0]):
        gate = (weight_ref[...] * expert_ref[k : k + 1, :]).astype(BF16).astype(F32)
        gates = gates + jnp.where(lane == local_ref[k : k + 1, :], gate, 0.0)
    gates = gates.astype(BF16)
    slot = lax.broadcasted_iota(jnp.int32, (cap, count), 0)
    picks = [
        ((slot == place) & (choice == (own ^ k))).astype(F32).astype(BF16)
        for k in range(groups)
    ]
    gate_rows = [dot(pick, gates, ROWS_COLS).astype(BF16) for pick in picks]
    copies[4].wait()
    for k in range(1, groups):
        tok_out[k - 1][...] = dot(picks[k], tok_ref[...], COLS_ROWS).astype(BF16)
    own_out[:, :width] = dot(picks[0], tok_ref[...], COLS_ROWS).astype(BF16)
    copies[5].wait()
    for k in range(1, groups):
        cot_out[k - 1][:, :width] = dot(picks[k], cot_ref[...], COLS_ROWS).astype(BF16)
        cot_out[k - 1][:, width:] = gate_rows[k]
    own_out[:, width : 2 * width] = dot(picks[0], cot_ref[...], COLS_ROWS).astype(BF16)
    own_out[:, 2 * width :] = gate_rows[0]


def picks_body(groups, cap, parts, choice_ref, out_ref):
    choice = choice_ref[...]
    count = choice.shape[1]
    own = lax.axis_index("ep") // EPG
    padded = -(-groups // 8) * 8
    member = (lax.broadcasted_iota(jnp.int32, (padded, count), 0) == choice).astype(F32)
    before = (
        lax.broadcasted_iota(jnp.int32, (count, count), 0)
        < lax.broadcasted_iota(jnp.int32, (count, count), 1)
    ).astype(BF16)
    ahead = dot(member.astype(BF16), before, COLS_ROWS)
    place = jnp.sum(ahead * member, axis=0, keepdims=True).astype(jnp.int32)
    slot = lax.broadcasted_iota(jnp.int32, (cap, count), 0)
    for i, k in enumerate(parts):
        pick = (slot == place) & (choice == (own ^ k))
        out_ref[pl.ds(i * cap, cap), :] = pick.astype(F32).astype(BF16)


def expert_body(lanes, width, *refs):
    tok = [refs[c * lanes : (c + 1) * lanes] for c in range(2)]
    cot = [refs[(2 + c) * lanes : (3 + c) * lanes] for c in range(2)]
    gate_w, up_w, down_w = refs[4 * lanes : 4 * lanes + 3]
    sums = refs[4 * lanes + 3 : 4 * lanes + 5]
    grads = refs[4 * lanes + 5 : 4 * lanes + 7]
    scaled_hidden = refs[4 * lanes + 7 : 4 * lanes + 9]
    rows = tok[0][0].shape[0]
    cols = gate_w.shape[1]
    mine = lax.axis_index("ep") % EPG
    rank = lax.axis_index("tp")
    spans = [
        pl.ds(pl.multiple_of(((rank + lanes - j) % lanes) * width, width), width)
        for j in range(lanes)
    ]
    lane = lax.broadcasted_iota(jnp.int32, (rows, LANES), 1)
    for c in range(2):
        pre_gate = jnp.zeros((rows, cols), F32)
        pre_up = jnp.zeros((rows, cols), F32)
        back = jnp.zeros((rows, cols), F32)
        for j in range(lanes):
            part = tok[c][j][...]
            pre_gate = pre_gate + dot(part, gate_w[spans[j], :], COLS_ROWS)
            pre_up = pre_up + dot(part, up_w[spans[j], :], COLS_ROWS)
            back = back + dot(cot[c][j][:, :width], down_w[:, spans[j]], ROWS_COLS)
        gates = cot[c][0][:, width:].astype(F32)
        gate = jnp.sum(jnp.where(lane == mine, gates, 0.0), axis=1, keepdims=True)
        sigma = jax.nn.sigmoid(pre_gate)
        swish = pre_gate * sigma
        hidden = swish * pre_up
        gate_part = jnp.sum(hidden * back, axis=1, keepdims=True)
        scaled = gate * back
        grad_gate = (scaled * pre_up * sigma * (1.0 + pre_gate * (1.0 - sigma))).astype(BF16)
        grad_up = (scaled * swish).astype(BF16)
        grads[c][:, :cols] = grad_gate
        grads[c][:, cols:] = grad_up
        scaled_hidden[c][...] = (gate * hidden).astype(BF16)
        for j in range(lanes):
            total = dot(grad_gate, gate_w[spans[j], :], ROWS_COLS)
            total = total + dot(grad_up, up_w[spans[j], :], ROWS_COLS)
            sums[c][:, j * width : (j + 1) * width] = total.astype(sums[c].dtype)
        high = gate_part.astype(BF16).astype(F32)
        low = gate_part - high
        tail = jnp.where(lane == mine, high, jnp.where(lane == mine + EPG, low, 0.0))
        sums[c][:, lanes * width :] = tail.astype(sums[c].dtype)


def weight_body(lanes, width, *refs):
    tok = [refs[b * lanes : (b + 1) * lanes] for b in range(4)]
    cot = [refs[(4 + b) * lanes : (5 + b) * lanes] for b in range(4)]
    grads = refs[8 * lanes : 8 * lanes + 4]
    scaled_hidden = refs[8 * lanes + 4 : 8 * lanes + 8]
    gate_out, up_out, down_out = refs[8 * lanes + 8 :]
    cols = gate_out.shape[1]
    rank = lax.axis_index("tp")
    chunk = min(width, 512)
    for j in range(lanes):
        base = ((rank + lanes - j) % lanes) * width
        for s in range(0, width, chunk):
            span = pl.ds(pl.multiple_of(base + s, chunk), chunk)
            total = dot(tok[0][j][:, s : s + chunk], grads[0][...], ROWS_ROWS)
            down = dot(scaled_hidden[0][...], cot[0][j][:, s : s + chunk], ROWS_ROWS)
            for b in range(1, 4):
                total = total + dot(tok[b][j][:, s : s + chunk], grads[b][...], ROWS_ROWS)
                down = down + dot(scaled_hidden[b][...], cot[b][j][:, s : s + chunk], ROWS_ROWS)
            gate_out[span, :] = total[:, :cols]
            up_out[span, :] = total[:, cols:]
            down_out[:, span] = down


def final_body(groups, cap, *refs):
    back = refs[:groups]
    pick_refs = refs[groups : groups + 3]
    local_ref, weight_ref, expert_ref = refs[groups + 3 : groups + 6]
    tok_out, group_out, expert_out = refs[groups + 6 :]
    count, width = tok_out.shape
    total = jnp.zeros((count, width), F32)
    held = jnp.zeros((LANES, count), F32)
    for k in range(groups):
        pick = pick_refs[min(k, 2)][pl.ds(max(k - 2, 0) * cap, cap), :]
        total = total + dot(pick, back[k][:, :width], ROWS_ROWS)
        held = held + dot(back[k][:, width:], pick, ROWS_ROWS)
    tok_out[...] = total
    lane = lax.broadcasted_iota(jnp.int32, (LANES, count), 0)
    group_sum = jnp.zeros((1, count), F32)
    for k in range(local_ref.shape[0]):
        grad = jnp.sum(
            jnp.where(lane == local_ref[k : k + 1, :], held, 0.0), axis=0, keepdims=True
        )
        group_sum = group_sum + expert_ref[k : k + 1, :] * grad
        expert_out[k : k + 1, :] = weight_ref[...] * grad
    group_out[...] = group_sum


def layer(
    tokens, cotangent, group_weight, expert_weight, group_choice, local_choice, w_gate, w_up, w_down
):
    count, features = tokens.shape
    picks = expert_weight.shape[1]
    experts = lax.axis_size("ep")
    lanes = lax.axis_size("tp")
    groups = experts // EPG
    width = features // lanes
    capacity = picks * (3 * count // (2 * experts))
    cap = min(count, EPG * capacity // picks)
    cap = -(-cap // 16) * 16
    rows = groups * cap
    cols = w_gate.shape[2]

    def along_groups(a, k):
        return lax.ppermute(a, "ep", [(e, e ^ (k * EPG)) for e in range(experts)])

    def along_side(a):
        return lax.ppermute(a, "ep", [(e, e ^ 2) for e in range(experts)])

    def along_core(a):
        return lax.ppermute(a, "ep", [(e, e ^ 1) for e in range(experts)])

    def along_tp(a, j):
        return lax.ppermute(a, "tp", [(r, (r + j) % lanes) for r in range(lanes)])

    shape = jax.ShapeDtypeStruct
    choice_row = group_choice.reshape(1, count)
    weight_row = group_weight.reshape(1, count)
    local_rows = local_choice.T
    expert_rows = expert_weight.T
    routed = call(
        functools.partial(route_body, groups, cap, width),
        [shape((cap, 2 * width + LANES), BF16)]
        + [shape((cap, width), BF16)] * (groups - 1)
        + [shape((cap, width + LANES), BF16)] * (groups - 1),
        space=pltpu.HBM,
        scratch=[
            pltpu.VMEM((1, count), jnp.int32),
            pltpu.VMEM((picks, count), jnp.int32),
            pltpu.VMEM((1, count), F32),
            pltpu.VMEM((picks, count), F32),
            pltpu.VMEM((count, width), BF16),
            pltpu.VMEM((count, width), BF16),
            pltpu.SemaphoreType.DMA((6,)),
        ],
    )(
        *(
            pltpu.with_memory_space_constraint(a, pltpu.HBM)
            for a in (choice_row, local_rows, weight_row, expert_rows, tokens, cotangent)
        )
    )
    parts = [[0], [1], list(range(2, groups))]
    picked = [
        call(
            functools.partial(picks_body, groups, cap, part),
            shape((len(part) * cap, count), BF16),
            10**6,
        )(choice_row)
        for part in parts
    ]
    own = routed[0]
    others = range(groups - 1, 0, -1)
    tok_sent = {k: along_groups(routed[k], k) for k in others}
    own_side = along_side(own)
    own_lane = [along_tp(own, j) for j in range(1, lanes)]
    cot_sent = {k: along_groups(routed[groups - 1 + k], k) for k in others}
    own_tok_both = [along_tp(own_side[:, :width], j) for j in range(1, lanes)]
    own_cot_both = [along_side(a[:, width : 2 * width]) for a in own_lane]
    tok = jnp.concatenate([tok_sent[k] for k in range(1, groups)], axis=0)
    cot = jnp.concatenate([cot_sent[k] for k in range(1, groups)], axis=0)
    cot_bare = jnp.concatenate([cot_sent[k][:, :width] for k in range(1, groups)], axis=0)
    tok_side = along_side(tok)
    tok_lane = [along_tp(tok, j) for j in range(1, lanes)]
    cot_side = along_side(cot)
    cot_lane = [along_tp(cot_bare, j) for j in range(1, lanes)]
    cut = width // 2 if width % (2 * LANES) == 0 else width

    def diagonal(side, lane):
        parts_a = [along_tp(side[:, :cut], j) for j in range(1, lanes)]
        if cut == width:
            return parts_a
        parts_b = [along_side(a[:, cut:width]) for a in lane]
        return [jnp.concatenate([a, b], axis=1) for a, b in zip(parts_a, parts_b)]

    tok_both = diagonal(tok_side, tok_lane)
    cot_both = diagonal(cot_side, cot_lane)

    def join(head, rest):
        return jnp.concatenate([head, rest], axis=0)

    tok_near = [join(own[:, :width], tok)]
    tok_near += [join(a[:, :width], b) for a, b in zip(own_lane, tok_lane)]
    cot_near = [join(own[:, width:], cot)]
    cot_near += [join(a[:, width : 2 * width], b) for a, b in zip(own_lane, cot_lane)]
    tok_far = [join(own_side[:, :width], tok_side)]
    tok_far += [join(a, b) for a, b in zip(own_tok_both, tok_both)]
    cot_far = [join(own_side[:, width:], cot_side)]
    cot_far += [join(a, b) for a, b in zip(own_cot_both, cot_both)]
    first, second, third = w_gate[0], w_up[0], w_down[0]
    work = 2 * 5 * 2 * rows * features * cols

    def experts_on(tok_list, cot_list):
        tok_other = [along_core(a) for a in tok_list]
        cot_other = [along_core(a) for a in cot_list]
        outs = call(
            functools.partial(expert_body, lanes, width),
            [shape((rows, features + LANES), F32), shape((rows, features + LANES), BF16)]
            + [shape((rows, 2 * cols), BF16)] * 2
            + [shape((rows, cols), BF16)] * 2,
            work,
        )(*tok_list, *tok_other, *cot_list, *cot_other, first, second, third)
        return outs, tok_list + tok_other, cot_list + cot_other

    near, tok_a, cot_a = experts_on(tok_near, cot_near)
    far, tok_b, cot_b = experts_on(tok_far, cot_far)
    near_sum = near[0] + along_core(near[1]).astype(F32)
    far_sum = far[0] + along_core(far[1]).astype(F32)
    if lanes == 2:
        half = width // 2
        tail = far_sum[:, features:]
        side_out = jnp.concatenate(
            [far_sum[:, :half], far_sum[:, width : width + half], tail], axis=1
        ).astype(BF16)
        lane_out = jnp.concatenate(
            [near_sum[:, width + half : features], far_sum[:, width + half : features]], axis=0
        ).astype(BF16)
        side_in = along_side(side_out).astype(F32)
        lane_in = along_tp(lane_out, 1).astype(F32)
        lane_next = jnp.concatenate(
            [
                near_sum[:, width : width + half] + side_in[:, half:width],
                near_sum[:, features:] + side_in[:, width:],
            ],
            axis=1,
        )
        side_next = (far_sum[:, half:width] + lane_in[rows:]).astype(BF16)
        lane_last = along_tp(lane_next.astype(BF16), 1).astype(F32)
        side_last = along_side(side_next).astype(F32)
        tail = lane_next[:, half:] + lane_last[:, half:]
        body = jnp.concatenate(
            [
                near_sum[:, :half] + side_in[:, :half] + lane_last[:, :half],
                near_sum[:, half:width] + lane_in[:rows] + side_last,
            ],
            axis=1,
        )
    else:
        both = near_sum + along_side(far_sum.astype(BF16)).astype(F32)
        tail = both[:, features:]
        body = both[:, :width]
        for j in range(1, lanes):
            piece = jnp.concatenate(
                [both[:, j * width : (j + 1) * width], both[:, features:]], axis=1
            )
            piece = along_tp(piece.astype(BF16), lanes - j).astype(F32)
            body = body + piece[:, :width]
            tail = tail + piece[:, width:]
    held = tail[:, :EPG] + tail[:, EPG : 2 * EPG]
    held = jnp.pad(held, ((0, 0), (0, LANES - EPG)))
    result = jnp.concatenate([body, held], axis=1).astype(BF16)
    sent = {k: along_groups(result[k * cap : (k + 1) * cap], k) for k in others}
    returned = [result[:cap]] + [sent[k] for k in range(1, groups)]
    grads = list(near[2:4]) + list(far[2:4])
    scaled_hidden = list(near[4:6]) + list(far[4:6])
    first_grad, second_grad, third_grad = call(
        functools.partial(weight_body, lanes, width),
        [shape((features, cols), F32)] * 2 + [shape((cols, features), F32)],
        2 * 3 * 4 * rows * features * cols,
    )(*tok_a, *tok_b, *cot_a, *cot_b, *grads, *scaled_hidden)
    token_grad, group_grad, expert_grad = call(
        functools.partial(final_body, groups, cap),
        [shape((count, width), F32), shape((1, count), F32), shape((picks, count), F32)],
    )(*returned, *picked, local_rows, weight_row, expert_rows)
    return (
        token_grad,
        group_grad.reshape(count),
        expert_grad.T,
        first_grad[None],
        second_grad[None],
        third_grad[None],
    )


def solution(mesh):
    in_specs = (
        P("ep", None),
        P("ep", None),
        P("ep"),
        P("ep", None),
        P("ep"),
        P("ep", None),
        P("ep", None, "tp"),
        P("ep", None, "tp"),
        P("ep", "tp", None),
    )
    out_specs = (
        P("ep", "tp"),
        P("ep"),
        P("ep", None),
        P("ep", None, "tp"),
        P("ep", None, "tp"),
        P("ep", "tp", None),
    )
    return jax.shard_map(layer, mesh=mesh, in_specs=in_specs, out_specs=out_specs, check_vma=False)
```

profile of v0, /device:TPU:0, one launch (start us, length us, event | category | flops | bytes accessed | tf_op | source)
XLA Modules:
  0.0 100.1 jit_solution(10432640165391144256)
XLA Ops:
  0.6 1.7 %shard_map.136 = (bf16[48,2176]{1,0:T(8,128)(2,1)S(1)}, bf16[48,1024]{1,0:T(8,128)(2,1)S(1)}, bf16[48,1024]{1,0:T(8,128)(2,1)S(1)}, bf16[48,1024]{1,0:T(8,128)(2...) custom-call(s32[1,128]{1,0:T(1,128)} %bitcast.12, ...), custom_call_target="tpu_custom_call" | custom-call | tf_op jit(solution)/shard_map/pallas_call | solution.py:27
  2.3 3.1 %collective-permute-start = (bf16[48,1024]{1,0:T(8,128)(2,1)S(1)}, bf16[48,1024]{1,0:T(8,128)(2,1)S(1)}, u32[]{:S(2)}, u32[]{:S(2)}) collective-permute-start(bf16[48,1024]{1,0:T(8,128)(2,1)S(1)} %get-tuple-element.32), channel_id=1, source_target_pairs={{0,8},{2,10},{4,12},{6,14},{8,0},{10,2},{12,4},{14,6},{16,24},{18,... | collective-permute-start | bytes 294920 | tf_op jit(solution)/shard_map/ppermute | solution.py:222
  5.4 1.5 %collective-permute-start.14 = (bf16[48,2176]{1,0:T(8,128)(2,1)S(1)}, bf16[48,2176]{1,0:T(8,128)(2,1)S(1)}, u32[]{:S(2)}, u32[]{:S(2)}) collective-permute-start(bf16[48,2176]{1,0:T(8,128)(2,1)S(1)} %get-tuple-element.31), channel_id=1, source_target_pairs={{0,4},{2,6},{4,0},{6,2},{8,12},{10,14},{12,8},{14,10},{16,20},{18,... | collective-permute-start | bytes 626696 | tf_op jit(solution)/shard_map/ppermute | solution.py:225
  6.9 1.5 %collective-permute-start.3 = (bf16[48,2176]{1,0:T(8,128)(2,1)S(1)}, bf16[48,2176]{1,0:T(8,128)(2,1)S(1)}, u32[]{:S(2)}, u32[]{:S(2)}) collective-permute-start(bf16[48,2176]{1,0:T(8,128)(2,1)S(1)} %get-tuple-element.31), channel_id=1, source_target_pairs={{0,1},{1,0},{2,3},{3,2},{4,5},{5,4},{6,7},{7,6},{8,9},{9,8},{10,11... | collective-permute-start | bytes 626696 | tf_op jit(solution)/shard_map/ppermute | solution.py:231
  8.4 2.6 %collective-permute-start.1 = (bf16[48,1024]{1,0:T(8,128)(2,1)S(1)}, bf16[48,1024]{1,0:T(8,128)(2,1)S(1)}, u32[]{:S(2)}, u32[]{:S(2)}) collective-permute-start(bf16[48,1024]{1,0:T(8,128)(2,1)S(1)} %get-tuple-element.33), channel_id=1, source_target_pairs={{0,16},{2,18},{4,20},{6,22},{8,24},{10,26},{12,28},{14,30},{16,0},... | collective-permute-start | bytes 294920 | tf_op jit(solution)/shard_map/ppermute | solution.py:222
  11.0 0.2 collective-permute-start.2
  11.3 0.0 collective-permute-done
  11.3 3.7 %collective-permute-start.9 = (bf16[48,1152]{1,0:T(8,128)(2,1)S(1)}, bf16[48,1152]{1,0:T(8,128)(2,1)S(1)}, u32[]{:S(2)}, u32[]{:S(2)}) collective-permute-start(bf16[48,1152]{1,0:T(8,128)(2,1)S(1)} %get-tuple-element.37), channel_id=1, source_target_pairs={{0,24},{2,26},{4,28},{6,30},{8,16},{10,18},{12,20},{14,22},{16,8},... | collective-permute-start | bytes 331784 | tf_op jit(solution)/shard_map/ppermute | solution.py:222
  15.0 6.8 %collective-permute-done.1 = bf16[48,1024]{1,0:T(8,128)(2,1)S(1)} collective-permute-done((bf16[48,1024]{1,0:T(8,128)(2,1)S(1)}, bf16[48,1024]{1,0:T(8,128)(2,1)S(1)}, u32[]{:S(2)}, u32[]{:S(2)}) %collective-permute-start.1) | collective-permute-done | bytes 98336 | tf_op jit(solution)/shard_map/ppermute | solution.py:222
  21.7 3.3 %collective-permute-start.7 = (bf16[48,1152]{1,0:T(8,128)(2,1)S(1)}, bf16[48,1152]{1,0:T(8,128)(2,1)S(1)}, u32[]{:S(2)}, u32[]{:S(2)}) collective-permute-start(bf16[48,1152]{1,0:T(8,128)(2,1)S(1)} %get-tuple-element.35), channel_id=1, source_target_pairs={{0,8},{2,10},{4,12},{6,14},{8,0},{10,2},{12,4},{14,6},{16,24},{18,... | collective-permute-start | bytes 331784 | tf_op jit(solution)/shard_map/ppermute | solution.py:222
  25.1 0.1 collective-permute-start.15
  25.2 3.7 %collective-permute-done.8 = bf16[48,1152]{1,0:T(8,128)(2,1)S(1)} collective-permute-done((bf16[48,1152]{1,0:T(8,128)(2,1)S(1)}, bf16[48,1152]{1,0:T(8,128)(2,1)S(1)}, u32[]{:S(2)}, u32[]{:S(2)}) %collective-permute-start.8) | collective-permute-done | bytes 110624 | tf_op jit(solution)/shard_map/ppermute | solution.py:222
  28.8 0.6 collective-permute-start.4
  29.6 1.5 %collective-permute-start.10 = (bf16[144,1024]{1,0:T(8,128)(2,1)S(1)}, bf16[144,1024]{1,0:T(8,128)(2,1)S(1)}, u32[]{:S(2)}, u32[]{:S(2)}) collective-permute-start(bf16[144,1024]{1,0:T(8,128)(2,1)S(1)} %pad_maximum_fusion.9), channel_id=1, source_target_pairs={{0,1},{1,0},{2,3},{3,2},{4,5},{5,4},{6,7},{7,6},{8,9},{9,8},{10,11... | collective-permute-start | bytes 884744 | tf_op jit(solution)/shard_map/ppermute | solution.py:231
  31.1 7.6 %collective-permute-done.4 = bf16[144,1024]{1,0:T(8,128)(2,1)S(1)} collective-permute-done((bf16[144,1024]{1,0:T(8,128)(2,1)S(1)}, bf16[144,1024]{1,0:T(8,128)(2,1)S(1)}, u32[]{:S(2)}, u32[]{:S(2)}) %collective-permute-start.4) | collective-permute-done | bytes 294944 | tf_op jit(solution)/shard_map/ppermute | solution.py:231
  38.7 0.6 collective-permute-start.21
  39.3 3.7 %collective-permute-done.10 = bf16[144,1024]{1,0:T(8,128)(2,1)S(1)} collective-permute-done((bf16[144,1024]{1,0:T(8,128)(2,1)S(1)}, bf16[144,1024]{1,0:T(8,128)(2,1)S(1)}, u32[]{:S(2)}, u32[]{:S(2)}) %collective-permute-start.10) | collective-permute-done | bytes 294944 | tf_op jit(solution)/shard_map/ppermute | solution.py:231
  43.1 0.0 copy-start.4
  43.1 0.0 copy-start.5
  43.1 0.0 copy-start.6
  43.1 0.6 collective-permute-start.6
  43.7 0.1 collective-permute-start.12
  43.9 1.9 %collective-permute-done.21 = bf16[144,1152]{1,0:T(8,128)(2,1)S(1)} collective-permute-done((bf16[144,1152]{1,0:T(8,128)(2,1)S(1)}, bf16[144,1152]{1,0:T(8,128)(2,1)S(1)}, u32[]{:S(2)}, u32[]{:S(2)}) %collective-permute-start.21) | collective-permute-done | bytes 331808 | tf_op jit(solution)/shard_map/ppermute | solution.py:225
  45.8 0.6 collective-permute-start.16
  46.5 0.7 collective-permute-start.18
  47.1 1.5 %collective-permute-start.17 = (bf16[144,512]{1,0:T(8,128)(2,1)S(1)}, bf16[144,512]{1,0:T(8,128)(2,1)S(1)}, u32[]{:S(2)}, u32[]{:S(2)}) collective-permute-start(bf16[144,512]{1,0:T(8,128)(2,1)S(1)} %slice.158), channel_id=1, source_target_pairs={{0,1},{1,0},{2,3},{3,2},{4,5},{5,4},{6,7},{7,6},{8,9},{9,8},{10,11... | collective-permute-start | bytes 442376 | tf_op jit(solution)/shard_map/ppermute | solution.py:231
  48.6 1.4 %collective-permute-start.24 = (bf16[144,512]{1,0:T(8,128)(2,1)S(1)}, bf16[144,512]{1,0:T(8,128)(2,1)S(1)}, u32[]{:S(2)}, u32[]{:S(2)}) collective-permute-start(bf16[144,512]{1,0:T(8,128)(2,1)S(1)} %slice.162), channel_id=1, source_target_pairs={{0,4},{2,6},{4,0},{6,2},{8,12},{10,14},{12,8},{14,10},{16,20},{18,... | collective-permute-start | bytes 442376 | tf_op jit(solution)/shard_map/ppermute | solution.py:225
  50.0 0.6 collective-permute-start.23
  50.6 3.5 %shard_map.137 = (f32[192,2176]{1,0:T(8,128)S(1)}, bf16[192,2176]{1,0:T(8,128)(2,1)S(1)}, bf16[192,512]{1,0:T(8,128)(2,1)S(1)}, bf16[192,512]{1,0:T(8,128)(2,1)S...) custom-call(bf16[192,1024]{1,0:T(8,128)(2,1)S(1)} %pad_maximum_fusion.3.refs_0_, ...), custom_call_target="tpu_custom_call" | custom-call | flops 2013265920 | tf_op jit(solution)/shard_map/pallas_call | solution.py:27
  54.1 0.7 collective-permute-start.22
  54.8 0.5 collective-permute-start.13
  55.4 3.5 %collective-permute-done.22 = bf16[48,1024]{1,0:T(8,128)(2,1)S(1)} collective-permute-done((bf16[48,1024]{1,0:T(8,128)(2,1)S(1)}, bf16[48,1024]{1,0:T(8,128)(2,1)S(1)}, u32[]{:S(2)}, u32[]{:S(2)}) %collective-permute-start.22) | collective-permute-done | bytes 98336 | tf_op jit(solution)/shard_map/ppermute | solution.py:225
  58.8 0.5 collective-permute-start.20
  59.4 0.1 collective-permute-start.26
  59.5 1.1 %collective-permute-done.25.refs_6_.refs_14_ = bf16[192,1152]{1,0:T(8,128)(2,1)S(1)} collective-permute-done((bf16[192,1152]{1,0:T(8,128)(2,1)S(1)}, bf16[192,1152]{1,0:T(8,128)(2,1)S(1)}, u32[]{:S(2)}, u32[]{:S(2)}) %collective-permute-start.25) | collective-permute-done | bytes 442400 | tf_op jit(solution)/shard_map/ppermute | solution.py:228
  60.6 0.6 collective-permute-done.20.refs_3_.refs_7_
  61.2 0.6 collective-permute-done.26.refs_7_.refs_15_
  61.7 3.5 %shard_map.138 = (f32[192,2176]{1,0:T(8,128)S(1)}, bf16[192,2176]{1,0:T(8,128)(2,1)S(1)}, bf16[192,512]{1,0:T(8,128)(2,1)S(1)}, bf16[192,512]{1,0:T(8,128)(2,1)S...) custom-call(bf16[192,1024]{1,0:T(8,128)(2,1)S(1)} %pad_maximum_fusion.6.refs_0_.refs_4_, ...), custom_call_target="tpu_custom_call" | custom-call | flops 2013265920 | tf_op jit(solution)/shard_map/pallas_call | solution.py:27
  65.3 0.2 collective-permute-start.27
  65.5 0.1 convert_add_fusion.1
  65.7 2.0 %collective-permute-done.27 = bf16[192,2176]{1,0:T(8,128)(2,1)S(1)} collective-permute-done((bf16[192,2176]{1,0:T(8,128)(2,1)S(1)}, bf16[192,2176]{1,0:T(8,128)(2,1)S(1)}, u32[]{:S(2)}, u32[]{:S(2)}) %collective-permute-start.27) | collective-permute-done | bytes 835616 | tf_op jit(solution)/shard_map/ppermute | solution.py:228
  67.7 0.2 fusion.9
  67.9 0.0 copy-start
  68.0 0.7 collective-permute-start.28
  68.7 1.5 %collective-permute-start.30 = (bf16[384,512]{1,0:T(8,128)(2,1)S(1)}, bf16[384,512]{1,0:T(8,128)(2,1)S(1)}, u32[]{:S(2)}, u32[]{:S(2)}) collective-permute-start(bf16[384,512]{1,0:T(8,128)(2,1)S(1)} %pad_maximum_fusion.7), channel_id=1, source_target_pairs={{0,1},{1,0},{2,3},{3,2},{4,5},{5,4},{6,7},{7,6},{8,9},{9,8},{10,11... | collective-permute-start | bytes 1179656 | tf_op jit(solution)/shard_map/ppermute | solution.py:231
  70.2 0.1 shard_map.139.refs_4_
  70.4 0.1 shard_map.140.refs_5_
  70.5 0.1 shard_map.141.refs_6_
  70.7 9.0 %collective-permute-done.30 = bf16[384,512]{1,0:T(8,128)(2,1)S(1)} collective-permute-done((bf16[384,512]{1,0:T(8,128)(2,1)S(1)}, bf16[384,512]{1,0:T(8,128)(2,1)S(1)}, u32[]{:S(2)}, u32[]{:S(2)}) %collective-permute-start.30) | collective-permute-done | bytes 393248 | tf_op jit(solution)/shard_map/ppermute | solution.py:231
  79.6 0.1 convert_element_type.31
  79.7 0.6 collective-permute-done.28
  80.3 0.1 convert_element_type.29
  80.5 1.5 %collective-permute-start.29 = (bf16[192,640]{1,0:T(8,128)(2,1)S(1)}, bf16[192,640]{1,0:T(8,128)(2,1)S(1)}, u32[]{:S(2)}, u32[]{:S(2)}) collective-permute-start(bf16[192,640]{1,0:T(8,128)(2,1)S(1)} %pad_maximum_fusion.10), channel_id=1, source_target_pairs={{0,1},{1,0},{2,3},{3,2},{4,5},{5,4},{6,7},{7,6},{8,9},{9,8},{10,11... | collective-permute-start | bytes 737288 | tf_op jit(solution)/shard_map/ppermute | solution.py:231
  82.0 0.1 fusion.2
  82.0 1.0 collective-permute-start.31
  83.0 4.7 %collective-permute-done.29 = bf16[192,640]{1,0:T(8,128)(2,1)S(1)} collective-permute-done((bf16[192,640]{1,0:T(8,128)(2,1)S(1)}, bf16[192,640]{1,0:T(8,128)(2,1)S(1)}, u32[]{:S(2)}, u32[]{:S(2)}) %collective-permute-start.29) | collective-permute-done | bytes 245792 | tf_op jit(solution)/shard_map/ppermute | solution.py:231
  87.7 0.1 fusion.7
  87.8 0.1 collective-permute-done.31
  87.9 0.1 fusion.5
  88.2 0.1 collective-permute-start.32
  88.2 3.1 %collective-permute-start.33 = (bf16[48,1152]{1,0:T(8,128)(2,1)S(1)}, bf16[48,1152]{1,0:T(8,128)(2,1)S(1)}, u32[]{:S(2)}, u32[]{:S(2)}) collective-permute-start(bf16[48,1152]{1,0:T(8,128)(2,1)S(1)} %get-tuple-element.64), channel_id=1, source_target_pairs={{0,16},{2,18},{4,20},{6,22},{8,24},{10,26},{12,28},{14,30},{16,0},... | collective-permute-start | bytes 331784 | tf_op jit(solution)/shard_map/ppermute | solution.py:222
  91.4 1.2 %collective-permute-start.34 = (bf16[48,1152]{1,0:T(8,128)(2,1)S(1)}, bf16[48,1152]{1,0:T(8,128)(2,1)S(1)}, u32[]{:S(2)}, u32[]{:S(2)}) collective-permute-start(bf16[48,1152]{1,0:T(8,128)(2,1)S(1)} %get-tuple-element.63), channel_id=1, source_target_pairs={{0,24},{2,26},{4,28},{6,30},{8,16},{10,18},{12,20},{14,22},{16,8},... | collective-permute-start | bytes 331784 | tf_op jit(solution)/shard_map/ppermute | solution.py:222
  92.6 6.2 %shard_map.143 = (f32[2048,256]{1,0:T(8,128)}, f32[2048,256]{1,0:T(8,128)}, f32[256,2048]{1,0:T(8,128)}) custom-call(bf16[192,1024]{1,0:T(8,128)(2,1)S(1)} %pad_maximum_fusion.3.refs_0_, bf16[192,1024]{1,0:T(8,128)(2,1)S(1)} %pad_maximum_fusion.4.refs_1_, bf16[192,1024]{1,0:T(8,128)(2,1)S(1)} %collective-permute-done.5.refs_2_, ...), custom_call_target="tpu_custom_call" | custom-call | flops 2415919104 | tf_op jit(solution)/shard_map/pallas_call | solution.py:27
  98.8 1.3 %shard_map.142 = (f32[128,1024]{1,0:T(8,128)}, f32[1,128]{1,0:T(1,128)}, f32[2,128]{1,0:T(2,128)}) custom-call(bf16[48,1152]{1,0:T(8,128)(2,1)S(1)} %get-tuple-element.66.refs_0_, bf16[48,1152]{1,0:T(8,128)(2,1)S(1)} %collective-permute-done.32.refs_1_, bf16[48,1152]{1,0:T(8,128)(2,1)S(1)} %collective-permute-done.33.refs_2_, ...), custom_call_target="tpu_custom_call" | custom-call | tf_op jit(solution)/shard_map/pallas_call | solution.py:27
  (72 shorter events, 0.9 us)
Async XLA Ops:
  2.3 9.0 %collective-permute-start = (bf16[48,1024]{1,0:T(8,128)(2,1)S(1)}, bf16[48,1024]{1,0:T(8,128)(2,1)S(1)}, u32[]{:S(2)}, u32[]{:S(2)}) collective-permute-start(bf16[48,1024]{1,0:T(8,128)(2,1)S(1)} %get-tuple-element.32), channel_id=1, source_target_pairs={{0,8},{2,10},{4,12},{6,14},{8,0},{10,2},{12,4},{14,6},{16,24},{18,... | collective-permute-start | bytes 294920 | tf_op jit(solution)/shard_map/ppermute | solution.py:222
  5.4 37.7 %collective-permute-start.14 = (bf16[48,2176]{1,0:T(8,128)(2,1)S(1)}, bf16[48,2176]{1,0:T(8,128)(2,1)S(1)}, u32[]{:S(2)}, u32[]{:S(2)}) collective-permute-start(bf16[48,2176]{1,0:T(8,128)(2,1)S(1)} %get-tuple-element.31), channel_id=1, source_target_pairs={{0,4},{2,6},{4,0},{6,2},{8,12},{10,14},{12,8},{14,10},{16,20},{18,... | collective-permute-start | bytes 626696 | tf_op jit(solution)/shard_map/ppermute | solution.py:225
  6.9 22.6 %collective-permute-start.3 = (bf16[48,2176]{1,0:T(8,128)(2,1)S(1)}, bf16[48,2176]{1,0:T(8,128)(2,1)S(1)}, u32[]{:S(2)}, u32[]{:S(2)}) collective-permute-start(bf16[48,2176]{1,0:T(8,128)(2,1)S(1)} %get-tuple-element.31), channel_id=1, source_target_pairs={{0,1},{1,0},{2,3},{3,2},{4,5},{5,4},{6,7},{7,6},{8,9},{9,8},{10,11... | collective-permute-start | bytes 626696 | tf_op jit(solution)/shard_map/ppermute | solution.py:231
  8.4 13.3 %collective-permute-start.1 = (bf16[48,1024]{1,0:T(8,128)(2,1)S(1)}, bf16[48,1024]{1,0:T(8,128)(2,1)S(1)}, u32[]{:S(2)}, u32[]{:S(2)}) collective-permute-start(bf16[48,1024]{1,0:T(8,128)(2,1)S(1)} %get-tuple-element.33), channel_id=1, source_target_pairs={{0,16},{2,18},{4,20},{6,22},{8,24},{10,26},{12,28},{14,30},{16,0},... | collective-permute-start | bytes 294920 | tf_op jit(solution)/shard_map/ppermute | solution.py:222
  11.0 10.7 %collective-permute-start.2 = (bf16[48,1024]{1,0:T(8,128)(2,1)S(1)}, bf16[48,1024]{1,0:T(8,128)(2,1)S(1)}, u32[]{:S(2)}, u32[]{:S(2)}) collective-permute-start(bf16[48,1024]{1,0:T(8,128)(2,1)S(1)} %get-tuple-element.34), channel_id=1, source_target_pairs={{0,24},{2,26},{4,28},{6,30},{8,16},{10,18},{12,20},{14,22},{16,8},... | collective-permute-start | bytes 294920 | tf_op jit(solution)/shard_map/ppermute | solution.py:222
  11.3 13.8 %collective-permute-start.9 = (bf16[48,1152]{1,0:T(8,128)(2,1)S(1)}, bf16[48,1152]{1,0:T(8,128)(2,1)S(1)}, u32[]{:S(2)}, u32[]{:S(2)}) collective-permute-start(bf16[48,1152]{1,0:T(8,128)(2,1)S(1)} %get-tuple-element.37), channel_id=1, source_target_pairs={{0,24},{2,26},{4,28},{6,30},{8,16},{10,18},{12,20},{14,22},{16,8},... | collective-permute-start | bytes 331784 | tf_op jit(solution)/shard_map/ppermute | solution.py:222
  21.7 7.1 %collective-permute-start.8 = (bf16[48,1152]{1,0:T(8,128)(2,1)S(1)}, bf16[48,1152]{1,0:T(8,128)(2,1)S(1)}, u32[]{:S(2)}, u32[]{:S(2)}) collective-permute-start(bf16[48,1152]{1,0:T(8,128)(2,1)S(1)} %get-tuple-element.36), channel_id=1, source_target_pairs={{0,16},{2,18},{4,20},{6,22},{8,24},{10,26},{12,28},{14,30},{16,0},... | collective-permute-start | bytes 331784 | tf_op jit(solution)/shard_map/ppermute | solution.py:222
  21.7 7.7 %collective-permute-start.7 = (bf16[48,1152]{1,0:T(8,128)(2,1)S(1)}, bf16[48,1152]{1,0:T(8,128)(2,1)S(1)}, u32[]{:S(2)}, u32[]{:S(2)}) collective-permute-start(bf16[48,1152]{1,0:T(8,128)(2,1)S(1)} %get-tuple-element.35), channel_id=1, source_target_pairs={{0,8},{2,10},{4,12},{6,14},{8,0},{10,2},{12,4},{14,6},{16,24},{18,... | collective-permute-start | bytes 331784 | tf_op jit(solution)/shard_map/ppermute | solution.py:222
  25.1 18.6 %collective-permute-start.15 = (bf16[144,1024]{1,0:T(8,128)(2,1)S(1)}, bf16[144,1024]{1,0:T(8,128)(2,1)S(1)}, u32[]{:S(2)}, u32[]{:S(2)}) collective-permute-start(bf16[144,1024]{1,0:T(8,128)(2,1)S(1)} %constant_dynamic-update-slice_fusion), channel_id=1, source_target_pairs={{0,4},{2,6},{4,0},{6,2},{8,12},{10,14},{12,8},{14,10},{16,20},{18,... | collective-permute-start | bytes 884744 | tf_op jit(solution)/shard_map/ppermute | solution.py:225
  28.8 9.9 %collective-permute-start.4 = (bf16[144,1024]{1,0:T(8,128)(2,1)S(1)}, bf16[144,1024]{1,0:T(8,128)(2,1)S(1)}, u32[]{:S(2)}, u32[]{:S(2)}) collective-permute-start(bf16[144,1024]{1,0:T(8,128)(2,1)S(1)} %constant_dynamic-update-slice_fusion), channel_id=1, source_target_pairs={{0,1},{1,0},{2,3},{3,2},{4,5},{5,4},{6,7},{7,6},{8,9},{9,8},{10,11... | collective-permute-start | bytes 884744 | tf_op jit(solution)/shard_map/ppermute | solution.py:231
  29.4 17.1 %collective-permute-start.5 = (bf16[192,1024]{1,0:T(8,128)(2,1)S(1)}, bf16[192,1024]{1,0:T(8,128)(2,1)S(1)}, u32[]{:S(2)}, u32[]{:S(2)}) collective-permute-start(bf16[192,1024]{1,0:T(8,128)(2,1)S(1)} %pad_maximum_fusion.3.refs_0_), channel_id=1, source_target_pairs={{0,2},{2,0},{4,6},{6,4},{8,10},{10,8},{12,14},{14,12},{16,18},{18,... | collective-permute-start | bytes 1179656 | tf_op jit(solution)/shard_map/ppermute | solution.py:228
  29.6 13.5 %collective-permute-start.10 = (bf16[144,1024]{1,0:T(8,128)(2,1)S(1)}, bf16[144,1024]{1,0:T(8,128)(2,1)S(1)}, u32[]{:S(2)}, u32[]{:S(2)}) collective-permute-start(bf16[144,1024]{1,0:T(8,128)(2,1)S(1)} %pad_maximum_fusion.9), channel_id=1, source_target_pairs={{0,1},{1,0},{2,3},{3,2},{4,5},{5,4},{6,7},{7,6},{8,9},{9,8},{10,11... | collective-permute-start | bytes 884744 | tf_op jit(solution)/shard_map/ppermute | solution.py:231
  38.7 7.1 %collective-permute-start.21 = (bf16[144,1152]{1,0:T(8,128)(2,1)S(1)}, bf16[144,1152]{1,0:T(8,128)(2,1)S(1)}, u32[]{:S(2)}, u32[]{:S(2)}) collective-permute-start(bf16[144,1152]{1,0:T(8,128)(2,1)S(1)} %pad_maximum_fusion.8), channel_id=1, source_target_pairs={{0,4},{2,6},{4,0},{6,2},{8,12},{10,14},{12,8},{14,10},{16,20},{18,... | collective-permute-start | bytes 995336 | tf_op jit(solution)/shard_map/ppermute | solution.py:225
  43.1 4.1 %collective-permute-start.11 = (bf16[192,1152]{1,0:T(8,128)(2,1)S(1)}, bf16[192,1152]{1,0:T(8,128)(2,1)S(1)}, u32[]{:S(2)}, u32[]{:S(2)}) collective-permute-start(bf16[192,1152]{1,0:T(8,128)(2,1)S(1)} %pad_maximum_fusion.refs_4_.refs_8_), channel_id=1, source_target_pairs={{0,2},{2,0},{4,6},{6,4},{8,10},{10,8},{12,14},{14,12},{16,18},{18,... | collective-permute-start | bytes 1327112 | tf_op jit(solution)/shard_map/ppermute | solution.py:228
  43.1 7.5 %copy-start.4 = (bf16[1,2048,256]{2,1,0:T(8,128)(2,1)S(1)}, bf16[1,2048,256]{2,1,0:T(8,128)(2,1)}, u32[]{:S(2)}) copy-start(bf16[1,2048,256]{2,1,0:T(8,128)(2,1)} %param.15) | copy-start | bytes 3145732
  43.1 7.5 %copy-start.5 = (bf16[1,2048,256]{2,1,0:T(8,128)(2,1)S(1)}, bf16[1,2048,256]{2,1,0:T(8,128)(2,1)}, u32[]{:S(2)}) copy-start(bf16[1,2048,256]{2,1,0:T(8,128)(2,1)} %param.16) | copy-start | bytes 3145732
  43.1 7.5 %copy-start.6 = (bf16[1,256,2048]{2,1,0:T(8,128)(2,1)S(1)}, bf16[1,256,2048]{2,1,0:T(8,128)(2,1)}, u32[]{:S(2)}) copy-start(bf16[1,256,2048]{2,1,0:T(8,128)(2,1)} %param.17) | copy-start | bytes 3145732
  43.1 5.5 %collective-permute-start.6 = (bf16[192,1024]{1,0:T(8,128)(2,1)S(1)}, bf16[192,1024]{1,0:T(8,128)(2,1)S(1)}, u32[]{:S(2)}, u32[]{:S(2)}) collective-permute-start(bf16[192,1024]{1,0:T(8,128)(2,1)S(1)} %pad_maximum_fusion.4.refs_1_), channel_id=1, source_target_pairs={{0,2},{2,0},{4,6},{6,4},{8,10},{10,8},{12,14},{14,12},{16,18},{18,... | collective-permute-start | bytes 1179656 | tf_op jit(solution)/shard_map/ppermute | solution.py:228
  43.7 6.3 %collective-permute-start.12 = (bf16[192,1024]{1,0:T(8,128)(2,1)S(1)}, bf16[192,1024]{1,0:T(8,128)(2,1)S(1)}, u32[]{:S(2)}, u32[]{:S(2)}) collective-permute-start(bf16[192,1024]{1,0:T(8,128)(2,1)S(1)} %pad_maximum_fusion.5.refs_5_.refs_9_), channel_id=1, source_target_pairs={{0,2},{2,0},{4,6},{6,4},{8,10},{10,8},{12,14},{14,12},{16,18},{18,... | collective-permute-start | bytes 1179656 | tf_op jit(solution)/shard_map/ppermute | solution.py:228
  45.8 8.3 %collective-permute-start.16 = (bf16[48,1024]{1,0:T(8,128)(2,1)S(1)}, bf16[48,1024]{1,0:T(8,128)(2,1)S(1)}, u32[]{:S(2)}, u32[]{:S(2)}) collective-permute-start(bf16[48,1024]{1,0:T(8,128)(2,1)S(1)} %slice.157), channel_id=1, source_target_pairs={{0,1},{1,0},{2,3},{3,2},{4,5},{5,4},{6,7},{7,6},{8,9},{9,8},{10,11... | collective-permute-start | bytes 294920 | tf_op jit(solution)/shard_map/ppermute | solution.py:231
  46.5 8.3 %collective-permute-start.18 = (bf16[144,512]{1,0:T(8,128)(2,1)S(1)}, bf16[144,512]{1,0:T(8,128)(2,1)S(1)}, u32[]{:S(2)}, u32[]{:S(2)}) collective-permute-start(bf16[144,512]{1,0:T(8,128)(2,1)S(1)} %slice.159), channel_id=1, source_target_pairs={{0,4},{2,6},{4,0},{6,2},{8,12},{10,14},{12,8},{14,10},{16,20},{18,... | collective-permute-start | bytes 442376 | tf_op jit(solution)/shard_map/ppermute | solution.py:225
  47.1 7.7 %collective-permute-start.17 = (bf16[144,512]{1,0:T(8,128)(2,1)S(1)}, bf16[144,512]{1,0:T(8,128)(2,1)S(1)}, u32[]{:S(2)}, u32[]{:S(2)}) collective-permute-start(bf16[144,512]{1,0:T(8,128)(2,1)S(1)} %slice.158), channel_id=1, source_target_pairs={{0,1},{1,0},{2,3},{3,2},{4,5},{5,4},{6,7},{7,6},{8,9},{9,8},{10,11... | collective-permute-start | bytes 442376 | tf_op jit(solution)/shard_map/ppermute | solution.py:231
  48.6 10.2 %collective-permute-start.24 = (bf16[144,512]{1,0:T(8,128)(2,1)S(1)}, bf16[144,512]{1,0:T(8,128)(2,1)S(1)}, u32[]{:S(2)}, u32[]{:S(2)}) collective-permute-start(bf16[144,512]{1,0:T(8,128)(2,1)S(1)} %slice.162), channel_id=1, source_target_pairs={{0,4},{2,6},{4,0},{6,2},{8,12},{10,14},{12,8},{14,10},{16,20},{18,... | collective-permute-start | bytes 442376 | tf_op jit(solution)/shard_map/ppermute | solution.py:225
  50.0 9.3 %collective-permute-start.23 = (bf16[144,512]{1,0:T(8,128)(2,1)S(1)}, bf16[144,512]{1,0:T(8,128)(2,1)S(1)}, u32[]{:S(2)}, u32[]{:S(2)}) collective-permute-start(bf16[144,512]{1,0:T(8,128)(2,1)S(1)} %slice.161), channel_id=1, source_target_pairs={{0,1},{1,0},{2,3},{3,2},{4,5},{5,4},{6,7},{7,6},{8,9},{9,8},{10,11... | collective-permute-start | bytes 442376 | tf_op jit(solution)/shard_map/ppermute | solution.py:231
  54.1 4.7 %collective-permute-start.22 = (bf16[48,1024]{1,0:T(8,128)(2,1)S(1)}, bf16[48,1024]{1,0:T(8,128)(2,1)S(1)}, u32[]{:S(2)}, u32[]{:S(2)}) collective-permute-start(bf16[48,1024]{1,0:T(8,128)(2,1)S(1)} %get-tuple-element.68), channel_id=1, source_target_pairs={{0,4},{2,6},{4,0},{6,2},{8,12},{10,14},{12,8},{14,10},{16,20},{18,... | collective-permute-start | bytes 294920 | tf_op jit(solution)/shard_map/ppermute | solution.py:225
  54.8 4.7 %collective-permute-start.19 = (bf16[192,1024]{1,0:T(8,128)(2,1)S(1)}, bf16[192,1024]{1,0:T(8,128)(2,1)S(1)}, u32[]{:S(2)}, u32[]{:S(2)}) collective-permute-start(bf16[192,1024]{1,0:T(8,128)(2,1)S(1)} %pad_maximum_fusion.6.refs_0_.refs_4_), channel_id=1, source_target_pairs={{0,2},{2,0},{4,6},{6,4},{8,10},{10,8},{12,14},{14,12},{16,18},{18,... | collective-permute-start | bytes 1179656 | tf_op jit(solution)/shard_map/ppermute | solution.py:228
  54.8 10.7 %collective-permute-start.13 = (bf16[192,2176]{1,0:T(8,128)(2,1)S(1)}, bf16[192,2176]{1,0:T(8,128)(2,1)S(1)}, u32[]{:S(2)}, u32[]{:S(2)}) collective-permute-start(bf16[192,2176]{1,0:T(8,128)(2,1)S(1)} %get-tuple-element.39), channel_id=1, source_target_pairs={{0,2},{2,0},{4,6},{6,4},{8,10},{10,8},{12,14},{14,12},{16,18},{18,... | collective-permute-start | bytes 2506760 | tf_op jit(solution)/shard_map/ppermute | solution.py:228
  58.8 1.8 %collective-permute-start.25 = (bf16[192,1152]{1,0:T(8,128)(2,1)S(1)}, bf16[192,1152]{1,0:T(8,128)(2,1)S(1)}, u32[]{:S(2)}, u32[]{:S(2)}) collective-permute-start(bf16[192,1152]{1,0:T(8,128)(2,1)S(1)} %pad_maximum_fusion.1.refs_4_.refs_12_), channel_id=1, source_target_pairs={{0,2},{2,0},{4,6},{6,4},{8,10},{10,8},{12,14},{14,12},{16,18},{18,... | collective-permute-start | bytes 1327112 | tf_op jit(solution)/shard_map/ppermute | solution.py:228
  58.8 2.3 %collective-permute-start.20 = (bf16[192,1024]{1,0:T(8,128)(2,1)S(1)}, bf16[192,1024]{1,0:T(8,128)(2,1)S(1)}, u32[]{:S(2)}, u32[]{:S(2)}) collective-permute-start(bf16[192,1024]{1,0:T(8,128)(2,1)S(1)} %maximum_maximum_fusion.refs_1_.refs_5_), channel_id=1, source_target_pairs={{0,2},{2,0},{4,6},{6,4},{8,10},{10,8},{12,14},{14,12},{16,18},{18,... | collective-permute-start | bytes 1179656 | tf_op jit(solution)/shard_map/ppermute | solution.py:228
  59.4 2.4 %collective-permute-start.26 = (bf16[192,1024]{1,0:T(8,128)(2,1)S(1)}, bf16[192,1024]{1,0:T(8,128)(2,1)S(1)}, u32[]{:S(2)}, u32[]{:S(2)}) collective-permute-start(bf16[192,1024]{1,0:T(8,128)(2,1)S(1)} %maximum_maximum_fusion.1.refs_5_.refs_13_), channel_id=1, source_target_pairs={{0,2},{2,0},{4,6},{6,4},{8,10},{10,8},{12,14},{14,12},{16,18},{18,... | collective-permute-start | bytes 1179656 | tf_op jit(solution)/shard_map/ppermute | solution.py:228
  65.3 2.4 %collective-permute-start.27 = (bf16[192,2176]{1,0:T(8,128)(2,1)S(1)}, bf16[192,2176]{1,0:T(8,128)(2,1)S(1)}, u32[]{:S(2)}, u32[]{:S(2)}) collective-permute-start(bf16[192,2176]{1,0:T(8,128)(2,1)S(1)} %get-tuple-element.41), channel_id=1, source_target_pairs={{0,2},{2,0},{4,6},{6,4},{8,10},{10,8},{12,14},{14,12},{16,18},{18,... | collective-permute-start | bytes 2506760 | tf_op jit(solution)/shard_map/ppermute | solution.py:228
  67.9 2.3 %copy-start = (s32[128]{0:T(128)S(1)}, s32[128]{0:T(128)}, u32[]{:S(2)}) copy-start(s32[128]{0:T(128)} %param.13) | copy-start | bytes 1540
  68.0 12.3 %collective-permute-start.28 = (bf16[192,1152]{1,0:T(8,128)(2,1)S(1)}, bf16[192,1152]{1,0:T(8,128)(2,1)S(1)}, u32[]{:S(2)}, u32[]{:S(2)}) collective-permute-start(bf16[192,1152]{1,0:T(8,128)(2,1)S(1)} %pad_maximum_fusion.2), channel_id=1, source_target_pairs={{0,4},{2,6},{4,0},{6,2},{8,12},{10,14},{12,8},{14,10},{16,20},{18,... | collective-permute-start | bytes 1327112 | tf_op jit(solution)/shard_map/ppermute | solution.py:225
  68.7 10.9 %collective-permute-start.30 = (bf16[384,512]{1,0:T(8,128)(2,1)S(1)}, bf16[384,512]{1,0:T(8,128)(2,1)S(1)}, u32[]{:S(2)}, u32[]{:S(2)}) collective-permute-start(bf16[384,512]{1,0:T(8,128)(2,1)S(1)} %pad_maximum_fusion.7), channel_id=1, source_target_pairs={{0,1},{1,0},{2,3},{3,2},{4,5},{5,4},{6,7},{7,6},{8,9},{9,8},{10,11... | collective-permute-start | bytes 1179656 | tf_op jit(solution)/shard_map/ppermute | solution.py:231
  80.5 7.2 %collective-permute-start.29 = (bf16[192,640]{1,0:T(8,128)(2,1)S(1)}, bf16[192,640]{1,0:T(8,128)(2,1)S(1)}, u32[]{:S(2)}, u32[]{:S(2)}) collective-permute-start(bf16[192,640]{1,0:T(8,128)(2,1)S(1)} %pad_maximum_fusion.10), channel_id=1, source_target_pairs={{0,1},{1,0},{2,3},{3,2},{4,5},{5,4},{6,7},{7,6},{8,9},{9,8},{10,11... | collective-permute-start | bytes 737288 | tf_op jit(solution)/shard_map/ppermute | solution.py:231
  82.0 5.9 %collective-permute-start.31 = (bf16[192,512]{1,0:T(8,128)(2,1)S(1)}, bf16[192,512]{1,0:T(8,128)(2,1)S(1)}, u32[]{:S(2)}, u32[]{:S(2)}) collective-permute-start(bf16[192,512]{1,0:T(8,128)(2,1)S(1)} %fusion.2), channel_id=1, source_target_pairs={{0,4},{2,6},{4,0},{6,2},{8,12},{10,14},{12,8},{14,10},{16,20},{18,... | collective-permute-start | bytes 589832 | tf_op jit(solution)/shard_map/ppermute | solution.py:225
  88.2 10.6 %collective-permute-start.32 = (bf16[48,1152]{1,0:T(8,128)(2,1)S(1)}, bf16[48,1152]{1,0:T(8,128)(2,1)S(1)}, u32[]{:S(2)}, u32[]{:S(2)}) collective-permute-start(bf16[48,1152]{1,0:T(8,128)(2,1)S(1)} %get-tuple-element.65), channel_id=1, source_target_pairs={{0,8},{2,10},{4,12},{6,14},{8,0},{10,2},{12,4},{14,6},{16,24},{18,... | collective-permute-start | bytes 331784 | tf_op jit(solution)/shard_map/ppermute | solution.py:222
  88.2 10.6 %collective-permute-start.33 = (bf16[48,1152]{1,0:T(8,128)(2,1)S(1)}, bf16[48,1152]{1,0:T(8,128)(2,1)S(1)}, u32[]{:S(2)}, u32[]{:S(2)}) collective-permute-start(bf16[48,1152]{1,0:T(8,128)(2,1)S(1)} %get-tuple-element.64), channel_id=1, source_target_pairs={{0,16},{2,18},{4,20},{6,22},{8,24},{10,26},{12,28},{14,30},{16,0},... | collective-permute-start | bytes 331784 | tf_op jit(solution)/shard_map/ppermute | solution.py:222
  91.4 7.4 %collective-permute-start.34 = (bf16[48,1152]{1,0:T(8,128)(2,1)S(1)}, bf16[48,1152]{1,0:T(8,128)(2,1)S(1)}, u32[]{:S(2)}, u32[]{:S(2)}) collective-permute-start(bf16[48,1152]{1,0:T(8,128)(2,1)S(1)} %get-tuple-element.63), channel_id=1, source_target_pairs={{0,24},{2,26},{4,28},{6,30},{8,16},{10,18},{12,20},{14,22},{16,8},... | collective-permute-start | bytes 331784 | tf_op jit(solution)/shard_map/ppermute | solution.py:222
  92.6 6.2 %copy-start.1 = (s32[128,2]{0,1:T(2,128)S(1)}, s32[128,2]{0,1:T(2,128)}, u32[]{:S(2)}) copy-start(s32[128,2]{0,1:T(2,128)} %param.14) | copy-start | bytes 3076
  92.6 6.2 %copy-start.2 = (f32[128,2]{0,1:T(2,128)S(1)}, f32[128,2]{0,1:T(2,128)}, u32[]{:S(2)}) copy-start(f32[128,2]{0,1:T(2,128)} %param.12) | copy-start | bytes 3076
  92.6 6.2 %copy-start.3 = (f32[128]{0:T(128)S(1)}, f32[128]{0:T(128)}, u32[]{:S(2)}) copy-start(f32[128]{0:T(128)} %param.11) | copy-start | bytes 1540
where the time goes:
time: 100 us
  waiting for transfers between devices  45.7 us (46%)
  starting transfers between devices  35.1 us (35%)
  Pallas kernels  16.6 us (17%)
  other arithmetic  1.28 us (1%)
  between operations  1.1 us (1%)
    ppermute x8, waiting for transfers between devices, along_tp(): return lax.ppermute(a, 'tp', [(r, (r + j) % lanes) for r in range(lanes)])  25 us
    ppermute x9, starting transfers between devices, along_groups(): return lax.ppermute(a, 'ep', [(e, e ^ k * EPG) for e in range(experts)])  17.3 us
    pallas_call x8, Pallas kernels, run(): pl.pallas_call(body, out_shape=outs, in_specs=[pl.BlockSpec(memory_space=...  16.6 us
    ppermute x9, waiting for transfers between devices, along_groups(): return lax.ppermute(a, 'ep', [(e, e ^ k * EPG) for e in range(experts)])  10.4 us
    ppermute x8, starting transfers between devices, along_tp(): return lax.ppermute(a, 'tp', [(r, (r + j) % lanes) for r in range(lanes)])  9.25 us
    ppermute x8, starting transfers between devices, along_side(): return lax.ppermute(a, 'ep', [(e, e ^ 2) for e in range(experts)])  6.52 us
    ppermute x8, waiting for transfers between devices, along_side(): return lax.ppermute(a, 'ep', [(e, e ^ 2) for e in range(experts)])  6.05 us
    ppermute x10, waiting for transfers between devices, along_core(): return lax.ppermute(a, 'ep', [(e, e ^ 1) for e in range(experts)])  4.31 us
  transfers between devices with their start and end apart: 35, of which 14 were waited for; matrix products, arithmetic and copies ran while one was open for 1% of the time, Pallas kernels for 14%

commit v1 on v0

--- a/solution.py
+++ b/solution.py
@@ -156,12 +156,10 @@
         sums[c][:, lanes * width :] = tail.astype(sums[c].dtype)
 
 
-def weight_body(lanes, width, *refs):
+def up_body(lanes, width, *refs):
     tok = [refs[b * lanes : (b + 1) * lanes] for b in range(4)]
-    cot = [refs[(4 + b) * lanes : (5 + b) * lanes] for b in range(4)]
-    grads = refs[8 * lanes : 8 * lanes + 4]
-    scaled_hidden = refs[8 * lanes + 4 : 8 * lanes + 8]
-    gate_out, up_out, down_out = refs[8 * lanes + 8 :]
+    grads = refs[4 * lanes : 4 * lanes + 4]
+    gate_out, up_out = refs[4 * lanes + 4 :]
     cols = gate_out.shape[1]
     rank = lax.axis_index("tp")
     chunk = min(width, 512)
@@ -170,27 +168,40 @@
         for s in range(0, width, chunk):
             span = pl.ds(pl.multiple_of(base + s, chunk), chunk)
             total = dot(tok[0][j][:, s : s + chunk], grads[0][...], ROWS_ROWS)
+            for b in range(1, 4):
+                total = total + dot(tok[b][j][:, s : s + chunk], grads[b][...], ROWS_ROWS)
+            gate_out[span, :] = total[:, :cols]
+            up_out[span, :] = total[:, cols:]
+
+
+def down_body(lanes, width, *refs):
+    cot = [refs[b * lanes : (b + 1) * lanes] for b in range(4)]
+    scaled_hidden = refs[4 * lanes : 4 * lanes + 4]
+    down_out = refs[4 * lanes + 4]
+    rank = lax.axis_index("tp")
+    chunk = min(width, 512)
+    for j in range(lanes):
+        base = ((rank + lanes - j) % lanes) * width
+        for s in range(0, width, chunk):
+            span = pl.ds(pl.multiple_of(base + s, chunk), chunk)
             down = dot(scaled_hidden[0][...], cot[0][j][:, s : s + chunk], ROWS_ROWS)
             for b in range(1, 4):
-                total = total + dot(tok[b][j][:, s : s + chunk], grads[b][...], ROWS_ROWS)
                 down = down + dot(scaled_hidden[b][...], cot[b][j][:, s : s + chunk], ROWS_ROWS)
-            gate_out[span, :] = total[:, :cols]
-            up_out[span, :] = total[:, cols:]
             down_out[:, span] = down
 
 
 def final_body(groups, cap, *refs):
     back = refs[:groups]
-    pick_refs = refs[groups : groups + 3]
-    local_ref, weight_ref, expert_ref = refs[groups + 3 : groups + 6]
-    tok_out, group_out, expert_out = refs[groups + 6 :]
+    pick_refs = refs[groups : groups + 4]
+    local_ref, weight_ref, expert_ref = refs[groups + 4 : groups + 7]
+    tok_out, group_out, expert_out = refs[groups + 7 :]
     count, width = tok_out.shape
+    picks = [pick_refs[min(k, 3)][pl.ds(max(k - 3, 0) * cap, cap), :] for k in range(groups)]
     total = jnp.zeros((count, width), F32)
     held = jnp.zeros((LANES, count), F32)
     for k in range(groups):
-        pick = pick_refs[min(k, 2)][pl.ds(max(k - 2, 0) * cap, cap), :]
-        total = total + dot(pick, back[k][:, :width], ROWS_ROWS)
-        held = held + dot(back[k][:, width:], pick, ROWS_ROWS)
+        total = total + dot(picks[k], back[k][:, :width], ROWS_ROWS)
+        held = held + dot(back[k][:, width:], picks[k], ROWS_ROWS)
     tok_out[...] = total
     lane = lax.broadcasted_iota(jnp.int32, (LANES, count), 0)
     group_sum = jnp.zeros((1, count), F32)
@@ -229,6 +240,14 @@
 
     def along_tp(a, j):
         return lax.ppermute(a, "tp", [(r, (r + j) % lanes) for r in range(lanes)])
+
+    def along_both(a, j):
+        pairs = [
+            (e * lanes + r, (e ^ 2) * lanes + (r + j) % lanes)
+            for e in range(experts)
+            for r in range(lanes)
+        ]
+        return lax.ppermute(a, ("ep", "tp"), pairs)
 
     shape = jax.ShapeDtypeStruct
     choice_row = group_choice.reshape(1, count)
@@ -256,7 +275,7 @@
             for a in (choice_row, local_rows, weight_row, expert_rows, tokens, cotangent)
         )
     )
-    parts = [[0], [1], list(range(2, groups))]
+    parts = [[0], [1], [2], list(range(3, groups))]
     picked = [
         call(
             functools.partial(picks_body, groups, cap, part),
@@ -271,8 +290,7 @@
     own_side = along_side(own)
     own_lane = [along_tp(own, j) for j in range(1, lanes)]
     cot_sent = {k: along_groups(routed[groups - 1 + k], k) for k in others}
-    own_tok_both = [along_tp(own_side[:, :width], j) for j in range(1, lanes)]
-    own_cot_both = [along_side(a[:, width : 2 * width]) for a in own_lane]
+    own_both = [along_both(own, j) for j in range(1, lanes)]
     tok = jnp.concatenate([tok_sent[k] for k in range(1, groups)], axis=0)
     cot = jnp.concatenate([cot_sent[k] for k in range(1, groups)], axis=0)
     cot_bare = jnp.concatenate([cot_sent[k][:, :width] for k in range(1, groups)], axis=0)
@@ -300,9 +318,9 @@
     cot_near = [join(own[:, width:], cot)]
     cot_near += [join(a[:, width : 2 * width], b) for a, b in zip(own_lane, cot_lane)]
     tok_far = [join(own_side[:, :width], tok_side)]
-    tok_far += [join(a, b) for a, b in zip(own_tok_both, tok_both)]
+    tok_far += [join(a[:, :width], b) for a, b in zip(own_both, tok_both)]
     cot_far = [join(own_side[:, width:], cot_side)]
-    cot_far += [join(a, b) for a, b in zip(own_cot_both, cot_both)]
+    cot_far += [join(a[:, width : 2 * width], b) for a, b in zip(own_both, cot_both)]
     first, second, third = w_gate[0], w_up[0], w_down[0]
     work = 2 * 5 * 2 * rows * features * cols
 
@@ -322,35 +340,24 @@
     far, tok_b, cot_b = experts_on(tok_far, cot_far)
     near_sum = near[0] + along_core(near[1]).astype(F32)
     far_sum = far[0] + along_core(far[1]).astype(F32)
-    if lanes == 2:
-        half = width // 2
-        tail = far_sum[:, features:]
-        side_out = jnp.concatenate(
-            [far_sum[:, :half], far_sum[:, width : width + half], tail], axis=1
-        ).astype(BF16)
-        lane_out = jnp.concatenate(
-            [near_sum[:, width + half : features], far_sum[:, width + half : features]], axis=0
-        ).astype(BF16)
-        side_in = along_side(side_out).astype(F32)
-        lane_in = along_tp(lane_out, 1).astype(F32)
-        lane_next = jnp.concatenate(
-            [
-                near_sum[:, width : width + half] + side_in[:, half:width],
-                near_sum[:, features:] + side_in[:, width:],
-            ],
-            axis=1,
+    early = 3 * width // (8 * LANES) * LANES
+    if lanes == 2 and early > 0:
+        far_tail = far_sum[:, features:]
+        near_in = along_tp(near_sum[:, width + early : features].astype(BF16), 1)
+        lane_in = along_tp(far_sum[:, width + early : features].astype(BF16), 1)
+        side_out = jnp.concatenate([far_sum[:, width : width + early], far_tail], axis=1)
+        side_in = along_side(side_out.astype(BF16)).astype(F32)
+        own_in = along_side(far_sum[:, :early].astype(BF16))
+        last_in = along_side((far_sum[:, early:width] + lane_in.astype(F32)).astype(BF16))
+        near_out = jnp.concatenate(
+            [near_sum[:, width : width + early], near_sum[:, features:]], axis=1
         )
-        side_next = (far_sum[:, half:width] + lane_in[rows:]).astype(BF16)
-        lane_last = along_tp(lane_next.astype(BF16), 1).astype(F32)
-        side_last = along_side(side_next).astype(F32)
-        tail = lane_next[:, half:] + lane_last[:, half:]
-        body = jnp.concatenate(
-            [
-                near_sum[:, :half] + side_in[:, :half] + lane_last[:, :half],
-                near_sum[:, half:width] + lane_in[:rows] + side_last,
-            ],
-            axis=1,
-        )
+        next_out = near_out + side_in
+        next_in = along_tp(next_out.astype(BF16), 1).astype(F32)
+        tail = next_out[:, early:] + next_in[:, early:]
+        head = near_sum[:, :early] + own_in.astype(F32) + next_in[:, :early]
+        rest = near_sum[:, early:width] + near_in.astype(F32) + last_in.astype(F32)
+        body = jnp.concatenate([head, rest], axis=1)
     else:
         both = near_sum + along_side(far_sum.astype(BF16)).astype(F32)
         tail = both[:, features:]
@@ -369,11 +376,13 @@
     returned = [result[:cap]] + [sent[k] for k in range(1, groups)]
     grads = list(near[2:4]) + list(far[2:4])
     scaled_hidden = list(near[4:6]) + list(far[4:6])
-    first_grad, second_grad, third_grad = call(
-        functools.partial(weight_body, lanes, width),
-        [shape((features, cols), F32)] * 2 + [shape((cols, features), F32)],
-        2 * 3 * 4 * rows * features * cols,
-    )(*tok_a, *tok_b, *cot_a, *cot_b, *grads, *scaled_hidden)
+    up_work = 2 * 2 * 4 * rows * features * cols
+    first_grad, second_grad = call(
+        functools.partial(up_body, lanes, width), [shape((features, cols), F32)] * 2, up_work
+    )(*tok_a, *tok_b, *grads)
+    third_grad = call(
+        functools.partial(down_body, lanes, width), shape((cols, features), F32), up_work // 2
+    )(*cot_a, *cot_b, *scaled_hidden)
     token_grad, group_grad, expert_grad = call(
         functools.partial(final_body, groups, cap),
         [shape((count, width), F32), shape((1, count), F32), shape((picks, count), F32)],

time: 100 us -> 96.9 us (0.969)
  waiting for transfers between devices: 45.7 us -> 36.5 us
  starting transfers between devices: 35.1 us -> 40 us
  Pallas kernels: 16.6 us -> 17.6 us
    ppermute x8, starting transfers between devices: 6.52 us -> 12.1 us  [along_side(): return lax.ppermute(a, 'ep', [(e, e ^ 2) for e in range(experts)])]
    ppermute x8, waiting for transfers between devices: 25 us -> 20.3 us  [along_tp(): return lax.ppermute(a, 'tp', [(r, (r + j) % lanes) for r in range(lanes)])]
    ppermute x8, starting transfers between devices: 9.25 us -> 6.77 us  [along_tp(): return lax.ppermute(a, 'tp', [(r, (r + j) % lanes) for r in range(lanes)])]
    ppermute x10, waiting for transfers between devices: 4.31 us -> 2.01 us  [along_core(): return lax.ppermute(a, 'ep', [(e, e ^ 1) for e in range(experts)])]
    ppermute x0 -> x1, starting transfers between devices: none -> 1.49 us  [along_both(): return lax.ppermute(a, ('ep', 'tp'), pairs)]
    ppermute x9, waiting for transfers between devices: 10.4 us -> 9.07 us  [along_groups(): return lax.ppermute(a, 'ep', [(e, e ^ k * EPG) for e in range(experts)])]
    pallas_call x8 -> x10, Pallas kernels: 16.6 us -> 17.6 us  [run(): pl.pallas_call(body, out_shape=outs, in_specs=[pl.BlockSpec(memory_space=...]
  transfers between devices with their start and end apart: 35 -> 36, of which waited for: 14 -> 14; matrix products, arithmetic and copies ran while one was open for 1% -> 1% of each run, Pallas kernels for 14% -> 15%
where the time goes in v1:
time: 96.9 us; the launch traced here: 96.7 us
  starting transfers between devices  40 us (41%)
  waiting for transfers between devices  36.5 us (38%)
  Pallas kernels  17.6 us (18%)
  between operations  1.12 us (1%)
  other arithmetic  1.1 us (1%)
    ppermute x8, waiting for transfers between devices, along_tp(): return lax.ppermute(a, 'tp', [(r, (r + j) % lanes) for r in range(lanes)])  20.3 us
    pallas_call x10, Pallas kernels, run(): pl.pallas_call(body, out_shape=outs, in_specs=[pl.BlockSpec(memory_space=...  17.6 us
    ppermute x9, starting transfers between devices, along_groups(): return lax.ppermute(a, 'ep', [(e, e ^ k * EPG) for e in range(experts)])  17.3 us
    ppermute x8, starting transfers between devices, along_side(): return lax.ppermute(a, 'ep', [(e, e ^ 2) for e in range(experts)])  12.1 us
    ppermute x9, waiting for transfers between devices, along_groups(): return lax.ppermute(a, 'ep', [(e, e ^ k * EPG) for e in range(experts)])  9.07 us
    ppermute x8, starting transfers between devices, along_tp(): return lax.ppermute(a, 'tp', [(r, (r + j) % lanes) for r in range(lanes)])  6.77 us
    ppermute x8, waiting for transfers between devices, along_side(): return lax.ppermute(a, 'ep', [(e, e ^ 2) for e in range(experts)])  5.08 us
    ppermute x10, starting transfers between devices, along_core(): return lax.ppermute(a, 'ep', [(e, e ^ 1) for e in range(experts)])  2.35 us
  transfers between devices with their start and end apart: 36, of which 14 were waited for; matrix products, arithmetic and copies ran while one was open for 1% of the time, Pallas kernels for 15%

profile of v1, /device:TPU:0, one launch (start us, length us, event | category | flops | bytes accessed | tf_op | source)
XLA Modules:
  0.0 96.7 jit_solution(13454408765371561509)
XLA Ops:
  0.6 1.7 %shard_map.136 = (bf16[48,2176]{1,0:T(8,128)(2,1)S(1)}, bf16[48,1024]{1,0:T(8,128)(2,1)S(1)}, bf16[48,1024]{1,0:T(8,128)(2,1)S(1)}, bf16[48,1024]{1,0:T(8,128)(2...) custom-call(s32[1,128]{1,0:T(1,128)} %bitcast.12, ...), custom_call_target="tpu_custom_call" | custom-call | tf_op jit(solution)/shard_map/pallas_call | solution.py:27
  2.3 3.1 %collective-permute-start = (bf16[48,1024]{1,0:T(8,128)(2,1)S(1)}, bf16[48,1024]{1,0:T(8,128)(2,1)S(1)}, u32[]{:S(2)}, u32[]{:S(2)}) collective-permute-start(bf16[48,1024]{1,0:T(8,128)(2,1)S(1)} %get-tuple-element.31), channel_id=1, source_target_pairs={{0,8},{2,10},{4,12},{6,14},{8,0},{10,2},{12,4},{14,6},{16,24},{18,... | collective-permute-start | bytes 294920 | tf_op jit(solution)/shard_map/ppermute | solution.py:233
  5.4 1.5 %collective-permute-start.14 = (bf16[48,2176]{1,0:T(8,128)(2,1)S(1)}, bf16[48,2176]{1,0:T(8,128)(2,1)S(1)}, u32[]{:S(2)}, u32[]{:S(2)}) collective-permute-start(bf16[48,2176]{1,0:T(8,128)(2,1)S(1)} %get-tuple-element.30), channel_id=1, source_target_pairs={{0,4},{2,6},{4,0},{6,2},{8,12},{10,14},{12,8},{14,10},{16,20},{18,... | collective-permute-start | bytes 626696 | tf_op jit(solution)/shard_map/ppermute | solution.py:236
  6.9 1.5 %collective-permute-start.16 = (bf16[48,2176]{1,0:T(8,128)(2,1)S(1)}, bf16[48,2176]{1,0:T(8,128)(2,1)S(1)}, u32[]{:S(2)}, u32[]{:S(2)}) collective-permute-start(bf16[48,2176]{1,0:T(8,128)(2,1)S(1)} %get-tuple-element.30), channel_id=1, source_target_pairs={{0,5},{1,4},{2,7},{3,6},{4,1},{5,0},{6,3},{7,2},{8,13},{9,12},{10,... | collective-permute-start | bytes 626696 | tf_op jit(solution)/shard_map/ppermute | solution.py:250
  8.4 2.6 %collective-permute-start.1 = (bf16[48,1024]{1,0:T(8,128)(2,1)S(1)}, bf16[48,1024]{1,0:T(8,128)(2,1)S(1)}, u32[]{:S(2)}, u32[]{:S(2)}) collective-permute-start(bf16[48,1024]{1,0:T(8,128)(2,1)S(1)} %get-tuple-element.32), channel_id=1, source_target_pairs={{0,16},{2,18},{4,20},{6,22},{8,24},{10,26},{12,28},{14,30},{16,0},... | collective-permute-start | bytes 294920 | tf_op jit(solution)/shard_map/ppermute | solution.py:233
  11.0 0.2 collective-permute-start.2
  11.2 3.6 %collective-permute-start.9 = (bf16[48,1152]{1,0:T(8,128)(2,1)S(1)}, bf16[48,1152]{1,0:T(8,128)(2,1)S(1)}, u32[]{:S(2)}, u32[]{:S(2)}) collective-permute-start(bf16[48,1152]{1,0:T(8,128)(2,1)S(1)} %get-tuple-element.36), channel_id=1, source_target_pairs={{0,24},{2,26},{4,28},{6,30},{8,16},{10,18},{12,20},{14,22},{16,8},... | collective-permute-start | bytes 331784 | tf_op jit(solution)/shard_map/ppermute | solution.py:233
  14.8 6.8 %collective-permute-done.1 = bf16[48,1024]{1,0:T(8,128)(2,1)S(1)} collective-permute-done((bf16[48,1024]{1,0:T(8,128)(2,1)S(1)}, bf16[48,1024]{1,0:T(8,128)(2,1)S(1)}, u32[]{:S(2)}, u32[]{:S(2)}) %collective-permute-start.1) | collective-permute-done | bytes 98336 | tf_op jit(solution)/shard_map/ppermute | solution.py:233
  21.7 3.3 %collective-permute-start.7 = (bf16[48,1152]{1,0:T(8,128)(2,1)S(1)}, bf16[48,1152]{1,0:T(8,128)(2,1)S(1)}, u32[]{:S(2)}, u32[]{:S(2)}) collective-permute-start(bf16[48,1152]{1,0:T(8,128)(2,1)S(1)} %get-tuple-element.34), channel_id=1, source_target_pairs={{0,8},{2,10},{4,12},{6,14},{8,0},{10,2},{12,4},{14,6},{16,24},{18,... | collective-permute-start | bytes 331784 | tf_op jit(solution)/shard_map/ppermute | solution.py:233
  25.0 1.6 %collective-permute-start.15 = (bf16[144,1024]{1,0:T(8,128)(2,1)S(1)}, bf16[144,1024]{1,0:T(8,128)(2,1)S(1)}, u32[]{:S(2)}, u32[]{:S(2)}) collective-permute-start(bf16[144,1024]{1,0:T(8,128)(2,1)S(1)} %constant_dynamic-update-slice_fusion), channel_id=1, source_target_pairs={{0,4},{2,6},{4,0},{6,2},{8,12},{10,14},{12,8},{14,10},{16,20},{18,... | collective-permute-start | bytes 884744 | tf_op jit(solution)/shard_map/ppermute | solution.py:236
  26.6 2.2 %collective-permute-done.8 = bf16[48,1152]{1,0:T(8,128)(2,1)S(1)} collective-permute-done((bf16[48,1152]{1,0:T(8,128)(2,1)S(1)}, bf16[48,1152]{1,0:T(8,128)(2,1)S(1)}, u32[]{:S(2)}, u32[]{:S(2)}) %collective-permute-start.8) | collective-permute-done | bytes 110624 | tf_op jit(solution)/shard_map/ppermute | solution.py:233
  28.8 0.5 collective-permute-start.4
  29.4 1.6 %collective-permute-start.21 = (bf16[144,1152]{1,0:T(8,128)(2,1)S(1)}, bf16[144,1152]{1,0:T(8,128)(2,1)S(1)}, u32[]{:S(2)}, u32[]{:S(2)}) collective-permute-start(bf16[144,1152]{1,0:T(8,128)(2,1)S(1)} %pad_maximum_fusion.6), channel_id=1, source_target_pairs={{0,4},{2,6},{4,0},{6,2},{8,12},{10,14},{12,8},{14,10},{16,20},{18,... | collective-permute-start | bytes 995336 | tf_op jit(solution)/shard_map/ppermute | solution.py:236
  31.0 1.5 %collective-permute-start.10 = (bf16[144,1024]{1,0:T(8,128)(2,1)S(1)}, bf16[144,1024]{1,0:T(8,128)(2,1)S(1)}, u32[]{:S(2)}, u32[]{:S(2)}) collective-permute-start(bf16[144,1024]{1,0:T(8,128)(2,1)S(1)} %pad_maximum_fusion.7), channel_id=1, source_target_pairs={{0,1},{1,0},{2,3},{3,2},{4,5},{5,4},{6,7},{7,6},{8,9},{9,8},{10,11... | collective-permute-start | bytes 884744 | tf_op jit(solution)/shard_map/ppermute | solution.py:242
  32.6 6.1 %collective-permute-done.4 = bf16[144,1024]{1,0:T(8,128)(2,1)S(1)} collective-permute-done((bf16[144,1024]{1,0:T(8,128)(2,1)S(1)}, bf16[144,1024]{1,0:T(8,128)(2,1)S(1)}, u32[]{:S(2)}, u32[]{:S(2)}) %collective-permute-start.4) | collective-permute-done | bytes 294944 | tf_op jit(solution)/shard_map/ppermute | solution.py:242
  38.7 1.6 %collective-permute-start.18 = (bf16[144,512]{1,0:T(8,128)(2,1)S(1)}, bf16[144,512]{1,0:T(8,128)(2,1)S(1)}, u32[]{:S(2)}, u32[]{:S(2)}) collective-permute-start(bf16[144,512]{1,0:T(8,128)(2,1)S(1)} %slice.150), channel_id=1, source_target_pairs={{0,4},{2,6},{4,0},{6,2},{8,12},{10,14},{12,8},{14,10},{16,20},{18,... | collective-permute-start | bytes 442376 | tf_op jit(solution)/shard_map/ppermute | solution.py:236
  40.3 0.6 collective-permute-start.17
  40.9 0.1 collective-permute-start.19
  41.0 2.9 %collective-permute-done.10 = bf16[144,1024]{1,0:T(8,128)(2,1)S(1)} collective-permute-done((bf16[144,1024]{1,0:T(8,128)(2,1)S(1)}, bf16[144,1024]{1,0:T(8,128)(2,1)S(1)}, u32[]{:S(2)}, u32[]{:S(2)}) %collective-permute-start.10) | collective-permute-done | bytes 294944 | tf_op jit(solution)/shard_map/ppermute | solution.py:242
  43.9 2.3 %collective-permute-start.23 = (bf16[144,512]{1,0:T(8,128)(2,1)S(1)}, bf16[144,512]{1,0:T(8,128)(2,1)S(1)}, u32[]{:S(2)}, u32[]{:S(2)}) collective-permute-start(bf16[144,512]{1,0:T(8,128)(2,1)S(1)} %slice.154), channel_id=1, source_target_pairs={{0,4},{2,6},{4,0},{6,2},{8,12},{10,14},{12,8},{14,10},{16,20},{18,... | collective-permute-start | bytes 442376 | tf_op jit(solution)/shard_map/ppermute | solution.py:236
  46.3 0.7 collective-permute-start.22
  47.0 0.1 collective-permute-start.24
  47.2 0.5 collective-permute-start.20
  47.7 1.6 %collective-permute-done.23 = bf16[144,512]{1,0:T(8,128)(2,1)S(1)} collective-permute-done((bf16[144,512]{1,0:T(8,128)(2,1)S(1)}, bf16[144,512]{1,0:T(8,128)(2,1)S(1)}, u32[]{:S(2)}, u32[]{:S(2)}) %collective-permute-start.23) | collective-permute-done | bytes 147488 | tf_op jit(solution)/shard_map/ppermute | solution.py:236
  49.4 2.1 %collective-permute-done.22 = bf16[144,512]{1,0:T(8,128)(2,1)S(1)} collective-permute-done((bf16[144,512]{1,0:T(8,128)(2,1)S(1)}, bf16[144,512]{1,0:T(8,128)(2,1)S(1)}, u32[]{:S(2)}, u32[]{:S(2)}) %collective-permute-start.22) | collective-permute-done | bytes 147488 | tf_op jit(solution)/shard_map/ppermute | solution.py:242
  51.5 0.1 collective-permute-start.25
  51.6 0.7 collective-permute-start.3
  52.4 0.2 collective-permute-start.5
  52.6 0.4 collective-permute-start.11
  53.0 0.3 collective-permute-done.25.refs_7_
  53.3 3.5 %shard_map.138 = (f32[192,2176]{1,0:T(8,128)S(1)}, bf16[192,2176]{1,0:T(8,128)(2,1)S(1)}, bf16[192,512]{1,0:T(8,128)(2,1)S(1)}, bf16[192,512]{1,0:T(8,128)(2,1)S...) custom-call(bf16[192,1024]{1,0:T(8,128)(2,1)S(1)} %pad_maximum_fusion.5.refs_0_.refs_4_, ...), custom_call_target="tpu_custom_call" | custom-call | flops 2013265920 | tf_op jit(solution)/shard_map/pallas_call | solution.py:27
  56.9 0.2 collective-permute-start.26
  57.1 2.1 %collective-permute-done.3 = bf16[48,2176]{1,0:T(8,128)(2,1)S(1)} collective-permute-done((bf16[48,2176]{1,0:T(8,128)(2,1)S(1)}, bf16[48,2176]{1,0:T(8,128)(2,1)S(1)}, u32[]{:S(2)}, u32[]{:S(2)}) %collective-permute-start.3) | collective-permute-done | bytes 208928 | tf_op jit(solution)/shard_map/ppermute | solution.py:242
  59.2 0.1 collective-permute-start.6
  59.3 0.6 collective-permute-start.12
  59.9 0.1 shard_map.139.refs_4_
  60.0 0.1 shard_map.140.refs_5_
  60.2 0.1 shard_map.141.refs_6_
  60.3 0.1 shard_map.142.refs_7_
  60.5 0.5 collective-permute-done.6.refs_3_
  61.0 0.6 collective-permute-done.12.refs_7_.refs_3_
  61.6 3.5 %shard_map.137 = (f32[192,2176]{1,0:T(8,128)S(1)}, bf16[192,2176]{1,0:T(8,128)(2,1)S(1)}, bf16[192,512]{1,0:T(8,128)(2,1)S(1)}, bf16[192,512]{1,0:T(8,128)(2,1)S...) custom-call(bf16[192,1024]{1,0:T(8,128)(2,1)S(1)} %pad_maximum_fusion.2.refs_0_, ...), custom_call_target="tpu_custom_call" | custom-call | flops 2013265920 | tf_op jit(solution)/shard_map/pallas_call | solution.py:27
  65.1 0.2 collective-permute-start.13
  65.3 0.2 fusion.8
  65.6 0.1 collective-permute-start.28
  65.7 1.2 %collective-permute-start.31 = (bf16[192,640]{1,0:T(8,128)(2,1)S(1)}, bf16[192,640]{1,0:T(8,128)(2,1)S(1)}, u32[]{:S(2)}, u32[]{:S(2)}) collective-permute-start(bf16[192,640]{1,0:T(8,128)(2,1)S(1)} %slice.164), channel_id=1, source_target_pairs={{0,1},{1,0},{2,3},{3,2},{4,5},{5,4},{6,7},{7,6},{8,9},{9,8},{10,11... | collective-permute-start | bytes 737288 | tf_op jit(solution)/shard_map/ppermute | solution.py:242
  66.9 0.6 collective-permute-done.13
  67.5 0.1 convert_add_fusion.1
  67.7 0.7 collective-permute-start.30
  68.5 1.5 %collective-permute-start.27 = (bf16[192,384]{1,0:T(8,128)(2,1)S(1)}, bf16[192,384]{1,0:T(8,128)(2,1)S(1)}, u32[]{:S(2)}, u32[]{:S(2)}) collective-permute-start(bf16[192,384]{1,0:T(8,128)(2,1)S(1)} %get-tuple-element.58), channel_id=1, source_target_pairs={{0,4},{2,6},{4,0},{6,2},{8,12},{10,14},{12,8},{14,10},{16,20},{18,... | collective-permute-start | bytes 442376 | tf_op jit(solution)/shard_map/ppermute | solution.py:236
  70.0 3.4 %collective-permute-done.28 = bf16[192,512]{1,0:T(8,128)(2,1)S(1)} collective-permute-done((bf16[192,512]{1,0:T(8,128)(2,1)S(1)}, bf16[192,512]{1,0:T(8,128)(2,1)S(1)}, u32[]{:S(2)}, u32[]{:S(2)}) %collective-permute-start.28) | collective-permute-done | bytes 196640 | tf_op jit(solution)/shard_map/ppermute | solution.py:236
  73.4 0.1 fusion.7
  73.5 0.7 collective-permute-start.29
  74.2 0.4 collective-permute-done.31
  74.6 2.0 %collective-permute-start.32 = (bf16[192,640]{1,0:T(8,128)(2,1)S(1)}, bf16[192,640]{1,0:T(8,128)(2,1)S(1)}, u32[]{:S(2)}, u32[]{:S(2)}) collective-permute-start(bf16[192,640]{1,0:T(8,128)(2,1)S(1)} %fusion.1), channel_id=1, source_target_pairs={{0,4},{2,6},{4,0},{6,2},{8,12},{10,14},{12,8},{14,10},{16,20},{18,... | collective-permute-start | bytes 737288 | tf_op jit(solution)/shard_map/ppermute | solution.py:236
  76.6 6.8 %collective-permute-done.29 = bf16[192,512]{1,0:T(8,128)(2,1)S(1)} collective-permute-done((bf16[192,512]{1,0:T(8,128)(2,1)S(1)}, bf16[192,512]{1,0:T(8,128)(2,1)S(1)}, u32[]{:S(2)}, u32[]{:S(2)}) %collective-permute-start.29) | collective-permute-done | bytes 196640 | tf_op jit(solution)/shard_map/ppermute | solution.py:242
  83.5 0.1 fusion.6
  83.7 0.1 fusion.3
  83.9 0.1 collective-permute-start.33
  84.0 3.1 %collective-permute-start.34 = (bf16[48,1152]{1,0:T(8,128)(2,1)S(1)}, bf16[48,1152]{1,0:T(8,128)(2,1)S(1)}, u32[]{:S(2)}, u32[]{:S(2)}) collective-permute-start(bf16[48,1152]{1,0:T(8,128)(2,1)S(1)} %get-tuple-element.61), channel_id=1, source_target_pairs={{0,16},{2,18},{4,20},{6,22},{8,24},{10,26},{12,28},{14,30},{16,0},... | collective-permute-start | bytes 331784 | tf_op jit(solution)/shard_map/ppermute | solution.py:233
  87.1 1.2 %collective-permute-start.35 = (bf16[48,1152]{1,0:T(8,128)(2,1)S(1)}, bf16[48,1152]{1,0:T(8,128)(2,1)S(1)}, u32[]{:S(2)}, u32[]{:S(2)}) collective-permute-start(bf16[48,1152]{1,0:T(8,128)(2,1)S(1)} %get-tuple-element.60), channel_id=1, source_target_pairs={{0,24},{2,26},{4,28},{6,30},{8,16},{10,18},{12,20},{14,22},{16,8},... | collective-permute-start | bytes 331784 | tf_op jit(solution)/shard_map/ppermute | solution.py:233
  88.4 4.4 %shard_map.144 = (f32[2048,256]{1,0:T(8,128)}, f32[2048,256]{1,0:T(8,128)}) custom-call(bf16[192,1024]{1,0:T(8,128)(2,1)S(1)} %pad_maximum_fusion.2.refs_0_, bf16[192,1024]{1,0:T(8,128)(2,1)S(1)} %pad_maximum_fusion.3.refs_1_, bf16[192,1024]{1,0:T(8,128)(2,1)S(1)} %collective-permute-done.5.refs_2_, bf16[192,1024]{1,0:T(8,128)(2,1)S(1)} %collective-permute-done.6.refs_3_, ...), custom_call_target="tpu_custom_call" | custom-call | flops 1610612736 | tf_op jit(solution)/shard_map/pallas_call | solution.py:27
  92.8 2.6 %shard_map.145 = f32[256,2048]{1,0:T(8,128)} custom-call(bf16[192,1152]{1,0:T(8,128)(2,1)S(1)} %pad_maximum_fusion.refs_4_.refs_0_, bf16[192,1024]{1,0:T(8,128)(2,1)S(1)} %pad_maximum_fusion.4.refs_5_.refs_1_, bf16[192,1152]{1,0:T(8,128)(2,1)S(1)} %collective-permute-done.11.refs_6_.refs_2_, bf16[192,1024]{1,0:T(8,128)(2,1)S(1)} %collective-permute-done.12.refs_7_.refs_3_, ...), custom_call_target="tpu_custom_call" | custom-call | flops 805306368 | tf_op jit(solution)/shard_map/pallas_call | solution.py:27
  95.4 1.3 %shard_map.143 = (f32[128,1024]{1,0:T(8,128)}, f32[1,128]{1,0:T(1,128)}, f32[2,128]{1,0:T(2,128)}) custom-call(bf16[48,1152]{1,0:T(8,128)(2,1)S(1)} %get-tuple-element.63.refs_0_, bf16[48,1152]{1,0:T(8,128)(2,1)S(1)} %collective-permute-done.33.refs_1_, bf16[48,1152]{1,0:T(8,128)(2,1)S(1)} %collective-permute-done.34.refs_2_, ...), custom_call_target="tpu_custom_call" | custom-call | tf_op jit(solution)/shard_map/pallas_call | solution.py:27
  (76 shorter events, 0.9 us)
Async XLA Ops:
  2.3 8.9 %collective-permute-start = (bf16[48,1024]{1,0:T(8,128)(2,1)S(1)}, bf16[48,1024]{1,0:T(8,128)(2,1)S(1)}, u32[]{:S(2)}, u32[]{:S(2)}) collective-permute-start(bf16[48,1024]{1,0:T(8,128)(2,1)S(1)} %get-tuple-element.31), channel_id=1, source_target_pairs={{0,8},{2,10},{4,12},{6,14},{8,0},{10,2},{12,4},{14,6},{16,24},{18,... | collective-permute-start | bytes 294920 | tf_op jit(solution)/shard_map/ppermute | solution.py:233
  5.4 25.6 %collective-permute-start.14 = (bf16[48,2176]{1,0:T(8,128)(2,1)S(1)}, bf16[48,2176]{1,0:T(8,128)(2,1)S(1)}, u32[]{:S(2)}, u32[]{:S(2)}) collective-permute-start(bf16[48,2176]{1,0:T(8,128)(2,1)S(1)} %get-tuple-element.30), channel_id=1, source_target_pairs={{0,4},{2,6},{4,0},{6,2},{8,12},{10,14},{12,8},{14,10},{16,20},{18,... | collective-permute-start | bytes 626696 | tf_op jit(solution)/shard_map/ppermute | solution.py:236
  6.9 25.7 %collective-permute-start.16 = (bf16[48,2176]{1,0:T(8,128)(2,1)S(1)}, bf16[48,2176]{1,0:T(8,128)(2,1)S(1)}, u32[]{:S(2)}, u32[]{:S(2)}) collective-permute-start(bf16[48,2176]{1,0:T(8,128)(2,1)S(1)} %get-tuple-element.30), channel_id=1, source_target_pairs={{0,5},{1,4},{2,7},{3,6},{4,1},{5,0},{6,3},{7,2},{8,13},{9,12},{10,... | collective-permute-start | bytes 626696 | tf_op jit(solution)/shard_map/ppermute | solution.py:250
  8.4 13.3 %collective-permute-start.1 = (bf16[48,1024]{1,0:T(8,128)(2,1)S(1)}, bf16[48,1024]{1,0:T(8,128)(2,1)S(1)}, u32[]{:S(2)}, u32[]{:S(2)}) collective-permute-start(bf16[48,1024]{1,0:T(8,128)(2,1)S(1)} %get-tuple-element.32), channel_id=1, source_target_pairs={{0,16},{2,18},{4,20},{6,22},{8,24},{10,26},{12,28},{14,30},{16,0},... | collective-permute-start | bytes 294920 | tf_op jit(solution)/shard_map/ppermute | solution.py:233
  11.0 10.7 %collective-permute-start.2 = (bf16[48,1024]{1,0:T(8,128)(2,1)S(1)}, bf16[48,1024]{1,0:T(8,128)(2,1)S(1)}, u32[]{:S(2)}, u32[]{:S(2)}) collective-permute-start(bf16[48,1024]{1,0:T(8,128)(2,1)S(1)} %get-tuple-element.33), channel_id=1, source_target_pairs={{0,24},{2,26},{4,28},{6,30},{8,16},{10,18},{12,20},{14,22},{16,8},... | collective-permute-start | bytes 294920 | tf_op jit(solution)/shard_map/ppermute | solution.py:233
  11.2 13.8 %collective-permute-start.9 = (bf16[48,1152]{1,0:T(8,128)(2,1)S(1)}, bf16[48,1152]{1,0:T(8,128)(2,1)S(1)}, u32[]{:S(2)}, u32[]{:S(2)}) collective-permute-start(bf16[48,1152]{1,0:T(8,128)(2,1)S(1)} %get-tuple-element.36), channel_id=1, source_target_pairs={{0,24},{2,26},{4,28},{6,30},{8,16},{10,18},{12,20},{14,22},{16,8},... | collective-permute-start | bytes 331784 | tf_op jit(solution)/shard_map/ppermute | solution.py:233
  21.7 7.1 %collective-permute-start.8 = (bf16[48,1152]{1,0:T(8,128)(2,1)S(1)}, bf16[48,1152]{1,0:T(8,128)(2,1)S(1)}, u32[]{:S(2)}, u32[]{:S(2)}) collective-permute-start(bf16[48,1152]{1,0:T(8,128)(2,1)S(1)} %get-tuple-element.35), channel_id=1, source_target_pairs={{0,16},{2,18},{4,20},{6,22},{8,24},{10,26},{12,28},{14,30},{16,0},... | collective-permute-start | bytes 331784 | tf_op jit(solution)/shard_map/ppermute | solution.py:233
  21.7 7.6 %collective-permute-start.7 = (bf16[48,1152]{1,0:T(8,128)(2,1)S(1)}, bf16[48,1152]{1,0:T(8,128)(2,1)S(1)}, u32[]{:S(2)}, u32[]{:S(2)}) collective-permute-start(bf16[48,1152]{1,0:T(8,128)(2,1)S(1)} %get-tuple-element.34), channel_id=1, source_target_pairs={{0,8},{2,10},{4,12},{6,14},{8,0},{10,2},{12,4},{14,6},{16,24},{18,... | collective-permute-start | bytes 331784 | tf_op jit(solution)/shard_map/ppermute | solution.py:233
  25.0 15.2 %collective-permute-start.15 = (bf16[144,1024]{1,0:T(8,128)(2,1)S(1)}, bf16[144,1024]{1,0:T(8,128)(2,1)S(1)}, u32[]{:S(2)}, u32[]{:S(2)}) collective-permute-start(bf16[144,1024]{1,0:T(8,128)(2,1)S(1)} %constant_dynamic-update-slice_fusion), channel_id=1, source_target_pairs={{0,4},{2,6},{4,0},{6,2},{8,12},{10,14},{12,8},{14,10},{16,20},{18,... | collective-permute-start | bytes 884744 | tf_op jit(solution)/shard_map/ppermute | solution.py:236
  28.8 9.9 %collective-permute-start.4 = (bf16[144,1024]{1,0:T(8,128)(2,1)S(1)}, bf16[144,1024]{1,0:T(8,128)(2,1)S(1)}, u32[]{:S(2)}, u32[]{:S(2)}) collective-permute-start(bf16[144,1024]{1,0:T(8,128)(2,1)S(1)} %constant_dynamic-update-slice_fusion), channel_id=1, source_target_pairs={{0,1},{1,0},{2,3},{3,2},{4,5},{5,4},{6,7},{7,6},{8,9},{9,8},{10,11... | collective-permute-start | bytes 884744 | tf_op jit(solution)/shard_map/ppermute | solution.py:242
  29.4 16.9 %collective-permute-start.21 = (bf16[144,1152]{1,0:T(8,128)(2,1)S(1)}, bf16[144,1152]{1,0:T(8,128)(2,1)S(1)}, u32[]{:S(2)}, u32[]{:S(2)}) collective-permute-start(bf16[144,1152]{1,0:T(8,128)(2,1)S(1)} %pad_maximum_fusion.6), channel_id=1, source_target_pairs={{0,4},{2,6},{4,0},{6,2},{8,12},{10,14},{12,8},{14,10},{16,20},{18,... | collective-permute-start | bytes 995336 | tf_op jit(solution)/shard_map/ppermute | solution.py:236
  31.0 12.9 %collective-permute-start.10 = (bf16[144,1024]{1,0:T(8,128)(2,1)S(1)}, bf16[144,1024]{1,0:T(8,128)(2,1)S(1)}, u32[]{:S(2)}, u32[]{:S(2)}) collective-permute-start(bf16[144,1024]{1,0:T(8,128)(2,1)S(1)} %pad_maximum_fusion.7), channel_id=1, source_target_pairs={{0,1},{1,0},{2,3},{3,2},{4,5},{5,4},{6,7},{7,6},{8,9},{9,8},{10,11... | collective-permute-start | bytes 884744 | tf_op jit(solution)/shard_map/ppermute | solution.py:242
  38.7 8.3 %collective-permute-start.18 = (bf16[144,512]{1,0:T(8,128)(2,1)S(1)}, bf16[144,512]{1,0:T(8,128)(2,1)S(1)}, u32[]{:S(2)}, u32[]{:S(2)}) collective-permute-start(bf16[144,512]{1,0:T(8,128)(2,1)S(1)} %slice.150), channel_id=1, source_target_pairs={{0,4},{2,6},{4,0},{6,2},{8,12},{10,14},{12,8},{14,10},{16,20},{18,... | collective-permute-start | bytes 442376 | tf_op jit(solution)/shard_map/ppermute | solution.py:236
  40.3 6.8 %collective-permute-start.17 = (bf16[144,512]{1,0:T(8,128)(2,1)S(1)}, bf16[144,512]{1,0:T(8,128)(2,1)S(1)}, u32[]{:S(2)}, u32[]{:S(2)}) collective-permute-start(bf16[144,512]{1,0:T(8,128)(2,1)S(1)} %slice.149), channel_id=1, source_target_pairs={{0,1},{1,0},{2,3},{3,2},{4,5},{5,4},{6,7},{7,6},{8,9},{9,8},{10,11... | collective-permute-start | bytes 442376 | tf_op jit(solution)/shard_map/ppermute | solution.py:242
  40.9 11.5 %collective-permute-start.19 = (bf16[192,1024]{1,0:T(8,128)(2,1)S(1)}, bf16[192,1024]{1,0:T(8,128)(2,1)S(1)}, u32[]{:S(2)}, u32[]{:S(2)}) collective-permute-start(bf16[192,1024]{1,0:T(8,128)(2,1)S(1)} %pad_maximum_fusion.5.refs_0_.refs_4_), channel_id=1, source_target_pairs={{0,2},{2,0},{4,6},{6,4},{8,10},{10,8},{12,14},{14,12},{16,18},{18,... | collective-permute-start | bytes 1179656 | tf_op jit(solution)/shard_map/ppermute | solution.py:239
  43.9 5.5 %collective-permute-start.23 = (bf16[144,512]{1,0:T(8,128)(2,1)S(1)}, bf16[144,512]{1,0:T(8,128)(2,1)S(1)}, u32[]{:S(2)}, u32[]{:S(2)}) collective-permute-start(bf16[144,512]{1,0:T(8,128)(2,1)S(1)} %slice.154), channel_id=1, source_target_pairs={{0,4},{2,6},{4,0},{6,2},{8,12},{10,14},{12,8},{14,10},{16,20},{18,... | collective-permute-start | bytes 442376 | tf_op jit(solution)/shard_map/ppermute | solution.py:236
  46.3 5.2 %collective-permute-start.22 = (bf16[144,512]{1,0:T(8,128)(2,1)S(1)}, bf16[144,512]{1,0:T(8,128)(2,1)S(1)}, u32[]{:S(2)}, u32[]{:S(2)}) collective-permute-start(bf16[144,512]{1,0:T(8,128)(2,1)S(1)} %slice.153), channel_id=1, source_target_pairs={{0,1},{1,0},{2,3},{3,2},{4,5},{5,4},{6,7},{7,6},{8,9},{9,8},{10,11... | collective-permute-start | bytes 442376 | tf_op jit(solution)/shard_map/ppermute | solution.py:242
  47.0 5.6 %collective-permute-start.24 = (bf16[192,1152]{1,0:T(8,128)(2,1)S(1)}, bf16[192,1152]{1,0:T(8,128)(2,1)S(1)}, u32[]{:S(2)}, u32[]{:S(2)}) collective-permute-start(bf16[192,1152]{1,0:T(8,128)(2,1)S(1)} %pad_maximum_fusion.1.refs_4_), channel_id=1, source_target_pairs={{0,2},{2,0},{4,6},{6,4},{8,10},{10,8},{12,14},{14,12},{16,18},{18,... | collective-permute-start | bytes 1327112 | tf_op jit(solution)/shard_map/ppermute | solution.py:239
  47.1 6.2 %copy-start.4 = (bf16[1,2048,256]{2,1,0:T(8,128)(2,1)S(1)}, bf16[1,2048,256]{2,1,0:T(8,128)(2,1)}, u32[]{:S(2)}) copy-start(bf16[1,2048,256]{2,1,0:T(8,128)(2,1)} %param.15) | copy-start | bytes 3145732
  47.1 6.2 %copy-start.5 = (bf16[1,2048,256]{2,1,0:T(8,128)(2,1)S(1)}, bf16[1,2048,256]{2,1,0:T(8,128)(2,1)}, u32[]{:S(2)}) copy-start(bf16[1,2048,256]{2,1,0:T(8,128)(2,1)} %param.16) | copy-start | bytes 3145732
  47.1 6.2 %copy-start.6 = (bf16[1,256,2048]{2,1,0:T(8,128)(2,1)S(1)}, bf16[1,256,2048]{2,1,0:T(8,128)(2,1)}, u32[]{:S(2)}) copy-start(bf16[1,256,2048]{2,1,0:T(8,128)(2,1)} %param.17) | copy-start | bytes 3145732
  47.2 5.8 %collective-permute-start.20 = (bf16[192,1024]{1,0:T(8,128)(2,1)S(1)}, bf16[192,1024]{1,0:T(8,128)(2,1)S(1)}, u32[]{:S(2)}, u32[]{:S(2)}) collective-permute-start(bf16[192,1024]{1,0:T(8,128)(2,1)S(1)} %maximum_maximum_fusion.refs_1_.refs_5_), channel_id=1, source_target_pairs={{0,2},{2,0},{4,6},{6,4},{8,10},{10,8},{12,14},{14,12},{16,18},{18,... | collective-permute-start | bytes 1179656 | tf_op jit(solution)/shard_map/ppermute | solution.py:239
  51.5 1.8 %collective-permute-start.25 = (bf16[192,1024]{1,0:T(8,128)(2,1)S(1)}, bf16[192,1024]{1,0:T(8,128)(2,1)S(1)}, u32[]{:S(2)}, u32[]{:S(2)}) collective-permute-start(bf16[192,1024]{1,0:T(8,128)(2,1)S(1)} %maximum_maximum_fusion.1.refs_5_), channel_id=1, source_target_pairs={{0,2},{2,0},{4,6},{6,4},{8,10},{10,8},{12,14},{14,12},{16,18},{18,... | collective-permute-start | bytes 1179656 | tf_op jit(solution)/shard_map/ppermute | solution.py:239
  51.6 7.6 %collective-permute-start.3 = (bf16[48,2176]{1,0:T(8,128)(2,1)S(1)}, bf16[48,2176]{1,0:T(8,128)(2,1)S(1)}, u32[]{:S(2)}, u32[]{:S(2)}) collective-permute-start(bf16[48,2176]{1,0:T(8,128)(2,1)S(1)} %get-tuple-element.30), channel_id=1, source_target_pairs={{0,1},{1,0},{2,3},{3,2},{4,5},{5,4},{6,7},{7,6},{8,9},{9,8},{10,11... | collective-permute-start | bytes 626696 | tf_op jit(solution)/shard_map/ppermute | solution.py:242
  52.4 8.1 %collective-permute-start.5 = (bf16[192,1024]{1,0:T(8,128)(2,1)S(1)}, bf16[192,1024]{1,0:T(8,128)(2,1)S(1)}, u32[]{:S(2)}, u32[]{:S(2)}) collective-permute-start(bf16[192,1024]{1,0:T(8,128)(2,1)S(1)} %pad_maximum_fusion.2.refs_0_), channel_id=1, source_target_pairs={{0,2},{2,0},{4,6},{6,4},{8,10},{10,8},{12,14},{14,12},{16,18},{18,... | collective-permute-start | bytes 1179656 | tf_op jit(solution)/shard_map/ppermute | solution.py:239
  52.6 7.8 %collective-permute-start.11 = (bf16[192,1152]{1,0:T(8,128)(2,1)S(1)}, bf16[192,1152]{1,0:T(8,128)(2,1)S(1)}, u32[]{:S(2)}, u32[]{:S(2)}) collective-permute-start(bf16[192,1152]{1,0:T(8,128)(2,1)S(1)} %pad_maximum_fusion.refs_4_.refs_0_), channel_id=1, source_target_pairs={{0,2},{2,0},{4,6},{6,4},{8,10},{10,8},{12,14},{14,12},{16,18},{18,... | collective-permute-start | bytes 1327112 | tf_op jit(solution)/shard_map/ppermute | solution.py:239
  56.8 3.0 %copy-start = (s32[128]{0:T(128)S(1)}, s32[128]{0:T(128)}, u32[]{:S(2)}) copy-start(s32[128]{0:T(128)} %param.13) | copy-start | bytes 1540
  56.9 8.4 %collective-permute-start.26 = (bf16[192,2176]{1,0:T(8,128)(2,1)S(1)}, bf16[192,2176]{1,0:T(8,128)(2,1)S(1)}, u32[]{:S(2)}, u32[]{:S(2)}) collective-permute-start(bf16[192,2176]{1,0:T(8,128)(2,1)S(1)} %get-tuple-element.40), channel_id=1, source_target_pairs={{0,2},{2,0},{4,6},{6,4},{8,10},{10,8},{12,14},{14,12},{16,18},{18,... | collective-permute-start | bytes 2506760 | tf_op jit(solution)/shard_map/ppermute | solution.py:239
  59.2 1.8 %collective-permute-start.6 = (bf16[192,1024]{1,0:T(8,128)(2,1)S(1)}, bf16[192,1024]{1,0:T(8,128)(2,1)S(1)}, u32[]{:S(2)}, u32[]{:S(2)}) collective-permute-start(bf16[192,1024]{1,0:T(8,128)(2,1)S(1)} %pad_maximum_fusion.3.refs_1_), channel_id=1, source_target_pairs={{0,2},{2,0},{4,6},{6,4},{8,10},{10,8},{12,14},{14,12},{16,18},{18,... | collective-permute-start | bytes 1179656 | tf_op jit(solution)/shard_map/ppermute | solution.py:239
  59.3 2.2 %collective-permute-start.12 = (bf16[192,1024]{1,0:T(8,128)(2,1)S(1)}, bf16[192,1024]{1,0:T(8,128)(2,1)S(1)}, u32[]{:S(2)}, u32[]{:S(2)}) collective-permute-start(bf16[192,1024]{1,0:T(8,128)(2,1)S(1)} %pad_maximum_fusion.4.refs_5_.refs_1_), channel_id=1, source_target_pairs={{0,2},{2,0},{4,6},{6,4},{8,10},{10,8},{12,14},{14,12},{16,18},{18,... | collective-permute-start | bytes 1179656 | tf_op jit(solution)/shard_map/ppermute | solution.py:239
  65.1 2.4 %collective-permute-start.13 = (bf16[192,2176]{1,0:T(8,128)(2,1)S(1)}, bf16[192,2176]{1,0:T(8,128)(2,1)S(1)}, u32[]{:S(2)}, u32[]{:S(2)}) collective-permute-start(bf16[192,2176]{1,0:T(8,128)(2,1)S(1)} %get-tuple-element.38), channel_id=1, source_target_pairs={{0,2},{2,0},{4,6},{6,4},{8,10},{10,8},{12,14},{14,12},{16,18},{18,... | collective-permute-start | bytes 2506760 | tf_op jit(solution)/shard_map/ppermute | solution.py:239
  65.6 7.8 %collective-permute-start.28 = (bf16[192,512]{1,0:T(8,128)(2,1)S(1)}, bf16[192,512]{1,0:T(8,128)(2,1)S(1)}, u32[]{:S(2)}, u32[]{:S(2)}) collective-permute-start(bf16[192,512]{1,0:T(8,128)(2,1)S(1)} %pad_maximum_fusion.8), channel_id=1, source_target_pairs={{0,4},{2,6},{4,0},{6,2},{8,12},{10,14},{12,8},{14,10},{16,20},{18,... | collective-permute-start | bytes 589832 | tf_op jit(solution)/shard_map/ppermute | solution.py:236
  65.7 8.9 %collective-permute-start.31 = (bf16[192,640]{1,0:T(8,128)(2,1)S(1)}, bf16[192,640]{1,0:T(8,128)(2,1)S(1)}, u32[]{:S(2)}, u32[]{:S(2)}) collective-permute-start(bf16[192,640]{1,0:T(8,128)(2,1)S(1)} %slice.164), channel_id=1, source_target_pairs={{0,1},{1,0},{2,3},{3,2},{4,5},{5,4},{6,7},{7,6},{8,9},{9,8},{10,11... | collective-permute-start | bytes 737288 | tf_op jit(solution)/shard_map/ppermute | solution.py:242
  67.7 16.0 %collective-permute-start.30 = (bf16[192,640]{1,0:T(8,128)(2,1)S(1)}, bf16[192,640]{1,0:T(8,128)(2,1)S(1)}, u32[]{:S(2)}, u32[]{:S(2)}) collective-permute-start(bf16[192,640]{1,0:T(8,128)(2,1)S(1)} %slice.194), channel_id=1, source_target_pairs={{0,1},{1,0},{2,3},{3,2},{4,5},{5,4},{6,7},{7,6},{8,9},{9,8},{10,11... | collective-permute-start | bytes 737288 | tf_op jit(solution)/shard_map/ppermute | solution.py:242
  68.5 15.2 %collective-permute-start.27 = (bf16[192,384]{1,0:T(8,128)(2,1)S(1)}, bf16[192,384]{1,0:T(8,128)(2,1)S(1)}, u32[]{:S(2)}, u32[]{:S(2)}) collective-permute-start(bf16[192,384]{1,0:T(8,128)(2,1)S(1)} %get-tuple-element.58), channel_id=1, source_target_pairs={{0,4},{2,6},{4,0},{6,2},{8,12},{10,14},{12,8},{14,10},{16,20},{18,... | collective-permute-start | bytes 442376 | tf_op jit(solution)/shard_map/ppermute | solution.py:236
  73.5 9.9 %collective-permute-start.29 = (bf16[192,512]{1,0:T(8,128)(2,1)S(1)}, bf16[192,512]{1,0:T(8,128)(2,1)S(1)}, u32[]{:S(2)}, u32[]{:S(2)}) collective-permute-start(bf16[192,512]{1,0:T(8,128)(2,1)S(1)} %get-tuple-element.54), channel_id=1, source_target_pairs={{0,1},{1,0},{2,3},{3,2},{4,5},{5,4},{6,7},{7,6},{8,9},{9,8},{10,11... | collective-permute-start | bytes 589832 | tf_op jit(solution)/shard_map/ppermute | solution.py:242
  74.6 9.1 %collective-permute-start.32 = (bf16[192,640]{1,0:T(8,128)(2,1)S(1)}, bf16[192,640]{1,0:T(8,128)(2,1)S(1)}, u32[]{:S(2)}, u32[]{:S(2)}) collective-permute-start(bf16[192,640]{1,0:T(8,128)(2,1)S(1)} %fusion.1), channel_id=1, source_target_pairs={{0,4},{2,6},{4,0},{6,2},{8,12},{10,14},{12,8},{14,10},{16,20},{18,... | collective-permute-start | bytes 737288 | tf_op jit(solution)/shard_map/ppermute | solution.py:236
  83.9 11.5 %collective-permute-start.33 = (bf16[48,1152]{1,0:T(8,128)(2,1)S(1)}, bf16[48,1152]{1,0:T(8,128)(2,1)S(1)}, u32[]{:S(2)}, u32[]{:S(2)}) collective-permute-start(bf16[48,1152]{1,0:T(8,128)(2,1)S(1)} %get-tuple-element.62), channel_id=1, source_target_pairs={{0,8},{2,10},{4,12},{6,14},{8,0},{10,2},{12,4},{14,6},{16,24},{18,... | collective-permute-start | bytes 331784 | tf_op jit(solution)/shard_map/ppermute | solution.py:233
  84.0 11.4 %collective-permute-start.34 = (bf16[48,1152]{1,0:T(8,128)(2,1)S(1)}, bf16[48,1152]{1,0:T(8,128)(2,1)S(1)}, u32[]{:S(2)}, u32[]{:S(2)}) collective-permute-start(bf16[48,1152]{1,0:T(8,128)(2,1)S(1)} %get-tuple-element.61), channel_id=1, source_target_pairs={{0,16},{2,18},{4,20},{6,22},{8,24},{10,26},{12,28},{14,30},{16,0},... | collective-permute-start | bytes 331784 | tf_op jit(solution)/shard_map/ppermute | solution.py:233
  87.1 8.3 %collective-permute-start.35 = (bf16[48,1152]{1,0:T(8,128)(2,1)S(1)}, bf16[48,1152]{1,0:T(8,128)(2,1)S(1)}, u32[]{:S(2)}, u32[]{:S(2)}) collective-permute-start(bf16[48,1152]{1,0:T(8,128)(2,1)S(1)} %get-tuple-element.60), channel_id=1, source_target_pairs={{0,24},{2,26},{4,28},{6,30},{8,16},{10,18},{12,20},{14,22},{16,8},... | collective-permute-start | bytes 331784 | tf_op jit(solution)/shard_map/ppermute | solution.py:233
  92.8 2.6 %copy-start.1 = (s32[128,2]{0,1:T(2,128)S(1)}, s32[128,2]{0,1:T(2,128)}, u32[]{:S(2)}) copy-start(s32[128,2]{0,1:T(2,128)} %param.14) | copy-start | bytes 3076
  92.8 2.6 %copy-start.2 = (f32[128,2]{0,1:T(2,128)S(1)}, f32[128,2]{0,1:T(2,128)}, u32[]{:S(2)}) copy-start(f32[128,2]{0,1:T(2,128)} %param.12) | copy-start | bytes 3076
  92.8 2.7 %copy-start.3 = (f32[128]{0:T(128)S(1)}, f32[128]{0:T(128)}, u32[]{:S(2)}) copy-start(f32[128]{0:T(128)} %param.11) | copy-start | bytes 1540

commit v2 on v1

--- a/solution.py
+++ b/solution.py
@@ -39,10 +39,10 @@
 
 def route_body(groups, cap, width, *refs):
     sources = refs[:6]
-    own_out = refs[6]
-    tok_out = refs[7 : 6 + groups]
-    cot_out = refs[6 + groups : 5 + 2 * groups]
-    choice_ref, local_ref, weight_ref, expert_ref, tok_ref, cot_ref, sems = refs[5 + 2 * groups :]
+    whole_out = refs[6:8]
+    tok_out = refs[8 : 6 + groups]
+    cot_out = refs[6 + groups : 4 + 2 * groups]
+    choice_ref, local_ref, weight_ref, expert_ref, tok_ref, cot_ref, sems = refs[4 + 2 * groups :]
     count = tok_ref.shape[0]
     own = lax.axis_index("ep") // EPG
     start = pl.multiple_of(lax.axis_index("tp") * width, width)
@@ -80,15 +80,21 @@
     ]
     gate_rows = [dot(pick, gates, ROWS_COLS).astype(BF16) for pick in picks]
     copies[4].wait()
-    for k in range(1, groups):
-        tok_out[k - 1][...] = dot(picks[k], tok_ref[...], COLS_ROWS).astype(BF16)
-    own_out[:, :width] = dot(picks[0], tok_ref[...], COLS_ROWS).astype(BF16)
+    for k in range(groups):
+        rows = dot(picks[k], tok_ref[...], COLS_ROWS).astype(BF16)
+        if k < 2:
+            whole_out[k][:, :width] = rows
+        else:
+            tok_out[k - 2][...] = rows
     copies[5].wait()
-    for k in range(1, groups):
-        cot_out[k - 1][:, :width] = dot(picks[k], cot_ref[...], COLS_ROWS).astype(BF16)
-        cot_out[k - 1][:, width:] = gate_rows[k]
-    own_out[:, width : 2 * width] = dot(picks[0], cot_ref[...], COLS_ROWS).astype(BF16)
-    own_out[:, 2 * width :] = gate_rows[0]
+    for k in range(groups):
+        rows = dot(picks[k], cot_ref[...], COLS_ROWS).astype(BF16)
+        if k < 2:
+            whole_out[k][:, width : 2 * width] = rows
+            whole_out[k][:, 2 * width :] = gate_rows[k]
+        else:
+            cot_out[k - 2][:, :width] = rows
+            cot_out[k - 2][:, width:] = gate_rows[k]
 
 
 def picks_body(groups, cap, parts, choice_ref, out_ref):
@@ -109,31 +115,47 @@
         out_ref[pl.ds(i * cap, cap), :] = pick.astype(F32).astype(BF16)
 
 
-def expert_body(lanes, width, *refs):
-    tok = [refs[c * lanes : (c + 1) * lanes] for c in range(2)]
-    cot = [refs[(2 + c) * lanes : (3 + c) * lanes] for c in range(2)]
-    gate_w, up_w, down_w = refs[4 * lanes : 4 * lanes + 3]
-    sums = refs[4 * lanes + 3 : 4 * lanes + 5]
-    grads = refs[4 * lanes + 5 : 4 * lanes + 7]
-    scaled_hidden = refs[4 * lanes + 7 : 4 * lanes + 9]
-    rows = tok[0][0].shape[0]
-    cols = gate_w.shape[1]
-    mine = lax.axis_index("ep") % EPG
+def spans_of(lanes, width):
     rank = lax.axis_index("tp")
-    spans = [
+    return [
         pl.ds(pl.multiple_of(((rank + lanes - j) % lanes) * width, width), width)
         for j in range(lanes)
     ]
+
+
+def pre_body(lanes, width, *refs):
+    tok = [refs[c * lanes : (c + 1) * lanes] for c in range(2)]
+    gate_w, up_w = refs[2 * lanes : 2 * lanes + 2]
+    outs = refs[2 * lanes + 2 :]
+    cols = gate_w.shape[1]
+    spans = spans_of(lanes, width)
+    for c in range(2):
+        gate = dot(tok[c][0][...], gate_w[spans[0], :], COLS_ROWS)
+        up = dot(tok[c][0][...], up_w[spans[0], :], COLS_ROWS)
+        for j in range(1, lanes):
+            gate = gate + dot(tok[c][j][...], gate_w[spans[j], :], COLS_ROWS)
+            up = up + dot(tok[c][j][...], up_w[spans[j], :], COLS_ROWS)
+        outs[c][:, :cols] = gate
+        outs[c][:, cols:] = up
+
+
+def main_body(lanes, width, *refs):
+    pre = refs[:2]
+    cot = [refs[2 + c * lanes : 2 + (c + 1) * lanes] for c in range(2)]
+    gate_w, up_w, down_w = refs[2 + 2 * lanes : 5 + 2 * lanes]
+    outs = refs[5 + 2 * lanes :]
+    sums, grads, scaled_hidden = outs[:2], outs[2:4], outs[4:6]
+    rows = pre[0].shape[0]
+    cols = gate_w.shape[1]
+    mine = lax.axis_index("ep") % EPG
+    spans = spans_of(lanes, width)
     lane = lax.broadcasted_iota(jnp.int32, (rows, LANES), 1)
-    for c in range(2):
-        pre_gate = jnp.zeros((rows, cols), F32)
-        pre_up = jnp.zeros((rows, cols), F32)
-        back = jnp.zeros((rows, cols), F32)
-        for j in range(lanes):
-            part = tok[c][j][...]
-            pre_gate = pre_gate + dot(part, gate_w[spans[j], :], COLS_ROWS)
-            pre_up = pre_up + dot(part, up_w[spans[j], :], COLS_ROWS)
-            back = back + dot(cot[c][j][:, :width], down_w[:, spans[j]], ROWS_COLS)
+    for c in (1, 0):
+        pre_gate = pre[c][:, :cols]
+        pre_up = pre[c][:, cols:]
+        back = dot(cot[c][0][:, :width], down_w[:, spans[0]], ROWS_COLS)
+        for j in range(1, lanes):
+            back = back + dot(cot[c][j][...], down_w[:, spans[j]], ROWS_COLS)
         gates = cot[c][0][:, width:].astype(F32)
         gate = jnp.sum(jnp.where(lane == mine, gates, 0.0), axis=1, keepdims=True)
         sigma = jax.nn.sigmoid(pre_gate)
@@ -146,14 +168,24 @@
         grads[c][:, :cols] = grad_gate
         grads[c][:, cols:] = grad_up
         scaled_hidden[c][...] = (gate * hidden).astype(BF16)
-        for j in range(lanes):
+        for j in range(1, lanes):
             total = dot(grad_gate, gate_w[spans[j], :], ROWS_COLS)
             total = total + dot(grad_up, up_w[spans[j], :], ROWS_COLS)
-            sums[c][:, j * width : (j + 1) * width] = total.astype(sums[c].dtype)
+            sums[c][:, (j - 1) * width : j * width] = total.astype(sums[c].dtype)
         high = gate_part.astype(BF16).astype(F32)
         low = gate_part - high
         tail = jnp.where(lane == mine, high, jnp.where(lane == mine + EPG, low, 0.0))
-        sums[c][:, lanes * width :] = tail.astype(sums[c].dtype)
+        sums[c][:, (lanes - 1) * width :] = tail.astype(sums[c].dtype)
+
+
+def own_body(lanes, width, *refs):
+    grads, (gate_w, up_w), sums = refs[:2], refs[2:4], refs[4:]
+    cols = gate_w.shape[1]
+    span = spans_of(lanes, width)[0]
+    for c in (1, 0):
+        total = dot(grads[c][:, :cols], gate_w[span, :], ROWS_COLS)
+        total = total + dot(grads[c][:, cols:], up_w[span, :], ROWS_COLS)
+        sums[c][...] = total.astype(sums[c].dtype)
 
 
 def up_body(lanes, width, *refs):
@@ -241,14 +273,6 @@
     def along_tp(a, j):
         return lax.ppermute(a, "tp", [(r, (r + j) % lanes) for r in range(lanes)])
 
-    def along_both(a, j):
-        pairs = [
-            (e * lanes + r, (e ^ 2) * lanes + (r + j) % lanes)
-            for e in range(experts)
-            for r in range(lanes)
-        ]
-        return lax.ppermute(a, ("ep", "tp"), pairs)
-
     shape = jax.ShapeDtypeStruct
     choice_row = group_choice.reshape(1, count)
     weight_row = group_weight.reshape(1, count)
@@ -256,9 +280,9 @@
     expert_rows = expert_weight.T
     routed = call(
         functools.partial(route_body, groups, cap, width),
-        [shape((cap, 2 * width + LANES), BF16)]
-        + [shape((cap, width), BF16)] * (groups - 1)
-        + [shape((cap, width + LANES), BF16)] * (groups - 1),
+        [shape((cap, 2 * width + LANES), BF16)] * 2
+        + [shape((cap, width), BF16)] * (groups - 2)
+        + [shape((cap, width + LANES), BF16)] * (groups - 2),
         space=pltpu.HBM,
         scratch=[
             pltpu.VMEM((1, count), jnp.int32),
@@ -284,16 +308,26 @@
         )(choice_row)
         for part in parts
     ]
-    own = routed[0]
-    others = range(groups - 1, 0, -1)
+    others = range(groups - 1, 1, -1)
+    next_sent = along_groups(routed[1], 1)
     tok_sent = {k: along_groups(routed[k], k) for k in others}
-    own_side = along_side(own)
-    own_lane = [along_tp(own, j) for j in range(1, lanes)]
-    cot_sent = {k: along_groups(routed[groups - 1 + k], k) for k in others}
-    own_both = [along_both(own, j) for j in range(1, lanes)]
-    tok = jnp.concatenate([tok_sent[k] for k in range(1, groups)], axis=0)
-    cot = jnp.concatenate([cot_sent[k] for k in range(1, groups)], axis=0)
-    cot_bare = jnp.concatenate([cot_sent[k][:, :width] for k in range(1, groups)], axis=0)
+
+    def join(head, rest):
+        return jnp.concatenate([head, rest], axis=0)
+
+    own_side = along_side(routed[0])
+    own_lane = [along_tp(routed[0][:, : 2 * width], j) for j in range(1, lanes)]
+    next_side = along_side(next_sent)
+    next_lane = [along_tp(next_sent[:, : 2 * width], j) for j in range(1, lanes)]
+    own = join(routed[0], next_sent)
+    own_side = join(own_side, next_side)
+    own_lane = [join(a, b) for a, b in zip(own_lane, next_lane)]
+    cot_sent = {k: along_groups(routed[groups - 2 + k], k) for k in range(2, groups)}
+    own_tok_both = [along_tp(own_side[:, :width], j) for j in range(1, lanes)]
+    own_cot_both = [along_side(a[:, width:]) for a in own_lane]
+    tok = jnp.concatenate([tok_sent[k] for k in range(2, groups)], axis=0)
+    cot = jnp.concatenate([cot_sent[k] for k in range(2, groups)], axis=0)
+    cot_bare = jnp.concatenate([cot_sent[k][:, :width] for k in range(2, groups)], axis=0)
     tok_side = along_side(tok)
     tok_lane = [along_tp(tok, j) for j in range(1, lanes)]
     cot_side = along_side(cot)
@@ -310,61 +344,66 @@
     tok_both = diagonal(tok_side, tok_lane)
     cot_both = diagonal(cot_side, cot_lane)
 
-    def join(head, rest):
-        return jnp.concatenate([head, rest], axis=0)
-
     tok_near = [join(own[:, :width], tok)]
     tok_near += [join(a[:, :width], b) for a, b in zip(own_lane, tok_lane)]
     cot_near = [join(own[:, width:], cot)]
-    cot_near += [join(a[:, width : 2 * width], b) for a, b in zip(own_lane, cot_lane)]
+    cot_near += [join(a[:, width:], b) for a, b in zip(own_lane, cot_lane)]
     tok_far = [join(own_side[:, :width], tok_side)]
-    tok_far += [join(a[:, :width], b) for a, b in zip(own_both, tok_both)]
+    tok_far += [join(a, b) for a, b in zip(own_tok_both, tok_both)]
     cot_far = [join(own_side[:, width:], cot_side)]
-    cot_far += [join(a[:, width : 2 * width], b) for a, b in zip(own_both, cot_both)]
+    cot_far += [join(a, b) for a, b in zip(own_cot_both, cot_both)]
     first, second, third = w_gate[0], w_up[0], w_down[0]
-    work = 2 * 5 * 2 * rows * features * cols
+    work = 2 * 2 * rows * features * cols
+    rest_width = features - width
 
     def experts_on(tok_list, cot_list):
-        tok_other = [along_core(a) for a in tok_list]
-        cot_other = [along_core(a) for a in cot_list]
+        tok_other = [along_core(tok_list[0])]
+        cot_other = [along_core(cot_list[0])]
+        tok_other += [along_core(a) for a in tok_list[1:]]
+        cot_other += [along_core(a) for a in cot_list[1:]]
+        pre = call(
+            functools.partial(pre_body, lanes, width), [shape((rows, 2 * cols), F32)] * 2, 2 * work
+        )(*tok_list, *tok_other, first, second)
         outs = call(
-            functools.partial(expert_body, lanes, width),
-            [shape((rows, features + LANES), F32), shape((rows, features + LANES), BF16)]
+            functools.partial(main_body, lanes, width),
+            [shape((rows, rest_width + LANES), F32), shape((rows, rest_width + LANES), BF16)]
             + [shape((rows, 2 * cols), BF16)] * 2
             + [shape((rows, cols), BF16)] * 2,
+            2 * work,
+        )(*pre, *cot_list, *cot_other, first, second, third)
+        rest = outs[0] + along_core(outs[1]).astype(F32)
+        owned = call(
+            functools.partial(own_body, lanes, width),
+            [shape((rows, width), F32), shape((rows, width), BF16)],
             work,
-        )(*tok_list, *tok_other, *cot_list, *cot_other, first, second, third)
-        return outs, tok_list + tok_other, cot_list + cot_other
-
-    near, tok_a, cot_a = experts_on(tok_near, cot_near)
-    far, tok_b, cot_b = experts_on(tok_far, cot_far)
-    near_sum = near[0] + along_core(near[1]).astype(F32)
-    far_sum = far[0] + along_core(far[1]).astype(F32)
+        )(*outs[2:4], first, second)
+        owned = owned[0] + along_core(owned[1]).astype(F32)
+        return owned, rest, outs[2:4], outs[4:6], tok_list + tok_other, cot_list + cot_other
+
+    near_own, near_rest, near_grads, near_hidden, tok_a, cot_a = experts_on(tok_near, cot_near)
+    far_own, far_rest, far_grads, far_hidden, tok_b, cot_b = experts_on(tok_far, cot_far)
     early = 3 * width // (8 * LANES) * LANES
     if lanes == 2 and early > 0:
-        far_tail = far_sum[:, features:]
-        near_in = along_tp(near_sum[:, width + early : features].astype(BF16), 1)
-        lane_in = along_tp(far_sum[:, width + early : features].astype(BF16), 1)
-        side_out = jnp.concatenate([far_sum[:, width : width + early], far_tail], axis=1)
+        near_in = along_tp(near_rest[:, early:width].astype(BF16), 1)
+        lane_in = along_tp(far_rest[:, early:width].astype(BF16), 1)
+        side_out = jnp.concatenate([far_rest[:, :early], far_rest[:, width:]], axis=1)
         side_in = along_side(side_out.astype(BF16)).astype(F32)
-        own_in = along_side(far_sum[:, :early].astype(BF16))
-        last_in = along_side((far_sum[:, early:width] + lane_in.astype(F32)).astype(BF16))
-        near_out = jnp.concatenate(
-            [near_sum[:, width : width + early], near_sum[:, features:]], axis=1
-        )
+        own_in = along_side(far_own[:, :early].astype(BF16))
+        last_in = along_side((far_own[:, early:] + lane_in.astype(F32)).astype(BF16))
+        near_out = jnp.concatenate([near_rest[:, :early], near_rest[:, width:]], axis=1)
         next_out = near_out + side_in
         next_in = along_tp(next_out.astype(BF16), 1).astype(F32)
         tail = next_out[:, early:] + next_in[:, early:]
-        head = near_sum[:, :early] + own_in.astype(F32) + next_in[:, :early]
-        rest = near_sum[:, early:width] + near_in.astype(F32) + last_in.astype(F32)
+        head = near_own[:, :early] + own_in.astype(F32) + next_in[:, :early]
+        rest = near_own[:, early:] + near_in.astype(F32) + last_in.astype(F32)
         body = jnp.concatenate([head, rest], axis=1)
     else:
-        both = near_sum + along_side(far_sum.astype(BF16)).astype(F32)
-        tail = both[:, features:]
-        body = both[:, :width]
+        body = near_own + along_side(far_own.astype(BF16)).astype(F32)
+        both = near_rest + along_side(far_rest.astype(BF16)).astype(F32)
+        tail = both[:, rest_width:]
         for j in range(1, lanes):
             piece = jnp.concatenate(
-                [both[:, j * width : (j + 1) * width], both[:, features:]], axis=1
+                [both[:, (j - 1) * width : j * width], both[:, rest_width:]], axis=1
             )
             piece = along_tp(piece.astype(BF16), lanes - j).astype(F32)
             body = body + piece[:, :width]
@@ -372,10 +411,10 @@
     held = tail[:, :EPG] + tail[:, EPG : 2 * EPG]
     held = jnp.pad(held, ((0, 0), (0, LANES - EPG)))
     result = jnp.concatenate([body, held], axis=1).astype(BF16)
-    sent = {k: along_groups(result[k * cap : (k + 1) * cap], k) for k in others}
+    sent = {k: along_groups(result[k * cap : (k + 1) * cap], k) for k in range(groups - 1, 0, -1)}
     returned = [result[:cap]] + [sent[k] for k in range(1, groups)]
-    grads = list(near[2:4]) + list(far[2:4])
-    scaled_hidden = list(near[4:6]) + list(far[4:6])
+    grads = list(near_grads) + list(far_grads)
+    scaled_hidden = list(near_hidden) + list(far_hidden)
     up_work = 2 * 2 * 4 * rows * features * cols
     first_grad, second_grad = call(
         functools.partial(up_body, lanes, width), [shape((features, cols), F32)] * 2, up_work

time: 96.9 us -> 102 us (1.053)
  waiting for transfers between devices: 36.5 us -> 40.5 us
    ppermute x8 -> x10, waiting for transfers between devices: 5.08 us -> 13.7 us  [along_side(): return lax.ppermute(a, 'ep', [(e, e ^ 2) for e in range(experts)])]
    ppermute x8 -> x10, starting transfers between devices: 6.77 us -> 13.2 us  [along_tp(): return lax.ppermute(a, 'tp', [(r, (r + j) % lanes) for r in range(lanes)])]
    ppermute x9 -> x8, starting transfers between devices: 17.3 us -> 13.7 us  [along_groups(): return lax.ppermute(a, 'ep', [(e, e ^ k * EPG) for e in range(experts)])]
    ppermute x8 -> x10, waiting for transfers between devices: 20.3 us -> 17.7 us  [along_tp(): return lax.ppermute(a, 'tp', [(r, (r + j) % lanes) for r in range(lanes)])]
    ppermute x10 -> x12, waiting for transfers between devices: 2.01 us -> 0.03 us  [along_core(): return lax.ppermute(a, 'ep', [(e, e ^ 1) for e in range(experts)])]
    ppermute x1 -> x0, starting transfers between devices: 1.49 us -> none  [along_both(): return lax.ppermute(a, ('ep', 'tp'), pairs)]
    ppermute x8 -> x10, starting transfers between devices: 12.1 us -> 10.8 us  [along_side(): return lax.ppermute(a, 'ep', [(e, e ^ 2) for e in range(experts)])]
    pallas_call x10 -> x14, Pallas kernels: 17.6 us -> 18.2 us  [run(): pl.pallas_call(body, out_shape=outs, in_specs=[pl.BlockSpec(memory_space=...]
  transfers between devices with their start and end apart: 36 -> 40, of which waited for: 14 -> 15; matrix products, arithmetic and copies ran while one was open for 1% -> 1% of each run, Pallas kernels for 15% -> 15%
where the time goes in v2:
time: 102 us
  waiting for transfers between devices  40.5 us (40%)
  starting transfers between devices  40.2 us (39%)
  Pallas kernels  18.2 us (18%)
  between operations  1.16 us (1%)
  other arithmetic  1.12 us (1%)
    pallas_call x14, Pallas kernels, run(): pl.pallas_call(body, out_shape=outs, in_specs=[pl.BlockSpec(memory_space=...  18.2 us
    ppermute x10, waiting for transfers between devices, along_tp(): return lax.ppermute(a, 'tp', [(r, (r + j) % lanes) for r in range(lanes)])  17.7 us
    ppermute x8, starting transfers between devices, along_groups(): return lax.ppermute(a, 'ep', [(e, e ^ k * EPG) for e in range(experts)])  13.7 us
    ppermute x10, waiting for transfers between devices, along_side(): return lax.ppermute(a, 'ep', [(e, e ^ 2) for e in range(experts)])  13.7 us
    ppermute x10, starting transfers between devices, along_tp(): return lax.ppermute(a, 'tp', [(r, (r + j) % lanes) for r in range(lanes)])  13.2 us
    ppermute x10, starting transfers between devices, along_side(): return lax.ppermute(a, 'ep', [(e, e ^ 2) for e in range(experts)])  10.8 us
    ppermute x8, waiting for transfers between devices, along_groups(): return lax.ppermute(a, 'ep', [(e, e ^ k * EPG) for e in range(experts)])  9.09 us
    ppermute x12, starting transfers between devices, along_core(): return lax.ppermute(a, 'ep', [(e, e ^ 1) for e in range(experts)])  2.51 us
  transfers between devices with their start and end apart: 40, of which 15 were waited for; matrix products, arithmetic and copies ran while one was open for 1% of the time, Pallas kernels for 15%

profile of v2, /device:TPU:0, one launch (start us, length us, event | category | flops | bytes accessed | tf_op | source)
XLA Modules:
  0.0 101.7 jit_solution(13002405918009300393)
XLA Ops:
  0.6 1.7 %shard_map.136 = (bf16[48,2176]{1,0:T(8,128)(2,1)S(1)}, bf16[48,2176]{1,0:T(8,128)(2,1)S(1)}, bf16[48,1024]{1,0:T(8,128)(2,1)S(1)}, bf16[48,1024]{1,0:T(8,128)(2...) custom-call(s32[1,128]{1,0:T(1,128)} %bitcast.26, s32[2,128]{1,0:T(2,128)} %bitcast.31, ...), custom_call_target="tpu_custom_call" | custom-call | tf_op jit(solution)/shard_map/pallas_call | solution.py:27
  2.3 4.1 %collective-permute-start.1 = (bf16[48,1024]{1,0:T(8,128)(2,1)S(1)}, bf16[48,1024]{1,0:T(8,128)(2,1)S(1)}, u32[]{:S(2)}, u32[]{:S(2)}) collective-permute-start(bf16[48,1024]{1,0:T(8,128)(2,1)S(1)} %get-tuple-element.39), channel_id=1, source_target_pairs={{0,16},{2,18},{4,20},{6,22},{8,24},{10,26},{12,28},{14,30},{16,0},... | collective-permute-start | bytes 294920 | tf_op jit(solution)/shard_map/ppermute | solution.py:265
  6.5 1.3 %collective-permute-start.2 = (bf16[48,1024]{1,0:T(8,128)(2,1)S(1)}, bf16[48,1024]{1,0:T(8,128)(2,1)S(1)}, u32[]{:S(2)}, u32[]{:S(2)}) collective-permute-start(bf16[48,1024]{1,0:T(8,128)(2,1)S(1)} %get-tuple-element.40), channel_id=1, source_target_pairs={{0,24},{2,26},{4,28},{6,30},{8,16},{10,18},{12,20},{14,22},{16,8},... | collective-permute-start | bytes 294920 | tf_op jit(solution)/shard_map/ppermute | solution.py:265
  7.8 1.7 %collective-permute-start.8 = (bf16[48,1152]{1,0:T(8,128)(2,1)S(1)}, bf16[48,1152]{1,0:T(8,128)(2,1)S(1)}, u32[]{:S(2)}, u32[]{:S(2)}) collective-permute-start(bf16[48,1152]{1,0:T(8,128)(2,1)S(1)} %get-tuple-element.43), channel_id=1, source_target_pairs={{0,16},{2,18},{4,20},{6,22},{8,24},{10,26},{12,28},{14,30},{16,0},... | collective-permute-start | bytes 331784 | tf_op jit(solution)/shard_map/ppermute | solution.py:265
  9.5 0.9 collective-permute-start.9
  10.4 1.5 %collective-permute-start.14 = (bf16[48,2176]{1,0:T(8,128)(2,1)S(1)}, bf16[48,2176]{1,0:T(8,128)(2,1)S(1)}, u32[]{:S(2)}, u32[]{:S(2)}) collective-permute-start(bf16[48,2176]{1,0:T(8,128)(2,1)S(1)} %get-tuple-element.37), channel_id=1, source_target_pairs={{0,4},{2,6},{4,0},{6,2},{8,12},{10,14},{12,8},{14,10},{16,20},{18,... | collective-permute-start | bytes 626696 | tf_op jit(solution)/shard_map/ppermute | solution.py:268
  11.9 7.1 %collective-permute-done.1 = bf16[48,1024]{1,0:T(8,128)(2,1)S(1)} collective-permute-done((bf16[48,1024]{1,0:T(8,128)(2,1)S(1)}, bf16[48,1024]{1,0:T(8,128)(2,1)S(1)}, u32[]{:S(2)}, u32[]{:S(2)}) %collective-permute-start.1) | collective-permute-done | bytes 98336 | tf_op jit(solution)/shard_map/ppermute | solution.py:265
  19.1 1.7 %collective-permute-start.3 = (bf16[48,2048]{1,0:T(8,128)(2,1)S(1)}, bf16[48,2048]{1,0:T(8,128)(2,1)S(1)}, u32[]{:S(2)}, u32[]{:S(2)}) collective-permute-start(bf16[48,2048]{1,0:T(8,128)(2,1)S(1)} %slice.107), channel_id=1, source_target_pairs={{0,1},{1,0},{2,3},{3,2},{4,5},{5,4},{6,7},{7,6},{8,9},{9,8},{10,11... | collective-permute-start | bytes 589832 | tf_op jit(solution)/shard_map/ppermute | solution.py:274
  20.8 0.9 collective-permute-start
  21.7 1.8 %collective-permute-done.8 = bf16[48,1152]{1,0:T(8,128)(2,1)S(1)} collective-permute-done((bf16[48,1152]{1,0:T(8,128)(2,1)S(1)}, bf16[48,1152]{1,0:T(8,128)(2,1)S(1)}, u32[]{:S(2)}, u32[]{:S(2)}) %collective-permute-start.8) | collective-permute-done | bytes 110624 | tf_op jit(solution)/shard_map/ppermute | solution.py:265
  23.5 1.7 %collective-permute-start.16 = (bf16[96,1024]{1,0:T(8,128)(2,1)S(1)}, bf16[96,1024]{1,0:T(8,128)(2,1)S(1)}, u32[]{:S(2)}, u32[]{:S(2)}) collective-permute-start(bf16[96,1024]{1,0:T(8,128)(2,1)S(1)} %constant_dynamic-update-slice_fusion.4), channel_id=1, source_target_pairs={{0,4},{2,6},{4,0},{6,2},{8,12},{10,14},{12,8},{14,10},{16,20},{18,... | collective-permute-start | bytes 589832 | tf_op jit(solution)/shard_map/ppermute | solution.py:268
  25.2 1.6 %collective-permute-start.5 = (bf16[96,1024]{1,0:T(8,128)(2,1)S(1)}, bf16[96,1024]{1,0:T(8,128)(2,1)S(1)}, u32[]{:S(2)}, u32[]{:S(2)}) collective-permute-start(bf16[96,1024]{1,0:T(8,128)(2,1)S(1)} %constant_dynamic-update-slice_fusion.4), channel_id=1, source_target_pairs={{0,1},{1,0},{2,3},{3,2},{4,5},{5,4},{6,7},{7,6},{8,9},{9,8},{10,11... | collective-permute-start | bytes 589832 | tf_op jit(solution)/shard_map/ppermute | solution.py:274
  26.9 0.6 collective-permute-start.10
  27.5 1.3 %collective-permute-start.22 = (bf16[96,1152]{1,0:T(8,128)(2,1)S(1)}, bf16[96,1152]{1,0:T(8,128)(2,1)S(1)}, u32[]{:S(2)}, u32[]{:S(2)}) collective-permute-start(bf16[96,1152]{1,0:T(8,128)(2,1)S(1)} %pad_maximum_fusion.6), channel_id=1, source_target_pairs={{0,4},{2,6},{4,0},{6,2},{8,12},{10,14},{12,8},{14,10},{16,20},{18,... | collective-permute-start | bytes 663560 | tf_op jit(solution)/shard_map/ppermute | solution.py:268
  28.9 1.6 %collective-permute-start.4 = (bf16[48,2048]{1,0:T(8,128)(2,1)S(1)}, bf16[48,2048]{1,0:T(8,128)(2,1)S(1)}, u32[]{:S(2)}, u32[]{:S(2)}) collective-permute-start(bf16[48,2048]{1,0:T(8,128)(2,1)S(1)} %slice.140), channel_id=1, source_target_pairs={{0,1},{1,0},{2,3},{3,2},{4,5},{5,4},{6,7},{7,6},{8,9},{9,8},{10,11... | collective-permute-start | bytes 589832 | tf_op jit(solution)/shard_map/ppermute | solution.py:274
  30.7 2.4 %collective-permute-done.5 = bf16[96,1024]{1,0:T(8,128)(2,1)S(1)} collective-permute-done((bf16[96,1024]{1,0:T(8,128)(2,1)S(1)}, bf16[96,1024]{1,0:T(8,128)(2,1)S(1)}, u32[]{:S(2)}, u32[]{:S(2)}) %collective-permute-start.5) | collective-permute-done | bytes 196640 | tf_op jit(solution)/shard_map/ppermute | solution.py:274
  33.1 3.2 %collective-permute-done.10 = bf16[96,1024]{1,0:T(8,128)(2,1)S(1)} collective-permute-done((bf16[96,1024]{1,0:T(8,128)(2,1)S(1)}, bf16[96,1024]{1,0:T(8,128)(2,1)S(1)}, u32[]{:S(2)}, u32[]{:S(2)}) %collective-permute-start.10) | collective-permute-done | bytes 196640 | tf_op jit(solution)/shard_map/ppermute | solution.py:274
  36.3 0.7 collective-permute-start.15
  37.0 1.6 %collective-permute-start.18 = (bf16[96,512]{1,0:T(8,128)(2,1)S(1)}, bf16[96,512]{1,0:T(8,128)(2,1)S(1)}, u32[]{:S(2)}, u32[]{:S(2)}) collective-permute-start(bf16[96,512]{1,0:T(8,128)(2,1)S(1)} %slice.148), channel_id=1, source_target_pairs={{0,1},{1,0},{2,3},{3,2},{4,5},{5,4},{6,7},{7,6},{8,9},{9,8},{10,11... | collective-permute-start | bytes 294920 | tf_op jit(solution)/shard_map/ppermute | solution.py:274
  38.5 0.9 collective-permute-done.4
  39.4 0.6 collective-permute-start.19
  40.1 2.8 %collective-permute-done.15 = bf16[48,2176]{1,0:T(8,128)(2,1)S(1)} collective-permute-done((bf16[48,2176]{1,0:T(8,128)(2,1)S(1)}, bf16[48,2176]{1,0:T(8,128)(2,1)S(1)}, u32[]{:S(2)}, u32[]{:S(2)}) %collective-permute-start.15) | collective-permute-done | bytes 208928 | tf_op jit(solution)/shard_map/ppermute | solution.py:268
  42.9 0.9 collective-permute-start.25
  43.9 1.5 %collective-permute-start.24 = (bf16[96,512]{1,0:T(8,128)(2,1)S(1)}, bf16[96,512]{1,0:T(8,128)(2,1)S(1)}, u32[]{:S(2)}, u32[]{:S(2)}) collective-permute-start(bf16[96,512]{1,0:T(8,128)(2,1)S(1)} %slice.151), channel_id=1, source_target_pairs={{0,1},{1,0},{2,3},{3,2},{4,5},{5,4},{6,7},{7,6},{8,9},{9,8},{10,11... | collective-permute-start | bytes 294920 | tf_op jit(solution)/shard_map/ppermute | solution.py:274
  45.4 1.2 %collective-permute-start.23 = (bf16[96,1024]{1,0:T(8,128)(2,1)S(1)}, bf16[96,1024]{1,0:T(8,128)(2,1)S(1)}, u32[]{:S(2)}, u32[]{:S(2)}) collective-permute-start(bf16[96,1024]{1,0:T(8,128)(2,1)S(1)} %get-tuple-element.75), channel_id=1, source_target_pairs={{0,4},{2,6},{4,0},{6,2},{8,12},{10,14},{12,8},{14,10},{16,20},{18,... | collective-permute-start | bytes 589832 | tf_op jit(solution)/shard_map/ppermute | solution.py:268
  46.6 0.9 collective-permute-done.25
  47.6 0.9 collective-permute-done.24
  48.6 2.5 %collective-permute-done.23 = bf16[96,1024]{1,0:T(8,128)(2,1)S(1)} collective-permute-done((bf16[96,1024]{1,0:T(8,128)(2,1)S(1)}, bf16[96,1024]{1,0:T(8,128)(2,1)S(1)}, u32[]{:S(2)}, u32[]{:S(2)}) %collective-permute-start.23) | collective-permute-done | bytes 196640 | tf_op jit(solution)/shard_map/ppermute | solution.py:268
  51.1 1.2 %collective-permute-start.17 = (bf16[96,1024]{1,0:T(8,128)(2,1)S(1)}, bf16[96,1024]{1,0:T(8,128)(2,1)S(1)}, u32[]{:S(2)}, u32[]{:S(2)}) collective-permute-start(bf16[96,1024]{1,0:T(8,128)(2,1)S(1)} %slice.147), channel_id=1, source_target_pairs={{0,1},{1,0},{2,3},{3,2},{4,5},{5,4},{6,7},{7,6},{8,9},{9,8},{10,11... | collective-permute-start | bytes 589832 | tf_op jit(solution)/shard_map/ppermute | solution.py:274
  52.4 4.4 %collective-permute-done.17 = bf16[96,1024]{1,0:T(8,128)(2,1)S(1)} collective-permute-done((bf16[96,1024]{1,0:T(8,128)(2,1)S(1)}, bf16[96,1024]{1,0:T(8,128)(2,1)S(1)}, u32[]{:S(2)}, u32[]{:S(2)}) %collective-permute-start.17) | collective-permute-done | bytes 196640 | tf_op jit(solution)/shard_map/ppermute | solution.py:274
  56.8 0.6 collective-permute-start.26
  57.5 1.0 shard_map.137
  58.5 0.5 collective-permute-start.27
  59.0 2.0 %shard_map.138 = (f32[192,1152]{1,0:T(8,128)S(1)}, bf16[192,1152]{1,0:T(8,128)(2,1)S(1)}, bf16[192,512]{1,0:T(8,128)(2,1)S(1)}, bf16[192,512]{1,0:T(8,128)(2,1)S...) custom-call(f32[192,512]{1,0:T(8,128)S(1)} %get-tuple-element.41.refs_0_, ...), custom_call_target="tpu_custom_call" | custom-call | flops 805306368 | tf_op jit(solution)/shard_map/pallas_call | solution.py:27
  60.9 0.8 shard_map.139
  61.8 0.2 collective-permute-start.13
  61.9 0.1 shard_map.146.refs_7_
  62.1 0.1 shard_map.145.refs_6_
  62.2 0.1 shard_map.144.refs_5_
  62.4 0.1 shard_map.143.refs_4_
  62.5 0.5 collective-permute-start.30
  63.0 1.0 shard_map.140
  64.1 2.0 %shard_map.141 = (f32[192,1152]{1,0:T(8,128)S(1)}, bf16[192,1152]{1,0:T(8,128)(2,1)S(1)}, bf16[192,512]{1,0:T(8,128)(2,1)S(1)}, bf16[192,512]{1,0:T(8,128)(2,1)S...) custom-call(f32[192,512]{1,0:T(8,128)S(1)} %get-tuple-element.49.refs_0_, ...), custom_call_target="tpu_custom_call" | custom-call | flops 805306368 | tf_op jit(solution)/shard_map/pallas_call | solution.py:27
  66.0 0.2 collective-permute-start.31
  66.2 0.8 shard_map.142
  67.0 0.5 collective-permute-start.28
  67.5 0.1 convert_add_fusion.2
  67.8 1.3 %collective-permute-start.34 = (bf16[192,640]{1,0:T(8,128)(2,1)S(1)}, bf16[192,640]{1,0:T(8,128)(2,1)S(1)}, u32[]{:S(2)}, u32[]{:S(2)}) collective-permute-start(bf16[192,640]{1,0:T(8,128)(2,1)S(1)} %slice.193), channel_id=1, source_target_pairs={{0,1},{1,0},{2,3},{3,2},{4,5},{5,4},{6,7},{7,6},{8,9},{9,8},{10,11... | collective-permute-start | bytes 737288 | tf_op jit(solution)/shard_map/ppermute | solution.py:274
  69.2 0.8 collective-permute-start.32
  70.0 1.3 %collective-permute-start.35 = (bf16[192,640]{1,0:T(8,128)(2,1)S(1)}, bf16[192,640]{1,0:T(8,128)(2,1)S(1)}, u32[]{:S(2)}, u32[]{:S(2)}) collective-permute-start(bf16[192,640]{1,0:T(8,128)(2,1)S(1)} %slice.162), channel_id=1, source_target_pairs={{0,1},{1,0},{2,3},{3,2},{4,5},{5,4},{6,7},{7,6},{8,9},{9,8},{10,11... | collective-permute-start | bytes 737288 | tf_op jit(solution)/shard_map/ppermute | solution.py:274
  71.4 0.9 collective-permute-start.29
  72.3 4.7 %collective-permute-done.32 = bf16[192,512]{1,0:T(8,128)(2,1)S(1)} collective-permute-done((bf16[192,512]{1,0:T(8,128)(2,1)S(1)}, bf16[192,512]{1,0:T(8,128)(2,1)S(1)}, u32[]{:S(2)}, u32[]{:S(2)}) %collective-permute-start.32) | collective-permute-done | bytes 196640 | tf_op jit(solution)/shard_map/ppermute | solution.py:268
  77.1 0.9 collective-permute-start.33
  78.0 3.9 %collective-permute-done.35 = bf16[192,640]{1,0:T(8,128)(2,1)S(1)} collective-permute-done((bf16[192,640]{1,0:T(8,128)(2,1)S(1)}, bf16[192,640]{1,0:T(8,128)(2,1)S(1)}, u32[]{:S(2)}, u32[]{:S(2)}) %collective-permute-start.35) | collective-permute-done | bytes 245792 | tf_op jit(solution)/shard_map/ppermute | solution.py:274
  82.0 1.3 %collective-permute-start.36 = (bf16[192,640]{1,0:T(8,128)(2,1)S(1)}, bf16[192,640]{1,0:T(8,128)(2,1)S(1)}, u32[]{:S(2)}, u32[]{:S(2)}) collective-permute-start(bf16[192,640]{1,0:T(8,128)(2,1)S(1)} %fusion.1), channel_id=1, source_target_pairs={{0,4},{2,6},{4,0},{6,2},{8,12},{10,14},{12,8},{14,10},{16,20},{18,... | collective-permute-start | bytes 737288 | tf_op jit(solution)/shard_map/ppermute | solution.py:268
  83.2 2.0 %collective-permute-done.33 = bf16[192,512]{1,0:T(8,128)(2,1)S(1)} collective-permute-done((bf16[192,512]{1,0:T(8,128)(2,1)S(1)}, bf16[192,512]{1,0:T(8,128)(2,1)S(1)}, u32[]{:S(2)}, u32[]{:S(2)}) %collective-permute-start.33) | collective-permute-done | bytes 196640 | tf_op jit(solution)/shard_map/ppermute | solution.py:274
  85.3 0.1 fusion.6
  85.5 2.7 %collective-permute-done.36 = bf16[192,640]{1,0:T(8,128)(2,1)S(1)} collective-permute-done((bf16[192,640]{1,0:T(8,128)(2,1)S(1)}, bf16[192,640]{1,0:T(8,128)(2,1)S(1)}, u32[]{:S(2)}, u32[]{:S(2)}) %collective-permute-start.36) | collective-permute-done | bytes 245792 | tf_op jit(solution)/shard_map/ppermute | solution.py:268
  88.4 4.1 %collective-permute-start.39 = (bf16[48,1152]{1,0:T(8,128)(2,1)S(1)}, bf16[48,1152]{1,0:T(8,128)(2,1)S(1)}, u32[]{:S(2)}, u32[]{:S(2)}) collective-permute-start(bf16[48,1152]{1,0:T(8,128)(2,1)S(1)} %get-tuple-element.70), channel_id=1, source_target_pairs={{0,24},{2,26},{4,28},{6,30},{8,16},{10,18},{12,20},{14,22},{16,8},... | collective-permute-start | bytes 331784 | tf_op jit(solution)/shard_map/ppermute | solution.py:265
  92.6 0.6 collective-permute-start.37
  93.1 4.4 %shard_map.148 = (f32[2048,256]{1,0:T(8,128)}, f32[2048,256]{1,0:T(8,128)}) custom-call(bf16[192,1024]{1,0:T(8,128)(2,1)S(1)} %pad_maximum_fusion.2.refs_0_, bf16[192,1024]{1,0:T(8,128)(2,1)S(1)} %pad_maximum_fusion.3.refs_1_, bf16[192,1024]{1,0:T(8,128)(2,1)S(1)} %collective-permute-done.6.refs_2_, bf16[192,1024]{1,0:T(8,128)(2,1)S(1)} %collective-permute-done.7.refs_3_, ...), custom_call_target="tpu_custom_call" | custom-call | flops 1610612736 | tf_op jit(solution)/shard_map/pallas_call | solution.py:27
  97.6 2.6 %shard_map.149 = f32[256,2048]{1,0:T(8,128)} custom-call(bf16[192,1152]{1,0:T(8,128)(2,1)S(1)} %pad_maximum_fusion.refs_2_.refs_0_, bf16[192,1024]{1,0:T(8,128)(2,1)S(1)} %pad_maximum_fusion.4.refs_3_.refs_1_, bf16[192,1152]{1,0:T(8,128)(2,1)S(1)} %collective-permute-done.11.refs_4_.refs_2_, bf16[192,1024]{1,0:T(8,128)(2,1)S(1)} %collective-permute-done.12.refs_5_.refs_3_, ...), custom_call_target="tpu_custom_call" | custom-call | flops 805306368 | tf_op jit(solution)/shard_map/pallas_call | solution.py:27
  100.2 0.1 collective-permute-done.38.refs_2_
  100.4 1.3 %shard_map.147 = (f32[128,1024]{1,0:T(8,128)}, f32[1,128]{1,0:T(1,128)}, f32[2,128]{1,0:T(2,128)}) custom-call(bf16[48,1152]{1,0:T(8,128)(2,1)S(1)} %get-tuple-element.73.refs_0_, bf16[48,1152]{1,0:T(8,128)(2,1)S(1)} %collective-permute-done.37.refs_1_, bf16[48,1152]{1,0:T(8,128)(2,1)S(1)} %collective-permute-done.38.refs_2_, ...), custom_call_target="tpu_custom_call" | custom-call | tf_op jit(solution)/shard_map/pallas_call | solution.py:27
  (100 shorter events, 1.7 us)
Async XLA Ops:
  2.3 16.7 %collective-permute-start.1 = (bf16[48,1024]{1,0:T(8,128)(2,1)S(1)}, bf16[48,1024]{1,0:T(8,128)(2,1)S(1)}, u32[]{:S(2)}, u32[]{:S(2)}) collective-permute-start(bf16[48,1024]{1,0:T(8,128)(2,1)S(1)} %get-tuple-element.39), channel_id=1, source_target_pairs={{0,16},{2,18},{4,20},{6,22},{8,24},{10,26},{12,28},{14,30},{16,0},... | collective-permute-start | bytes 294920 | tf_op jit(solution)/shard_map/ppermute | solution.py:265
  6.5 14.3 %collective-permute-start.2 = (bf16[48,1024]{1,0:T(8,128)(2,1)S(1)}, bf16[48,1024]{1,0:T(8,128)(2,1)S(1)}, u32[]{:S(2)}, u32[]{:S(2)}) collective-permute-start(bf16[48,1024]{1,0:T(8,128)(2,1)S(1)} %get-tuple-element.40), channel_id=1, source_target_pairs={{0,24},{2,26},{4,28},{6,30},{8,16},{10,18},{12,20},{14,22},{16,8},... | collective-permute-start | bytes 294920 | tf_op jit(solution)/shard_map/ppermute | solution.py:265
  7.8 15.7 %collective-permute-start.8 = (bf16[48,1152]{1,0:T(8,128)(2,1)S(1)}, bf16[48,1152]{1,0:T(8,128)(2,1)S(1)}, u32[]{:S(2)}, u32[]{:S(2)}) collective-permute-start(bf16[48,1152]{1,0:T(8,128)(2,1)S(1)} %get-tuple-element.43), channel_id=1, source_target_pairs={{0,16},{2,18},{4,20},{6,22},{8,24},{10,26},{12,28},{14,30},{16,0},... | collective-permute-start | bytes 331784 | tf_op jit(solution)/shard_map/ppermute | solution.py:265
  9.5 15.7 %collective-permute-start.9 = (bf16[48,1152]{1,0:T(8,128)(2,1)S(1)}, bf16[48,1152]{1,0:T(8,128)(2,1)S(1)}, u32[]{:S(2)}, u32[]{:S(2)}) collective-permute-start(bf16[48,1152]{1,0:T(8,128)(2,1)S(1)} %get-tuple-element.44), channel_id=1, source_target_pairs={{0,24},{2,26},{4,28},{6,30},{8,16},{10,18},{12,20},{14,22},{16,8},... | collective-permute-start | bytes 331784 | tf_op jit(solution)/shard_map/ppermute | solution.py:265
  10.4 18.5 %collective-permute-start.14 = (bf16[48,2176]{1,0:T(8,128)(2,1)S(1)}, bf16[48,2176]{1,0:T(8,128)(2,1)S(1)}, u32[]{:S(2)}, u32[]{:S(2)}) collective-permute-start(bf16[48,2176]{1,0:T(8,128)(2,1)S(1)} %get-tuple-element.37), channel_id=1, source_target_pairs={{0,4},{2,6},{4,0},{6,2},{8,12},{10,14},{12,8},{14,10},{16,20},{18,... | collective-permute-start | bytes 626696 | tf_op jit(solution)/shard_map/ppermute | solution.py:268
  19.1 7.8 %collective-permute-start.3 = (bf16[48,2048]{1,0:T(8,128)(2,1)S(1)}, bf16[48,2048]{1,0:T(8,128)(2,1)S(1)}, u32[]{:S(2)}, u32[]{:S(2)}) collective-permute-start(bf16[48,2048]{1,0:T(8,128)(2,1)S(1)} %slice.107), channel_id=1, source_target_pairs={{0,1},{1,0},{2,3},{3,2},{4,5},{5,4},{6,7},{7,6},{8,9},{9,8},{10,11... | collective-permute-start | bytes 589832 | tf_op jit(solution)/shard_map/ppermute | solution.py:274
  20.8 6.7 %collective-permute-start = (bf16[48,2176]{1,0:T(8,128)(2,1)S(1)}, bf16[48,2176]{1,0:T(8,128)(2,1)S(1)}, u32[]{:S(2)}, u32[]{:S(2)}) collective-permute-start(bf16[48,2176]{1,0:T(8,128)(2,1)S(1)} %get-tuple-element.38), channel_id=1, source_target_pairs={{0,8},{2,10},{4,12},{6,14},{8,0},{10,2},{12,4},{14,6},{16,24},{18,... | collective-permute-start | bytes 626696 | tf_op jit(solution)/shard_map/ppermute | solution.py:265
  23.5 7.0 %collective-permute-start.16 = (bf16[96,1024]{1,0:T(8,128)(2,1)S(1)}, bf16[96,1024]{1,0:T(8,128)(2,1)S(1)}, u32[]{:S(2)}, u32[]{:S(2)}) collective-permute-start(bf16[96,1024]{1,0:T(8,128)(2,1)S(1)} %constant_dynamic-update-slice_fusion.4), channel_id=1, source_target_pairs={{0,4},{2,6},{4,0},{6,2},{8,12},{10,14},{12,8},{14,10},{16,20},{18,... | collective-permute-start | bytes 589832 | tf_op jit(solution)/shard_map/ppermute | solution.py:268
  25.2 7.8 %collective-permute-start.5 = (bf16[96,1024]{1,0:T(8,128)(2,1)S(1)}, bf16[96,1024]{1,0:T(8,128)(2,1)S(1)}, u32[]{:S(2)}, u32[]{:S(2)}) collective-permute-start(bf16[96,1024]{1,0:T(8,128)(2,1)S(1)} %constant_dynamic-update-slice_fusion.4), channel_id=1, source_target_pairs={{0,1},{1,0},{2,3},{3,2},{4,5},{5,4},{6,7},{7,6},{8,9},{9,8},{10,11... | collective-permute-start | bytes 589832 | tf_op jit(solution)/shard_map/ppermute | solution.py:274
  26.9 9.4 %collective-permute-start.10 = (bf16[96,1024]{1,0:T(8,128)(2,1)S(1)}, bf16[96,1024]{1,0:T(8,128)(2,1)S(1)}, u32[]{:S(2)}, u32[]{:S(2)}) collective-permute-start(bf16[96,1024]{1,0:T(8,128)(2,1)S(1)} %pad_maximum_fusion.7), channel_id=1, source_target_pairs={{0,1},{1,0},{2,3},{3,2},{4,5},{5,4},{6,7},{7,6},{8,9},{9,8},{10,11... | collective-permute-start | bytes 589832 | tf_op jit(solution)/shard_map/ppermute | solution.py:274
  27.5 9.5 %collective-permute-start.22 = (bf16[96,1152]{1,0:T(8,128)(2,1)S(1)}, bf16[96,1152]{1,0:T(8,128)(2,1)S(1)}, u32[]{:S(2)}, u32[]{:S(2)}) collective-permute-start(bf16[96,1152]{1,0:T(8,128)(2,1)S(1)} %pad_maximum_fusion.6), channel_id=1, source_target_pairs={{0,4},{2,6},{4,0},{6,2},{8,12},{10,14},{12,8},{14,10},{16,20},{18,... | collective-permute-start | bytes 663560 | tf_op jit(solution)/shard_map/ppermute | solution.py:268
  28.9 10.5 %collective-permute-start.4 = (bf16[48,2048]{1,0:T(8,128)(2,1)S(1)}, bf16[48,2048]{1,0:T(8,128)(2,1)S(1)}, u32[]{:S(2)}, u32[]{:S(2)}) collective-permute-start(bf16[48,2048]{1,0:T(8,128)(2,1)S(1)} %slice.140), channel_id=1, source_target_pairs={{0,1},{1,0},{2,3},{3,2},{4,5},{5,4},{6,7},{7,6},{8,9},{9,8},{10,11... | collective-permute-start | bytes 589832 | tf_op jit(solution)/shard_map/ppermute | solution.py:274
  30.6 26.2 %collective-permute-start.6 = (bf16[192,1024]{1,0:T(8,128)(2,1)S(1)}, bf16[192,1024]{1,0:T(8,128)(2,1)S(1)}, u32[]{:S(2)}, u32[]{:S(2)}) collective-permute-start(bf16[192,1024]{1,0:T(8,128)(2,1)S(1)} %pad_maximum_fusion.2.refs_0_), channel_id=1, source_target_pairs={{0,2},{2,0},{4,6},{6,4},{8,10},{10,8},{12,14},{14,12},{16,18},{18,... | collective-permute-start | bytes 1179656 | tf_op jit(solution)/shard_map/ppermute | solution.py:271
  33.1 25.4 %collective-permute-start.11 = (bf16[192,1152]{1,0:T(8,128)(2,1)S(1)}, bf16[192,1152]{1,0:T(8,128)(2,1)S(1)}, u32[]{:S(2)}, u32[]{:S(2)}) collective-permute-start(bf16[192,1152]{1,0:T(8,128)(2,1)S(1)} %pad_maximum_fusion.refs_2_.refs_0_), channel_id=1, source_target_pairs={{0,2},{2,0},{4,6},{6,4},{8,10},{10,8},{12,14},{14,12},{16,18},{18,... | collective-permute-start | bytes 1327112 | tf_op jit(solution)/shard_map/ppermute | solution.py:271
  36.3 6.7 %collective-permute-start.15 = (bf16[48,2176]{1,0:T(8,128)(2,1)S(1)}, bf16[48,2176]{1,0:T(8,128)(2,1)S(1)}, u32[]{:S(2)}, u32[]{:S(2)}) collective-permute-start(bf16[48,2176]{1,0:T(8,128)(2,1)S(1)} %collective-permute-done), channel_id=1, source_target_pairs={{0,4},{2,6},{4,0},{6,2},{8,12},{10,14},{12,8},{14,10},{16,20},{18,... | collective-permute-start | bytes 626696 | tf_op jit(solution)/shard_map/ppermute | solution.py:268
  37.0 6.9 %collective-permute-start.18 = (bf16[96,512]{1,0:T(8,128)(2,1)S(1)}, bf16[96,512]{1,0:T(8,128)(2,1)S(1)}, u32[]{:S(2)}, u32[]{:S(2)}) collective-permute-start(bf16[96,512]{1,0:T(8,128)(2,1)S(1)} %slice.148), channel_id=1, source_target_pairs={{0,1},{1,0},{2,3},{3,2},{4,5},{5,4},{6,7},{7,6},{8,9},{9,8},{10,11... | collective-permute-start | bytes 294920 | tf_op jit(solution)/shard_map/ppermute | solution.py:274
  39.4 6.0 %collective-permute-start.19 = (bf16[96,512]{1,0:T(8,128)(2,1)S(1)}, bf16[96,512]{1,0:T(8,128)(2,1)S(1)}, u32[]{:S(2)}, u32[]{:S(2)}) collective-permute-start(bf16[96,512]{1,0:T(8,128)(2,1)S(1)} %slice.149), channel_id=1, source_target_pairs={{0,4},{2,6},{4,0},{6,2},{8,12},{10,14},{12,8},{14,10},{16,20},{18,... | collective-permute-start | bytes 294920 | tf_op jit(solution)/shard_map/ppermute | solution.py:268
  42.9 4.6 %collective-permute-start.25 = (bf16[96,512]{1,0:T(8,128)(2,1)S(1)}, bf16[96,512]{1,0:T(8,128)(2,1)S(1)}, u32[]{:S(2)}, u32[]{:S(2)}) collective-permute-start(bf16[96,512]{1,0:T(8,128)(2,1)S(1)} %slice.152), channel_id=1, source_target_pairs={{0,4},{2,6},{4,0},{6,2},{8,12},{10,14},{12,8},{14,10},{16,20},{18,... | collective-permute-start | bytes 294920 | tf_op jit(solution)/shard_map/ppermute | solution.py:268
  43.8 13.7 %copy-start = (bf16[1,2048,256]{2,1,0:T(8,128)(2,1)S(1)}, bf16[1,2048,256]{2,1,0:T(8,128)(2,1)}, u32[]{:S(2)}) copy-start(bf16[1,2048,256]{2,1,0:T(8,128)(2,1)} %param.15) | copy-start | bytes 3145732
  43.8 13.7 %copy-start.1 = (bf16[1,2048,256]{2,1,0:T(8,128)(2,1)S(1)}, bf16[1,2048,256]{2,1,0:T(8,128)(2,1)}, u32[]{:S(2)}) copy-start(bf16[1,2048,256]{2,1,0:T(8,128)(2,1)} %param.16) | copy-start | bytes 3145732
  43.9 4.7 %collective-permute-start.24 = (bf16[96,512]{1,0:T(8,128)(2,1)S(1)}, bf16[96,512]{1,0:T(8,128)(2,1)S(1)}, u32[]{:S(2)}, u32[]{:S(2)}) collective-permute-start(bf16[96,512]{1,0:T(8,128)(2,1)S(1)} %slice.151), channel_id=1, source_target_pairs={{0,1},{1,0},{2,3},{3,2},{4,5},{5,4},{6,7},{7,6},{8,9},{9,8},{10,11... | collective-permute-start | bytes 294920 | tf_op jit(solution)/shard_map/ppermute | solution.py:274
  45.4 5.7 %collective-permute-start.23 = (bf16[96,1024]{1,0:T(8,128)(2,1)S(1)}, bf16[96,1024]{1,0:T(8,128)(2,1)S(1)}, u32[]{:S(2)}, u32[]{:S(2)}) collective-permute-start(bf16[96,1024]{1,0:T(8,128)(2,1)S(1)} %get-tuple-element.75), channel_id=1, source_target_pairs={{0,4},{2,6},{4,0},{6,2},{8,12},{10,14},{12,8},{14,10},{16,20},{18,... | collective-permute-start | bytes 589832 | tf_op jit(solution)/shard_map/ppermute | solution.py:268
  47.5 9.8 %collective-permute-start.7 = (bf16[192,1024]{1,0:T(8,128)(2,1)S(1)}, bf16[192,1024]{1,0:T(8,128)(2,1)S(1)}, u32[]{:S(2)}, u32[]{:S(2)}) collective-permute-start(bf16[192,1024]{1,0:T(8,128)(2,1)S(1)} %pad_maximum_fusion.3.refs_1_), channel_id=1, source_target_pairs={{0,2},{2,0},{4,6},{6,4},{8,10},{10,8},{12,14},{14,12},{16,18},{18,... | collective-permute-start | bytes 1179656 | tf_op jit(solution)/shard_map/ppermute | solution.py:271
  48.6 10.4 %collective-permute-start.12 = (bf16[192,1024]{1,0:T(8,128)(2,1)S(1)}, bf16[192,1024]{1,0:T(8,128)(2,1)S(1)}, u32[]{:S(2)}, u32[]{:S(2)}) collective-permute-start(bf16[192,1024]{1,0:T(8,128)(2,1)S(1)} %pad_maximum_fusion.4.refs_3_.refs_1_), channel_id=1, source_target_pairs={{0,2},{2,0},{4,6},{6,4},{8,10},{10,8},{12,14},{14,12},{16,18},{18,... | collective-permute-start | bytes 1179656 | tf_op jit(solution)/shard_map/ppermute | solution.py:271
  51.1 5.7 %collective-permute-start.17 = (bf16[96,1024]{1,0:T(8,128)(2,1)S(1)}, bf16[96,1024]{1,0:T(8,128)(2,1)S(1)}, u32[]{:S(2)}, u32[]{:S(2)}) collective-permute-start(bf16[96,1024]{1,0:T(8,128)(2,1)S(1)} %slice.147), channel_id=1, source_target_pairs={{0,1},{1,0},{2,3},{3,2},{4,5},{5,4},{6,7},{7,6},{8,9},{9,8},{10,11... | collective-permute-start | bytes 589832 | tf_op jit(solution)/shard_map/ppermute | solution.py:274
  52.3 6.6 %copy-start.2 = (bf16[1,256,2048]{2,1,0:T(8,128)(2,1)S(1)}, bf16[1,256,2048]{2,1,0:T(8,128)(2,1)}, u32[]{:S(2)}) copy-start(bf16[1,256,2048]{2,1,0:T(8,128)(2,1)} %param.17) | copy-start | bytes 3145732
  56.8 5.8 %collective-permute-start.20 = (bf16[192,1024]{1,0:T(8,128)(2,1)S(1)}, bf16[192,1024]{1,0:T(8,128)(2,1)S(1)}, u32[]{:S(2)}, u32[]{:S(2)}) collective-permute-start(bf16[192,1024]{1,0:T(8,128)(2,1)S(1)} %pad_maximum_fusion.5.refs_0_.refs_4_), channel_id=1, source_target_pairs={{0,2},{2,0},{4,6},{6,4},{8,10},{10,8},{12,14},{14,12},{16,18},{18,... | collective-permute-start | bytes 1179656 | tf_op jit(solution)/shard_map/ppermute | solution.py:271
  56.8 7.2 %collective-permute-start.26 = (bf16[192,1152]{1,0:T(8,128)(2,1)S(1)}, bf16[192,1152]{1,0:T(8,128)(2,1)S(1)}, u32[]{:S(2)}, u32[]{:S(2)}) collective-permute-start(bf16[192,1152]{1,0:T(8,128)(2,1)S(1)} %pad_maximum_fusion.1.refs_2_.refs_4_), channel_id=1, source_target_pairs={{0,2},{2,0},{4,6},{6,4},{8,10},{10,8},{12,14},{14,12},{16,18},{18,... | collective-permute-start | bytes 1327112 | tf_op jit(solution)/shard_map/ppermute | solution.py:271
  57.4 5.6 %collective-permute-start.21 = (bf16[192,1024]{1,0:T(8,128)(2,1)S(1)}, bf16[192,1024]{1,0:T(8,128)(2,1)S(1)}, u32[]{:S(2)}, u32[]{:S(2)}) collective-permute-start(bf16[192,1024]{1,0:T(8,128)(2,1)S(1)} %maximum_maximum_fusion.refs_1_.refs_5_), channel_id=1, source_target_pairs={{0,2},{2,0},{4,6},{6,4},{8,10},{10,8},{12,14},{14,12},{16,18},{18,... | collective-permute-start | bytes 1179656 | tf_op jit(solution)/shard_map/ppermute | solution.py:271
  58.5 5.6 %collective-permute-start.27 = (bf16[192,1024]{1,0:T(8,128)(2,1)S(1)}, bf16[192,1024]{1,0:T(8,128)(2,1)S(1)}, u32[]{:S(2)}, u32[]{:S(2)}) collective-permute-start(bf16[192,1024]{1,0:T(8,128)(2,1)S(1)} %maximum_maximum_fusion.1.refs_3_.refs_5_), channel_id=1, source_target_pairs={{0,2},{2,0},{4,6},{6,4},{8,10},{10,8},{12,14},{14,12},{16,18},{18,... | collective-permute-start | bytes 1179656 | tf_op jit(solution)/shard_map/ppermute | solution.py:271
  60.9 1.0 copy-start.3
  61.8 5.7 %collective-permute-start.13 = (bf16[192,1024]{1,0:T(8,128)(2,1)S(1)}, bf16[192,1024]{1,0:T(8,128)(2,1)S(1)}, u32[]{:S(2)}, u32[]{:S(2)}) collective-permute-start(bf16[192,1024]{1,0:T(8,128)(2,1)S(1)} %get-tuple-element.48), channel_id=1, source_target_pairs={{0,2},{2,0},{4,6},{6,4},{8,10},{10,8},{12,14},{14,12},{16,18},{18,... | collective-permute-start | bytes 1179656 | tf_op jit(solution)/shard_map/ppermute | solution.py:271
  62.5 5.1 %collective-permute-start.30 = (bf16[192,1152]{1,0:T(8,128)(2,1)S(1)}, bf16[192,1152]{1,0:T(8,128)(2,1)S(1)}, u32[]{:S(2)}, u32[]{:S(2)}) collective-permute-start(bf16[192,1152]{1,0:T(8,128)(2,1)S(1)} %get-tuple-element.56), channel_id=1, source_target_pairs={{0,2},{2,0},{4,6},{6,4},{8,10},{10,8},{12,14},{14,12},{16,18},{18,... | collective-permute-start | bytes 1327112 | tf_op jit(solution)/shard_map/ppermute | solution.py:271
  66.0 3.0 %collective-permute-start.31 = (bf16[192,1152]{1,0:T(8,128)(2,1)S(1)}, bf16[192,1152]{1,0:T(8,128)(2,1)S(1)}, u32[]{:S(2)}, u32[]{:S(2)}) collective-permute-start(bf16[192,1152]{1,0:T(8,128)(2,1)S(1)} %get-tuple-element.58), channel_id=1, source_target_pairs={{0,2},{2,0},{4,6},{6,4},{8,10},{10,8},{12,14},{14,12},{16,18},{18,... | collective-permute-start | bytes 1327112 | tf_op jit(solution)/shard_map/ppermute | solution.py:271
  67.0 4.3 %collective-permute-start.28 = (bf16[192,1024]{1,0:T(8,128)(2,1)S(1)}, bf16[192,1024]{1,0:T(8,128)(2,1)S(1)}, u32[]{:S(2)}, u32[]{:S(2)}) collective-permute-start(bf16[192,1024]{1,0:T(8,128)(2,1)S(1)} %get-tuple-element.54), channel_id=1, source_target_pairs={{0,2},{2,0},{4,6},{6,4},{8,10},{10,8},{12,14},{14,12},{16,18},{18,... | collective-permute-start | bytes 1179656 | tf_op jit(solution)/shard_map/ppermute | solution.py:271
  67.7 1.5 %copy-start.7 = (f32[192,1152]{1,0:T(8,128)}, f32[192,1152]{1,0:T(8,128)S(1)}, u32[]{:S(2)}) copy-start(f32[192,1152]{1,0:T(8,128)S(1)} %convert_add_fusion) | copy-start | bytes 2654212
  67.8 17.8 %collective-permute-start.34 = (bf16[192,640]{1,0:T(8,128)(2,1)S(1)}, bf16[192,640]{1,0:T(8,128)(2,1)S(1)}, u32[]{:S(2)}, u32[]{:S(2)}) collective-permute-start(bf16[192,640]{1,0:T(8,128)(2,1)S(1)} %slice.193), channel_id=1, source_target_pairs={{0,1},{1,0},{2,3},{3,2},{4,5},{5,4},{6,7},{7,6},{8,9},{9,8},{10,11... | collective-permute-start | bytes 737288 | tf_op jit(solution)/shard_map/ppermute | solution.py:274
  69.2 7.8 %collective-permute-start.32 = (bf16[192,512]{1,0:T(8,128)(2,1)S(1)}, bf16[192,512]{1,0:T(8,128)(2,1)S(1)}, u32[]{:S(2)}, u32[]{:S(2)}) collective-permute-start(bf16[192,512]{1,0:T(8,128)(2,1)S(1)} %pad_maximum_fusion.8), channel_id=1, source_target_pairs={{0,4},{2,6},{4,0},{6,2},{8,12},{10,14},{12,8},{14,10},{16,20},{18,... | collective-permute-start | bytes 589832 | tf_op jit(solution)/shard_map/ppermute | solution.py:268
  70.0 7.0 %slice-start = ((f32[192,1152]{1,0:T(8,128)}), f32[192,128]{1,0:T(8,128)S(1)}, s32[]{:S(2)}) async-start(f32[192,1152]{1,0:T(8,128)} %copy-done.7), calls=%async_computation | async-start | bytes 196608 | tf_op jit(solution)/shard_map/slice | solution.py:393
  70.0 7.0 %slice-start.1 = ((f32[192,1152]{1,0:T(8,128)}), f32[192,384]{1,0:T(8,128)S(1)}, s32[]{:S(2)}) async-start(f32[192,1152]{1,0:T(8,128)} %copy-done.7), calls=%async_computation.1 | async-start | bytes 589824 | tf_op jit(solution)/shard_map/slice | solution.py:393
  70.0 11.9 %collective-permute-start.35 = (bf16[192,640]{1,0:T(8,128)(2,1)S(1)}, bf16[192,640]{1,0:T(8,128)(2,1)S(1)}, u32[]{:S(2)}, u32[]{:S(2)}) collective-permute-start(bf16[192,640]{1,0:T(8,128)(2,1)S(1)} %slice.162), channel_id=1, source_target_pairs={{0,1},{1,0},{2,3},{3,2},{4,5},{5,4},{6,7},{7,6},{8,9},{9,8},{10,11... | collective-permute-start | bytes 737288 | tf_op jit(solution)/shard_map/ppermute | solution.py:274
  71.4 14.0 %collective-permute-start.29 = (bf16[192,384]{1,0:T(8,128)(2,1)S(1)}, bf16[192,384]{1,0:T(8,128)(2,1)S(1)}, u32[]{:S(2)}, u32[]{:S(2)}) collective-permute-start(bf16[192,384]{1,0:T(8,128)(2,1)S(1)} %slice.194), channel_id=1, source_target_pairs={{0,4},{2,6},{4,0},{6,2},{8,12},{10,14},{12,8},{14,10},{16,20},{18,... | collective-permute-start | bytes 442376 | tf_op jit(solution)/shard_map/ppermute | solution.py:268
  77.1 8.1 %collective-permute-start.33 = (bf16[192,512]{1,0:T(8,128)(2,1)S(1)}, bf16[192,512]{1,0:T(8,128)(2,1)S(1)}, u32[]{:S(2)}, u32[]{:S(2)}) collective-permute-start(bf16[192,512]{1,0:T(8,128)(2,1)S(1)} %get-tuple-element.68), channel_id=1, source_target_pairs={{0,1},{1,0},{2,3},{3,2},{4,5},{5,4},{6,7},{7,6},{8,9},{9,8},{10,11... | collective-permute-start | bytes 589832 | tf_op jit(solution)/shard_map/ppermute | solution.py:274
  82.0 6.3 %collective-permute-start.36 = (bf16[192,640]{1,0:T(8,128)(2,1)S(1)}, bf16[192,640]{1,0:T(8,128)(2,1)S(1)}, u32[]{:S(2)}, u32[]{:S(2)}) collective-permute-start(bf16[192,640]{1,0:T(8,128)(2,1)S(1)} %fusion.1), channel_id=1, source_target_pairs={{0,4},{2,6},{4,0},{6,2},{8,12},{10,14},{12,8},{14,10},{16,20},{18,... | collective-permute-start | bytes 737288 | tf_op jit(solution)/shard_map/ppermute | solution.py:268
  88.4 11.8 %collective-permute-start.39 = (bf16[48,1152]{1,0:T(8,128)(2,1)S(1)}, bf16[48,1152]{1,0:T(8,128)(2,1)S(1)}, u32[]{:S(2)}, u32[]{:S(2)}) collective-permute-start(bf16[48,1152]{1,0:T(8,128)(2,1)S(1)} %get-tuple-element.70), channel_id=1, source_target_pairs={{0,24},{2,26},{4,28},{6,30},{8,16},{10,18},{12,20},{14,22},{16,8},... | collective-permute-start | bytes 331784 | tf_op jit(solution)/shard_map/ppermute | solution.py:265
  92.5 7.8 %collective-permute-start.38 = (bf16[48,1152]{1,0:T(8,128)(2,1)S(1)}, bf16[48,1152]{1,0:T(8,128)(2,1)S(1)}, u32[]{:S(2)}, u32[]{:S(2)}) collective-permute-start(bf16[48,1152]{1,0:T(8,128)(2,1)S(1)} %get-tuple-element.71), channel_id=1, source_target_pairs={{0,16},{2,18},{4,20},{6,22},{8,24},{10,26},{12,28},{14,30},{16,0},... | collective-permute-start | bytes 331784 | tf_op jit(solution)/shard_map/ppermute | solution.py:265
  92.6 7.8 %collective-permute-start.37 = (bf16[48,1152]{1,0:T(8,128)(2,1)S(1)}, bf16[48,1152]{1,0:T(8,128)(2,1)S(1)}, u32[]{:S(2)}, u32[]{:S(2)}) collective-permute-start(bf16[48,1152]{1,0:T(8,128)(2,1)S(1)} %get-tuple-element.72), channel_id=1, source_target_pairs={{0,8},{2,10},{4,12},{6,14},{8,0},{10,2},{12,4},{14,6},{16,24},{18,... | collective-permute-start | bytes 331784 | tf_op jit(solution)/shard_map/ppermute | solution.py:265
  97.6 2.8 %copy-start.4 = (s32[128,2]{0,1:T(2,128)S(1)}, s32[128,2]{0,1:T(2,128)}, u32[]{:S(2)}) copy-start(s32[128,2]{0,1:T(2,128)} %param.14) | copy-start | bytes 3076
  97.6 2.8 %copy-start.5 = (f32[128,2]{0,1:T(2,128)S(1)}, f32[128,2]{0,1:T(2,128)}, u32[]{:S(2)}) copy-start(f32[128,2]{0,1:T(2,128)} %param.12) | copy-start | bytes 3076
  97.6 2.8 %copy-start.6 = (f32[128]{0:T(128)S(1)}, f32[128]{0:T(128)}, u32[]{:S(2)}) copy-start(f32[128]{0:T(128)} %param.11) | copy-start | bytes 1540

commit v3 on v2

--- a/solution.py
+++ b/solution.py
@@ -123,75 +123,78 @@
     ]
 
 
+def stack(parts):
+    return jnp.concatenate(parts, axis=0)
+
+
 def pre_body(lanes, width, *refs):
     tok = [refs[c * lanes : (c + 1) * lanes] for c in range(2)]
-    gate_w, up_w = refs[2 * lanes : 2 * lanes + 2]
-    outs = refs[2 * lanes + 2 :]
+    gate_w, up_w, out = refs[2 * lanes :]
     cols = gate_w.shape[1]
     spans = spans_of(lanes, width)
-    for c in range(2):
-        gate = dot(tok[c][0][...], gate_w[spans[0], :], COLS_ROWS)
-        up = dot(tok[c][0][...], up_w[spans[0], :], COLS_ROWS)
-        for j in range(1, lanes):
-            gate = gate + dot(tok[c][j][...], gate_w[spans[j], :], COLS_ROWS)
-            up = up + dot(tok[c][j][...], up_w[spans[j], :], COLS_ROWS)
-        outs[c][:, :cols] = gate
-        outs[c][:, cols:] = up
+    gate = up = 0.0
+    for j in range(lanes):
+        part = stack([tok[c][j][...] for c in range(2)])
+        gate = gate + dot(part, gate_w[spans[j], :], COLS_ROWS)
+        up = up + dot(part, up_w[spans[j], :], COLS_ROWS)
+    out[:, :cols] = gate
+    out[:, cols:] = up
 
 
 def main_body(lanes, width, *refs):
-    pre = refs[:2]
-    cot = [refs[2 + c * lanes : 2 + (c + 1) * lanes] for c in range(2)]
-    gate_w, up_w, down_w = refs[2 + 2 * lanes : 5 + 2 * lanes]
-    outs = refs[5 + 2 * lanes :]
-    sums, grads, scaled_hidden = outs[:2], outs[2:4], outs[4:6]
-    rows = pre[0].shape[0]
+    pre = refs[0]
+    cot = [refs[1 + c * lanes : 1 + (c + 1) * lanes] for c in range(2)]
+    gate_w, up_w, down_w = refs[1 + 2 * lanes : 4 + 2 * lanes]
+    keep, send, grads, scaled_hidden = refs[4 + 2 * lanes :]
+    rows = keep.shape[0]
     cols = gate_w.shape[1]
     mine = lax.axis_index("ep") % EPG
     spans = spans_of(lanes, width)
-    lane = lax.broadcasted_iota(jnp.int32, (rows, LANES), 1)
-    for c in (1, 0):
-        pre_gate = pre[c][:, :cols]
-        pre_up = pre[c][:, cols:]
-        back = dot(cot[c][0][:, :width], down_w[:, spans[0]], ROWS_COLS)
-        for j in range(1, lanes):
-            back = back + dot(cot[c][j][...], down_w[:, spans[j]], ROWS_COLS)
-        gates = cot[c][0][:, width:].astype(F32)
-        gate = jnp.sum(jnp.where(lane == mine, gates, 0.0), axis=1, keepdims=True)
-        sigma = jax.nn.sigmoid(pre_gate)
-        swish = pre_gate * sigma
-        hidden = swish * pre_up
-        gate_part = jnp.sum(hidden * back, axis=1, keepdims=True)
-        scaled = gate * back
-        grad_gate = (scaled * pre_up * sigma * (1.0 + pre_gate * (1.0 - sigma))).astype(BF16)
-        grad_up = (scaled * swish).astype(BF16)
-        grads[c][:, :cols] = grad_gate
-        grads[c][:, cols:] = grad_up
-        scaled_hidden[c][...] = (gate * hidden).astype(BF16)
-        for j in range(1, lanes):
-            total = dot(grad_gate, gate_w[spans[j], :], ROWS_COLS)
-            total = total + dot(grad_up, up_w[spans[j], :], ROWS_COLS)
-            sums[c][:, (j - 1) * width : j * width] = total.astype(sums[c].dtype)
-        high = gate_part.astype(BF16).astype(F32)
-        low = gate_part - high
-        tail = jnp.where(lane == mine, high, jnp.where(lane == mine + EPG, low, 0.0))
-        sums[c][:, (lanes - 1) * width :] = tail.astype(sums[c].dtype)
-
-
-def own_body(lanes, width, *refs):
-    grads, (gate_w, up_w), sums = refs[:2], refs[2:4], refs[4:]
+    lane = lax.broadcasted_iota(jnp.int32, (2 * rows, LANES), 1)
+    pre_gate = pre[:, :cols]
+    pre_up = pre[:, cols:]
+    back = 0.0
+    for j in range(lanes):
+        part = stack([cot[c][j][:, :width] for c in range(2)])
+        back = back + dot(part, down_w[:, spans[j]], ROWS_COLS)
+    gates = stack([cot[c][0][:, width:] for c in range(2)]).astype(F32)
+    gate = jnp.sum(jnp.where(lane == mine, gates, 0.0), axis=1, keepdims=True)
+    sigma = jax.nn.sigmoid(pre_gate)
+    swish = pre_gate * sigma
+    hidden = swish * pre_up
+    gate_part = jnp.sum(hidden * back, axis=1, keepdims=True)
+    scaled = gate * back
+    grad_gate = (scaled * pre_up * sigma * (1.0 + pre_gate * (1.0 - sigma))).astype(BF16)
+    grad_up = (scaled * swish).astype(BF16)
+    grads[:, :cols] = grad_gate
+    grads[:, cols:] = grad_up
+    scaled_hidden[...] = (gate * hidden).astype(BF16)
+    for j in range(1, lanes):
+        total = dot(grad_gate, gate_w[spans[j], :], ROWS_COLS)
+        total = total + dot(grad_up, up_w[spans[j], :], ROWS_COLS)
+        keep[:, (j - 1) * width : j * width] = total[:rows]
+        send[:, (j - 1) * width : j * width] = total[rows:].astype(BF16)
+    high = gate_part.astype(BF16).astype(F32)
+    low = gate_part - high
+    tail = jnp.where(lane == mine, high, jnp.where(lane == mine + EPG, low, 0.0))
+    keep[:, (lanes - 1) * width :] = tail[:rows]
+    send[:, (lanes - 1) * width :] = tail[rows:].astype(BF16)
+
+
+def own_body(lanes, width, grads, gate_w, up_w, keep, send):
+    rows = keep.shape[0]
     cols = gate_w.shape[1]
     span = spans_of(lanes, width)[0]
-    for c in (1, 0):
-        total = dot(grads[c][:, :cols], gate_w[span, :], ROWS_COLS)
-        total = total + dot(grads[c][:, cols:], up_w[span, :], ROWS_COLS)
-        sums[c][...] = total.astype(sums[c].dtype)
-
-
-def up_body(lanes, width, *refs):
-    tok = [refs[b * lanes : (b + 1) * lanes] for b in range(4)]
-    grads = refs[4 * lanes : 4 * lanes + 4]
-    gate_out, up_out = refs[4 * lanes + 4 :]
+    total = dot(grads[:, :cols], gate_w[span, :], ROWS_COLS)
+    total = total + dot(grads[:, cols:], up_w[span, :], ROWS_COLS)
+    keep[...] = total[:rows]
+    send[...] = total[rows:].astype(BF16)
+
+
+def up_body(lanes, width, sets, *refs):
+    tok = [refs[b * lanes : (b + 1) * lanes] for b in range(2 * sets)]
+    grads = stack([ref[...] for ref in refs[2 * sets * lanes : 2 * sets * lanes + sets]])
+    gate_out, up_out = refs[2 * sets * lanes + sets :]
     cols = gate_out.shape[1]
     rank = lax.axis_index("tp")
     chunk = min(width, 512)
@@ -199,27 +202,24 @@
         base = ((rank + lanes - j) % lanes) * width
         for s in range(0, width, chunk):
             span = pl.ds(pl.multiple_of(base + s, chunk), chunk)
-            total = dot(tok[0][j][:, s : s + chunk], grads[0][...], ROWS_ROWS)
-            for b in range(1, 4):
-                total = total + dot(tok[b][j][:, s : s + chunk], grads[b][...], ROWS_ROWS)
+            part = stack([x[j][:, s : s + chunk] for x in tok])
+            total = dot(part, grads, ROWS_ROWS)
             gate_out[span, :] = total[:, :cols]
             up_out[span, :] = total[:, cols:]
 
 
-def down_body(lanes, width, *refs):
-    cot = [refs[b * lanes : (b + 1) * lanes] for b in range(4)]
-    scaled_hidden = refs[4 * lanes : 4 * lanes + 4]
-    down_out = refs[4 * lanes + 4]
+def down_body(lanes, width, sets, *refs):
+    cot = [refs[b * lanes : (b + 1) * lanes] for b in range(2 * sets)]
+    hidden = stack([ref[...] for ref in refs[2 * sets * lanes : 2 * sets * lanes + sets]])
+    down_out = refs[2 * sets * lanes + sets]
     rank = lax.axis_index("tp")
     chunk = min(width, 512)
     for j in range(lanes):
         base = ((rank + lanes - j) % lanes) * width
         for s in range(0, width, chunk):
             span = pl.ds(pl.multiple_of(base + s, chunk), chunk)
-            down = dot(scaled_hidden[0][...], cot[0][j][:, s : s + chunk], ROWS_ROWS)
-            for b in range(1, 4):
-                down = down + dot(scaled_hidden[b][...], cot[b][j][:, s : s + chunk], ROWS_ROWS)
-            down_out[:, span] = down
+            part = stack([x[j][:, s : s + chunk] for x in cot])
+            down_out[:, span] = dot(hidden, part, ROWS_ROWS)
 
 
 def final_body(groups, cap, *refs):
@@ -272,6 +272,19 @@
 
     def along_tp(a, j):
         return lax.ppermute(a, "tp", [(r, (r + j) % lanes) for r in range(lanes)])
+
+    core = lax.axis_index("ep") % 2
+
+    def along_diagonal(side, lane):
+        pieces = []
+        for j, a in enumerate(lane, 1):
+            pairs = []
+            for e in range(experts):
+                for r in range(lanes):
+                    there = (e ^ 2) * lanes + r if e % 2 else e * lanes + (r + j) % lanes
+                    pairs.append((e * lanes + r, there))
+            pieces.append(lax.ppermute(jnp.where(core == 0, side, a), ("ep", "tp"), pairs))
+        return pieces
 
     shape = jax.ShapeDtypeStruct
     choice_row = group_choice.reshape(1, count)
@@ -323,8 +336,7 @@
     own_side = join(own_side, next_side)
     own_lane = [join(a, b) for a, b in zip(own_lane, next_lane)]
     cot_sent = {k: along_groups(routed[groups - 2 + k], k) for k in range(2, groups)}
-    own_tok_both = [along_tp(own_side[:, :width], j) for j in range(1, lanes)]
-    own_cot_both = [along_side(a[:, width:]) for a in own_lane]
+    own_both = along_diagonal(own_side[:, : 2 * width], own_lane)
     tok = jnp.concatenate([tok_sent[k] for k in range(2, groups)], axis=0)
     cot = jnp.concatenate([cot_sent[k] for k in range(2, groups)], axis=0)
     cot_bare = jnp.concatenate([cot_sent[k][:, :width] for k in range(2, groups)], axis=0)
@@ -332,56 +344,47 @@
     tok_lane = [along_tp(tok, j) for j in range(1, lanes)]
     cot_side = along_side(cot)
     cot_lane = [along_tp(cot_bare, j) for j in range(1, lanes)]
-    cut = width // 2 if width % (2 * LANES) == 0 else width
-
-    def diagonal(side, lane):
-        parts_a = [along_tp(side[:, :cut], j) for j in range(1, lanes)]
-        if cut == width:
-            return parts_a
-        parts_b = [along_side(a[:, cut:width]) for a in lane]
-        return [jnp.concatenate([a, b], axis=1) for a, b in zip(parts_a, parts_b)]
-
-    tok_both = diagonal(tok_side, tok_lane)
-    cot_both = diagonal(cot_side, cot_lane)
+    tok_both = along_diagonal(tok_side, tok_lane)
+    cot_both = along_diagonal(cot_side[:, :width], cot_lane)
 
     tok_near = [join(own[:, :width], tok)]
     tok_near += [join(a[:, :width], b) for a, b in zip(own_lane, tok_lane)]
     cot_near = [join(own[:, width:], cot)]
     cot_near += [join(a[:, width:], b) for a, b in zip(own_lane, cot_lane)]
     tok_far = [join(own_side[:, :width], tok_side)]
-    tok_far += [join(a, b) for a, b in zip(own_tok_both, tok_both)]
+    tok_far += [join(a[:, :width], b) for a, b in zip(own_both, tok_both)]
     cot_far = [join(own_side[:, width:], cot_side)]
-    cot_far += [join(a, b) for a, b in zip(own_cot_both, cot_both)]
+    cot_far += [join(a[:, width:], b) for a, b in zip(own_both, cot_both)]
     first, second, third = w_gate[0], w_up[0], w_down[0]
-    work = 2 * 2 * rows * features * cols
     rest_width = features - width
 
     def experts_on(tok_list, cot_list):
+        size = tok_list[0].shape[0]
+        work = 2 * 2 * size * features * cols
         tok_other = [along_core(tok_list[0])]
         cot_other = [along_core(cot_list[0])]
         tok_other += [along_core(a) for a in tok_list[1:]]
         cot_other += [along_core(a) for a in cot_list[1:]]
         pre = call(
-            functools.partial(pre_body, lanes, width), [shape((rows, 2 * cols), F32)] * 2, 2 * work
+            functools.partial(pre_body, lanes, width), shape((2 * size, 2 * cols), F32), 2 * work
         )(*tok_list, *tok_other, first, second)
         outs = call(
             functools.partial(main_body, lanes, width),
-            [shape((rows, rest_width + LANES), F32), shape((rows, rest_width + LANES), BF16)]
-            + [shape((rows, 2 * cols), BF16)] * 2
-            + [shape((rows, cols), BF16)] * 2,
+            [shape((size, rest_width + LANES), F32), shape((size, rest_width + LANES), BF16)]
+            + [shape((2 * size, 2 * cols), BF16), shape((2 * size, cols), BF16)],
             2 * work,
-        )(*pre, *cot_list, *cot_other, first, second, third)
+        )(pre, *cot_list, *cot_other, first, second, third)
         rest = outs[0] + along_core(outs[1]).astype(F32)
         owned = call(
             functools.partial(own_body, lanes, width),
-            [shape((rows, width), F32), shape((rows, width), BF16)],
+            [shape((size, width), F32), shape((size, width), BF16)],
             work,
-        )(*outs[2:4], first, second)
+        )(outs[2], first, second)
         owned = owned[0] + along_core(owned[1]).astype(F32)
-        return owned, rest, outs[2:4], outs[4:6], tok_list + tok_other, cot_list + cot_other
-
-    near_own, near_rest, near_grads, near_hidden, tok_a, cot_a = experts_on(tok_near, cot_near)
-    far_own, far_rest, far_grads, far_hidden, tok_b, cot_b = experts_on(tok_far, cot_far)
+        return owned, rest, [outs[2]], [outs[3]], tok_list + tok_other, cot_list + cot_other
+
+    near_own, near_rest, *near = experts_on(tok_near, cot_near)
+    far_own, far_rest, *far = experts_on(tok_far, cot_far)
     early = 3 * width // (8 * LANES) * LANES
     if lanes == 2 and early > 0:
         near_in = along_tp(near_rest[:, early:width].astype(BF16), 1)
@@ -394,9 +397,9 @@
         next_out = near_out + side_in
         next_in = along_tp(next_out.astype(BF16), 1).astype(F32)
         tail = next_out[:, early:] + next_in[:, early:]
-        head = near_own[:, :early] + own_in.astype(F32) + next_in[:, :early]
-        rest = near_own[:, early:] + near_in.astype(F32) + last_in.astype(F32)
-        body = jnp.concatenate([head, rest], axis=1)
+        left = near_own[:, :early] + own_in.astype(F32) + next_in[:, :early]
+        right = near_own[:, early:] + near_in.astype(F32) + last_in.astype(F32)
+        body = jnp.concatenate([left, right], axis=1)
     else:
         body = near_own + along_side(far_own.astype(BF16)).astype(F32)
         both = near_rest + along_side(far_rest.astype(BF16)).astype(F32)
@@ -413,15 +416,18 @@
     result = jnp.concatenate([body, held], axis=1).astype(BF16)
     sent = {k: along_groups(result[k * cap : (k + 1) * cap], k) for k in range(groups - 1, 0, -1)}
     returned = [result[:cap]] + [sent[k] for k in range(1, groups)]
-    grads = list(near_grads) + list(far_grads)
-    scaled_hidden = list(near_hidden) + list(far_hidden)
+    grads, scaled_hidden, toks, cots = [near[i] + far[i] for i in range(4)]
     up_work = 2 * 2 * 4 * rows * features * cols
     first_grad, second_grad = call(
-        functools.partial(up_body, lanes, width), [shape((features, cols), F32)] * 2, up_work
-    )(*tok_a, *tok_b, *grads)
+        functools.partial(up_body, lanes, width, len(grads)),
+        [shape((features, cols), F32)] * 2,
+        up_work,
+    )(*toks, *grads)
     third_grad = call(
-        functools.partial(down_body, lanes, width), shape((cols, features), F32), up_work // 2
-    )(*cot_a, *cot_b, *scaled_hidden)
+        functools.partial(down_body, lanes, width, len(grads)),
+        shape((cols, features), F32),
+        up_work // 2,
+    )(*cots, *scaled_hidden)
     token_grad, group_grad, expert_grad = call(
         functools.partial(final_body, groups, cap),
         [shape((count, width), F32), shape((1, count), F32), shape((picks, count), F32)],

time: 102 us -> 93 us (0.912)
  starting transfers between devices: 40.2 us -> 36.1 us
  waiting for transfers between devices: 40.5 us -> 37.1 us
  Pallas kernels: 18.2 us -> 16.7 us
    ppermute x10 -> x7, starting transfers between devices: 13.2 us -> 8.18 us  [along_tp(): return lax.ppermute(a, 'tp', [(r, (r + j) % lanes) for r in range(lanes)])]
    ppermute x10 -> x7, waiting for transfers between devices: 17.7 us -> 13.3 us  [along_tp(): return lax.ppermute(a, 'tp', [(r, (r + j) % lanes) for r in range(lanes)])]
    ppermute x0 -> x3, waiting for transfers between devices: none -> 3.86 us  [along_diagonal(): lax.ppermute(jnp.where(core == 0, side, a), ('ep', 'tp'), pairs)]
    ppermute x0 -> x3, starting transfers between devices: none -> 3.68 us  [along_diagonal(): lax.ppermute(jnp.where(core == 0, side, a), ('ep', 'tp'), pairs)]
    ppermute x10 -> x7, waiting for transfers between devices: 13.7 us -> 10.8 us  [along_side(): return lax.ppermute(a, 'ep', [(e, e ^ 2) for e in range(experts)])]
    ppermute x10 -> x7, starting transfers between devices: 10.8 us -> 8.04 us  [along_side(): return lax.ppermute(a, 'ep', [(e, e ^ 2) for e in range(experts)])]
    pallas_call x14, Pallas kernels: 18.2 us -> 16.7 us  [run(): pl.pallas_call(body, out_shape=outs, in_specs=[pl.BlockSpec(memory_space=...]
  transfers between devices with their start and end apart: 40 -> 37, of which waited for: 15 -> 13; matrix products, arithmetic and copies ran while one was open for 1% -> 2% of each run, Pallas kernels for 15% -> 15%
where the time goes in v3:
time: 93 us; the launch traced here: 92.8 us
  waiting for transfers between devices  37.1 us (40%)
  starting transfers between devices  36.1 us (39%)
  Pallas kernels  16.7 us (18%)
  between operations  1.23 us (1%)
  other arithmetic  1.19 us (1%)
    pallas_call x14, Pallas kernels, run(): pl.pallas_call(body, out_shape=outs, in_specs=[pl.BlockSpec(memory_space=...  16.7 us
    ppermute x8, starting transfers between devices, along_groups(): return lax.ppermute(a, 'ep', [(e, e ^ k * EPG) for e in range(experts)])  13.5 us
    ppermute x7, waiting for transfers between devices, along_tp(): return lax.ppermute(a, 'tp', [(r, (r + j) % lanes) for r in range(lanes)])  13.3 us
    ppermute x7, waiting for transfers between devices, along_side(): return lax.ppermute(a, 'ep', [(e, e ^ 2) for e in range(experts)])  10.8 us
    ppermute x8, waiting for transfers between devices, along_groups(): return lax.ppermute(a, 'ep', [(e, e ^ k * EPG) for e in range(experts)])  9.07 us
    ppermute x7, starting transfers between devices, along_tp(): return lax.ppermute(a, 'tp', [(r, (r + j) % lanes) for r in range(lanes)])  8.18 us
    ppermute x7, starting transfers between devices, along_side(): return lax.ppermute(a, 'ep', [(e, e ^ 2) for e in range(experts)])  8.04 us
    ppermute x3, waiting for transfers between devices, along_diagonal(): lax.ppermute(jnp.where(core == 0, side, a), ('ep', 'tp'), pairs)  3.86 us
  transfers between devices with their start and end apart: 37, of which 13 were waited for; matrix products, arithmetic and copies ran while one was open for 2% of the time, Pallas kernels for 15%

profile of v3, /device:TPU:0, one launch (start us, length us, event | category | flops | bytes accessed | tf_op | source)
XLA Modules:
  0.0 92.8 jit_solution(18044427800180342903)
XLA Ops:
  0.6 1.7 %shard_map.136 = (bf16[48,2176]{1,0:T(8,128)(2,1)S(1)}, bf16[48,2176]{1,0:T(8,128)(2,1)S(1)}, bf16[48,1024]{1,0:T(8,128)(2,1)S(1)}, bf16[48,1024]{1,0:T(8,128)(2...) custom-call(s32[1,128]{1,0:T(1,128)} %bitcast.26, s32[2,128]{1,0:T(2,128)} %bitcast.31, ...), custom_call_target="tpu_custom_call" | custom-call | tf_op jit(solution)/shard_map/pallas_call | solution.py:27
  2.3 4.1 %collective-permute-start.1 = (bf16[48,1024]{1,0:T(8,128)(2,1)S(1)}, bf16[48,1024]{1,0:T(8,128)(2,1)S(1)}, u32[]{:S(2)}, u32[]{:S(2)}) collective-permute-start(bf16[48,1024]{1,0:T(8,128)(2,1)S(1)} %get-tuple-element.31), channel_id=1, source_target_pairs={{0,16},{2,18},{4,20},{6,22},{8,24},{10,26},{12,28},{14,30},{16,0},... | collective-permute-start | bytes 294920 | tf_op jit(solution)/shard_map/ppermute | solution.py:265
  6.5 1.3 %collective-permute-start.2 = (bf16[48,1024]{1,0:T(8,128)(2,1)S(1)}, bf16[48,1024]{1,0:T(8,128)(2,1)S(1)}, u32[]{:S(2)}, u32[]{:S(2)}) collective-permute-start(bf16[48,1024]{1,0:T(8,128)(2,1)S(1)} %get-tuple-element.32), channel_id=1, source_target_pairs={{0,24},{2,26},{4,28},{6,30},{8,16},{10,18},{12,20},{14,22},{16,8},... | collective-permute-start | bytes 294920 | tf_op jit(solution)/shard_map/ppermute | solution.py:265
  7.8 1.7 %collective-permute-start.8 = (bf16[48,1152]{1,0:T(8,128)(2,1)S(1)}, bf16[48,1152]{1,0:T(8,128)(2,1)S(1)}, u32[]{:S(2)}, u32[]{:S(2)}) collective-permute-start(bf16[48,1152]{1,0:T(8,128)(2,1)S(1)} %get-tuple-element.33), channel_id=1, source_target_pairs={{0,16},{2,18},{4,20},{6,22},{8,24},{10,26},{12,28},{14,30},{16,0},... | collective-permute-start | bytes 331784 | tf_op jit(solution)/shard_map/ppermute | solution.py:265
  9.5 0.9 collective-permute-start.9
  10.4 1.5 %collective-permute-start.14 = (bf16[48,2176]{1,0:T(8,128)(2,1)S(1)}, bf16[48,2176]{1,0:T(8,128)(2,1)S(1)}, u32[]{:S(2)}, u32[]{:S(2)}) collective-permute-start(bf16[48,2176]{1,0:T(8,128)(2,1)S(1)} %get-tuple-element.29), channel_id=1, source_target_pairs={{0,4},{2,6},{4,0},{6,2},{8,12},{10,14},{12,8},{14,10},{16,20},{18,... | collective-permute-start | bytes 626696 | tf_op jit(solution)/shard_map/ppermute | solution.py:268
  11.9 7.1 %collective-permute-done.1 = bf16[48,1024]{1,0:T(8,128)(2,1)S(1)} collective-permute-done((bf16[48,1024]{1,0:T(8,128)(2,1)S(1)}, bf16[48,1024]{1,0:T(8,128)(2,1)S(1)}, u32[]{:S(2)}, u32[]{:S(2)}) %collective-permute-start.1) | collective-permute-done | bytes 98336 | tf_op jit(solution)/shard_map/ppermute | solution.py:265
  19.1 1.7 %collective-permute-start.3 = (bf16[48,2048]{1,0:T(8,128)(2,1)S(1)}, bf16[48,2048]{1,0:T(8,128)(2,1)S(1)}, u32[]{:S(2)}, u32[]{:S(2)}) collective-permute-start(bf16[48,2048]{1,0:T(8,128)(2,1)S(1)} %slice.105), channel_id=1, source_target_pairs={{0,1},{1,0},{2,3},{3,2},{4,5},{5,4},{6,7},{7,6},{8,9},{9,8},{10,11... | collective-permute-start | bytes 589832 | tf_op jit(solution)/shard_map/ppermute | solution.py:274
  20.8 0.9 %collective-permute-start = (bf16[48,2176]{1,0:T(8,128)(2,1)S(1)}, bf16[48,2176]{1,0:T(8,128)(2,1)S(1)}, u32[]{:S(2)}, u32[]{:S(2)}) collective-permute-start(bf16[48,2176]{1,0:T(8,128)(2,1)S(1)} %get-tuple-element.30), channel_id=1, source_target_pairs={{0,8},{2,10},{4,12},{6,14},{8,0},{10,2},{12,4},{14,6},{16,24},{18,... | collective-permute-start | bytes 626696 | tf_op jit(solution)/shard_map/ppermute | solution.py:265
  21.7 1.8 %collective-permute-done.8 = bf16[48,1152]{1,0:T(8,128)(2,1)S(1)} collective-permute-done((bf16[48,1152]{1,0:T(8,128)(2,1)S(1)}, bf16[48,1152]{1,0:T(8,128)(2,1)S(1)}, u32[]{:S(2)}, u32[]{:S(2)}) %collective-permute-start.8) | collective-permute-done | bytes 110624 | tf_op jit(solution)/shard_map/ppermute | solution.py:265
  23.5 1.7 %collective-permute-start.16 = (bf16[96,1024]{1,0:T(8,128)(2,1)S(1)}, bf16[96,1024]{1,0:T(8,128)(2,1)S(1)}, u32[]{:S(2)}, u32[]{:S(2)}) collective-permute-start(bf16[96,1024]{1,0:T(8,128)(2,1)S(1)} %constant_dynamic-update-slice_fusion.4), channel_id=1, source_target_pairs={{0,4},{2,6},{4,0},{6,2},{8,12},{10,14},{12,8},{14,10},{16,20},{18,... | collective-permute-start | bytes 589832 | tf_op jit(solution)/shard_map/ppermute | solution.py:268
  25.2 1.6 %collective-permute-start.5 = (bf16[96,1024]{1,0:T(8,128)(2,1)S(1)}, bf16[96,1024]{1,0:T(8,128)(2,1)S(1)}, u32[]{:S(2)}, u32[]{:S(2)}) collective-permute-start(bf16[96,1024]{1,0:T(8,128)(2,1)S(1)} %constant_dynamic-update-slice_fusion.4), channel_id=1, source_target_pairs={{0,1},{1,0},{2,3},{3,2},{4,5},{5,4},{6,7},{7,6},{8,9},{9,8},{10,11... | collective-permute-start | bytes 589832 | tf_op jit(solution)/shard_map/ppermute | solution.py:274
  26.9 0.6 collective-permute-start.10
  27.5 1.3 %collective-permute-start.21 = (bf16[96,1152]{1,0:T(8,128)(2,1)S(1)}, bf16[96,1152]{1,0:T(8,128)(2,1)S(1)}, u32[]{:S(2)}, u32[]{:S(2)}) collective-permute-start(bf16[96,1152]{1,0:T(8,128)(2,1)S(1)} %pad_maximum_fusion.8), channel_id=1, source_target_pairs={{0,4},{2,6},{4,0},{6,2},{8,12},{10,14},{12,8},{14,10},{16,20},{18,... | collective-permute-start | bytes 663560 | tf_op jit(solution)/shard_map/ppermute | solution.py:268
  28.9 1.6 %collective-permute-start.4 = (bf16[48,2048]{1,0:T(8,128)(2,1)S(1)}, bf16[48,2048]{1,0:T(8,128)(2,1)S(1)}, u32[]{:S(2)}, u32[]{:S(2)}) collective-permute-start(bf16[48,2048]{1,0:T(8,128)(2,1)S(1)} %slice.138), channel_id=1, source_target_pairs={{0,1},{1,0},{2,3},{3,2},{4,5},{5,4},{6,7},{7,6},{8,9},{9,8},{10,11... | collective-permute-start | bytes 589832 | tf_op jit(solution)/shard_map/ppermute | solution.py:274
  30.6 0.1 collective-permute-start.6
  30.7 2.4 %collective-permute-done.5 = bf16[96,1024]{1,0:T(8,128)(2,1)S(1)} collective-permute-done((bf16[96,1024]{1,0:T(8,128)(2,1)S(1)}, bf16[96,1024]{1,0:T(8,128)(2,1)S(1)}, u32[]{:S(2)}, u32[]{:S(2)}) %collective-permute-start.5) | collective-permute-done | bytes 196640 | tf_op jit(solution)/shard_map/ppermute | solution.py:274
  33.1 3.2 %collective-permute-done.10 = bf16[96,1024]{1,0:T(8,128)(2,1)S(1)} collective-permute-done((bf16[96,1024]{1,0:T(8,128)(2,1)S(1)}, bf16[96,1024]{1,0:T(8,128)(2,1)S(1)}, u32[]{:S(2)}, u32[]{:S(2)}) %collective-permute-start.10) | collective-permute-done | bytes 196640 | tf_op jit(solution)/shard_map/ppermute | solution.py:274
  36.3 0.7 collective-permute-start.15
  37.0 1.4 %collective-permute-done.4 = bf16[48,2048]{1,0:T(8,128)(2,1)S(1)} collective-permute-done((bf16[48,2048]{1,0:T(8,128)(2,1)S(1)}, bf16[48,2048]{1,0:T(8,128)(2,1)S(1)}, u32[]{:S(2)}, u32[]{:S(2)}) %collective-permute-start.4) | collective-permute-done | bytes 196640 | tf_op jit(solution)/shard_map/ppermute | solution.py:274
  38.6 0.6 collective-permute-start.12
  39.1 3.0 %collective-permute-done.15 = bf16[48,2176]{1,0:T(8,128)(2,1)S(1)} collective-permute-done((bf16[48,2176]{1,0:T(8,128)(2,1)S(1)}, bf16[48,2176]{1,0:T(8,128)(2,1)S(1)}, u32[]{:S(2)}, u32[]{:S(2)}) %collective-permute-start.15) | collective-permute-done | bytes 208928 | tf_op jit(solution)/shard_map/ppermute | solution.py:268
  42.3 1.6 %collective-permute-start.17 = (bf16[96,2048]{1,0:T(8,128)(2,1)S(1)}, bf16[96,2048]{1,0:T(8,128)(2,1)S(1)}, u32[]{:S(2)}, u32[]{:S(2)}) collective-permute-start(bf16[96,2048]{1,0:T(8,128)(2,1)S(1)} %slice_select_fusion), channel_id=1, source_target_pairs={{0,1},{1,0},{2,6},{3,7},{4,5},{5,4},{6,2},{7,3},{8,9},{9,8},{10,14... | collective-permute-start | bytes 1179656 | tf_op jit(solution)/shard_map/ppermute | solution.py:286
  44.0 0.6 collective-permute-start.18
  44.5 1.5 %collective-permute-start.22 = (bf16[96,1024]{1,0:T(8,128)(2,1)S(1)}, bf16[96,1024]{1,0:T(8,128)(2,1)S(1)}, u32[]{:S(2)}, u32[]{:S(2)}) collective-permute-start(bf16[96,1024]{1,0:T(8,128)(2,1)S(1)} %slice_select_fusion.1), channel_id=1, source_target_pairs={{0,1},{1,0},{2,6},{3,7},{4,5},{5,4},{6,2},{7,3},{8,9},{9,8},{10,14... | collective-permute-start | bytes 589832 | tf_op jit(solution)/shard_map/ppermute | solution.py:286
  46.1 1.0 %shard_map.137.refs_0_ = f32[384,512]{1,0:T(8,128)S(1)} custom-call(bf16[192,1024]{1,0:T(8,128)(2,1)S(1)} %pad_maximum_fusion.2.refs_0_, bf16[192,1024]{1,0:T(8,128)(2,1)S(1)} %pad_maximum_fusion.3.refs_1_, bf16[192,1024]{1,0:T(8,128)(2,1)S(1)} %collective-permute-done.6.refs_2_, bf16[192,1024]{1,0:T(8,128)(2,1)S(1)} %collective-permute-done.7.refs_3_, ...), custom_call_target="tpu_custom_call" | custom-call | flops 805306368 | tf_op jit(solution)/shard_map/pallas_call | solution.py:27
  47.1 0.5 collective-permute-start.23
  47.6 1.9 %shard_map.138 = (f32[192,1152]{1,0:T(8,128)S(1)}, bf16[192,1152]{1,0:T(8,128)(2,1)S(1)}, bf16[384,512]{1,0:T(8,128)(2,1)S(1)}, bf16[384,256]{1,0:T(8,128)(2,1)S(1)}) custom-call(f32[384,512]{1,0:T(8,128)S(1)} %shard_map.137.refs_0_, bf16[192,1152]{1,0:T(8,128)(2,1)S(1)} %pad_maximum_fusion.refs_1_.refs_0_, ...), custom_call_target="tpu_custom_call" | custom-call | flops 805306368 | tf_op jit(solution)/shard_map/pallas_call | solution.py:27
  49.6 0.6 shard_map.139
  50.2 0.2 collective-permute-start.13
  50.4 1.9 %collective-permute-done.18 = bf16[96,1024]{1,0:T(8,128)(2,1)S(1)} collective-permute-done((bf16[96,1024]{1,0:T(8,128)(2,1)S(1)}, bf16[96,1024]{1,0:T(8,128)(2,1)S(1)}, u32[]{:S(2)}, u32[]{:S(2)}) %collective-permute-start.18) | collective-permute-done | bytes 196640 | tf_op jit(solution)/shard_map/ppermute | solution.py:286
  52.3 2.0 %collective-permute-done.22 = bf16[96,1024]{1,0:T(8,128)(2,1)S(1)} collective-permute-done((bf16[96,1024]{1,0:T(8,128)(2,1)S(1)}, bf16[96,1024]{1,0:T(8,128)(2,1)S(1)}, u32[]{:S(2)}, u32[]{:S(2)}) %collective-permute-start.22) | collective-permute-done | bytes 196640 | tf_op jit(solution)/shard_map/ppermute | solution.py:286
  54.5 0.1 shard_map.146.refs_7_
  54.6 0.1 shard_map.145.refs_6_
  54.7 0.1 shard_map.144.refs_5_
  54.9 0.1 shard_map.143.refs_4_
  55.1 0.6 collective-permute-start.27
  55.6 0.1 convert_add_fusion.2
  55.7 1.0 %shard_map.140.refs_0_ = f32[384,512]{1,0:T(8,128)S(1)} custom-call(bf16[192,1024]{1,0:T(8,128)(2,1)S(1)} %pad_maximum_fusion.5.refs_0_.refs_4_, bf16[192,1024]{1,0:T(8,128)(2,1)S(1)} %pad_maximum_fusion.6.refs_1_.refs_5_, bf16[192,1024]{1,0:T(8,128)(2,1)S(1)} %collective-permute-done.19.refs_2_.refs_6_, ...), custom_call_target="tpu_custom_call" | custom-call | flops 805306368 | tf_op jit(solution)/shard_map/pallas_call | solution.py:27
  56.8 1.9 %shard_map.141 = (f32[192,1152]{1,0:T(8,128)S(1)}, bf16[192,1152]{1,0:T(8,128)(2,1)S(1)}, bf16[384,512]{1,0:T(8,128)(2,1)S(1)}, bf16[384,256]{1,0:T(8,128)(2,1)S(1)}) custom-call(f32[384,512]{1,0:T(8,128)S(1)} %shard_map.140.refs_0_, bf16[192,1152]{1,0:T(8,128)(2,1)S(1)} %pad_maximum_fusion.1.refs_1_.refs_4_, ...), custom_call_target="tpu_custom_call" | custom-call | flops 805306368 | tf_op jit(solution)/shard_map/pallas_call | solution.py:27
  58.7 0.1 collective-permute-start.28
  58.8 0.6 shard_map.142
  59.4 0.5 collective-permute-start.25
  59.9 0.1 convert_add_fusion
  60.1 1.6 %collective-permute-start.31 = (bf16[192,640]{1,0:T(8,128)(2,1)S(1)}, bf16[192,640]{1,0:T(8,128)(2,1)S(1)}, u32[]{:S(2)}, u32[]{:S(2)}) collective-permute-start(bf16[192,640]{1,0:T(8,128)(2,1)S(1)} %slice.193), channel_id=1, source_target_pairs={{0,1},{1,0},{2,3},{3,2},{4,5},{5,4},{6,7},{7,6},{8,9},{9,8},{10,11... | collective-permute-start | bytes 737288 | tf_op jit(solution)/shard_map/ppermute | solution.py:274
  61.7 0.1 add_convert_fusion
  61.8 0.7 collective-permute-start.29
  62.6 0.5 collective-permute-start.32
  63.1 0.1 convert_add_fusion.1
  63.3 1.4 %collective-permute-start.26 = (bf16[192,384]{1,0:T(8,128)(2,1)S(1)}, bf16[192,384]{1,0:T(8,128)(2,1)S(1)}, u32[]{:S(2)}, u32[]{:S(2)}) collective-permute-start(bf16[192,384]{1,0:T(8,128)(2,1)S(1)} %slice.194), channel_id=1, source_target_pairs={{0,4},{2,6},{4,0},{6,2},{8,12},{10,14},{12,8},{14,10},{16,20},{18,... | collective-permute-start | bytes 442376 | tf_op jit(solution)/shard_map/ppermute | solution.py:268
  64.7 5.0 %collective-permute-done.29 = bf16[192,512]{1,0:T(8,128)(2,1)S(1)} collective-permute-done((bf16[192,512]{1,0:T(8,128)(2,1)S(1)}, bf16[192,512]{1,0:T(8,128)(2,1)S(1)}, u32[]{:S(2)}, u32[]{:S(2)}) %collective-permute-start.29) | collective-permute-done | bytes 196640 | tf_op jit(solution)/shard_map/ppermute | solution.py:268
  69.7 0.6 collective-permute-start.30
  70.4 3.9 %collective-permute-done.32 = bf16[192,640]{1,0:T(8,128)(2,1)S(1)} collective-permute-done((bf16[192,640]{1,0:T(8,128)(2,1)S(1)}, bf16[192,640]{1,0:T(8,128)(2,1)S(1)}, u32[]{:S(2)}, u32[]{:S(2)}) %collective-permute-start.32) | collective-permute-done | bytes 245792 | tf_op jit(solution)/shard_map/ppermute | solution.py:274
  74.3 0.7 collective-permute-start.33
  75.0 2.5 %collective-permute-done.30 = bf16[192,512]{1,0:T(8,128)(2,1)S(1)} collective-permute-done((bf16[192,512]{1,0:T(8,128)(2,1)S(1)}, bf16[192,512]{1,0:T(8,128)(2,1)S(1)}, u32[]{:S(2)}, u32[]{:S(2)}) %collective-permute-start.30) | collective-permute-done | bytes 196640 | tf_op jit(solution)/shard_map/ppermute | solution.py:274
  77.6 0.1 fusion.6
  77.8 2.8 %collective-permute-done.33 = bf16[192,640]{1,0:T(8,128)(2,1)S(1)} collective-permute-done((bf16[192,640]{1,0:T(8,128)(2,1)S(1)}, bf16[192,640]{1,0:T(8,128)(2,1)S(1)}, u32[]{:S(2)}, u32[]{:S(2)}) %collective-permute-start.33) | collective-permute-done | bytes 245792 | tf_op jit(solution)/shard_map/ppermute | solution.py:268
  80.5 0.1 fusion.3
  80.7 3.6 %collective-permute-start.36 = (bf16[48,1152]{1,0:T(8,128)(2,1)S(1)}, bf16[48,1152]{1,0:T(8,128)(2,1)S(1)}, u32[]{:S(2)}, u32[]{:S(2)}) collective-permute-start(bf16[48,1152]{1,0:T(8,128)(2,1)S(1)} %get-tuple-element.54), channel_id=1, source_target_pairs={{0,24},{2,26},{4,28},{6,30},{8,16},{10,18},{12,20},{14,22},{16,8},... | collective-permute-start | bytes 331784 | tf_op jit(solution)/shard_map/ppermute | solution.py:265
  84.3 0.9 collective-permute-start.34
  85.2 3.8 %shard_map.148 = (f32[2048,256]{1,0:T(8,128)}, f32[2048,256]{1,0:T(8,128)}) custom-call(bf16[192,1024]{1,0:T(8,128)(2,1)S(1)} %pad_maximum_fusion.2.refs_0_, bf16[192,1024]{1,0:T(8,128)(2,1)S(1)} %pad_maximum_fusion.3.refs_1_, bf16[192,1024]{1,0:T(8,128)(2,1)S(1)} %collective-permute-done.6.refs_2_, bf16[192,1024]{1,0:T(8,128)(2,1)S(1)} %collective-permute-done.7.refs_3_, ...), custom_call_target="tpu_custom_call" | custom-call | flops 1610612736 | tf_op jit(solution)/shard_map/pallas_call | solution.py:27
  89.0 2.3 %shard_map.149 = f32[256,2048]{1,0:T(8,128)} custom-call(bf16[192,1152]{1,0:T(8,128)(2,1)S(1)} %pad_maximum_fusion.refs_1_.refs_0_, bf16[192,1024]{1,0:T(8,128)(2,1)S(1)} %pad_maximum_fusion.4.refs_2_.refs_1_, bf16[192,1152]{1,0:T(8,128)(2,1)S(1)} %collective-permute-done.11.refs_3_.refs_2_, bf16[192,1024]{1,0:T(8,128)(2,1)S(1)} %collective-permute-done.12.refs_4_.refs_3_, ...), custom_call_target="tpu_custom_call" | custom-call | flops 805306368 | tf_op jit(solution)/shard_map/pallas_call | solution.py:27
  91.4 0.2 collective-permute-done.35.refs_2_
  91.5 1.3 %shard_map.147 = (f32[128,1024]{1,0:T(8,128)}, f32[1,128]{1,0:T(1,128)}, f32[2,128]{1,0:T(2,128)}) custom-call(bf16[48,1152]{1,0:T(8,128)(2,1)S(1)} %get-tuple-element.57.refs_0_, bf16[48,1152]{1,0:T(8,128)(2,1)S(1)} %collective-permute-done.34.refs_1_, bf16[48,1152]{1,0:T(8,128)(2,1)S(1)} %collective-permute-done.35.refs_2_, ...), custom_call_target="tpu_custom_call" | custom-call | tf_op jit(solution)/shard_map/pallas_call | solution.py:27
  (94 shorter events, 1.5 us)
Async XLA Ops:
  2.3 16.7 %collective-permute-start.1 = (bf16[48,1024]{1,0:T(8,128)(2,1)S(1)}, bf16[48,1024]{1,0:T(8,128)(2,1)S(1)}, u32[]{:S(2)}, u32[]{:S(2)}) collective-permute-start(bf16[48,1024]{1,0:T(8,128)(2,1)S(1)} %get-tuple-element.31), channel_id=1, source_target_pairs={{0,16},{2,18},{4,20},{6,22},{8,24},{10,26},{12,28},{14,30},{16,0},... | collective-permute-start | bytes 294920 | tf_op jit(solution)/shard_map/ppermute | solution.py:265
  6.5 14.3 %collective-permute-start.2 = (bf16[48,1024]{1,0:T(8,128)(2,1)S(1)}, bf16[48,1024]{1,0:T(8,128)(2,1)S(1)}, u32[]{:S(2)}, u32[]{:S(2)}) collective-permute-start(bf16[48,1024]{1,0:T(8,128)(2,1)S(1)} %get-tuple-element.32), channel_id=1, source_target_pairs={{0,24},{2,26},{4,28},{6,30},{8,16},{10,18},{12,20},{14,22},{16,8},... | collective-permute-start | bytes 294920 | tf_op jit(solution)/shard_map/ppermute | solution.py:265
  7.8 15.7 %collective-permute-start.8 = (bf16[48,1152]{1,0:T(8,128)(2,1)S(1)}, bf16[48,1152]{1,0:T(8,128)(2,1)S(1)}, u32[]{:S(2)}, u32[]{:S(2)}) collective-permute-start(bf16[48,1152]{1,0:T(8,128)(2,1)S(1)} %get-tuple-element.33), channel_id=1, source_target_pairs={{0,16},{2,18},{4,20},{6,22},{8,24},{10,26},{12,28},{14,30},{16,0},... | collective-permute-start | bytes 331784 | tf_op jit(solution)/shard_map/ppermute | solution.py:265
  9.5 15.7 %collective-permute-start.9 = (bf16[48,1152]{1,0:T(8,128)(2,1)S(1)}, bf16[48,1152]{1,0:T(8,128)(2,1)S(1)}, u32[]{:S(2)}, u32[]{:S(2)}) collective-permute-start(bf16[48,1152]{1,0:T(8,128)(2,1)S(1)} %get-tuple-element.34), channel_id=1, source_target_pairs={{0,24},{2,26},{4,28},{6,30},{8,16},{10,18},{12,20},{14,22},{16,8},... | collective-permute-start | bytes 331784 | tf_op jit(solution)/shard_map/ppermute | solution.py:265
  10.4 18.5 %collective-permute-start.14 = (bf16[48,2176]{1,0:T(8,128)(2,1)S(1)}, bf16[48,2176]{1,0:T(8,128)(2,1)S(1)}, u32[]{:S(2)}, u32[]{:S(2)}) collective-permute-start(bf16[48,2176]{1,0:T(8,128)(2,1)S(1)} %get-tuple-element.29), channel_id=1, source_target_pairs={{0,4},{2,6},{4,0},{6,2},{8,12},{10,14},{12,8},{14,10},{16,20},{18,... | collective-permute-start | bytes 626696 | tf_op jit(solution)/shard_map/ppermute | solution.py:268
  19.1 7.8 %collective-permute-start.3 = (bf16[48,2048]{1,0:T(8,128)(2,1)S(1)}, bf16[48,2048]{1,0:T(8,128)(2,1)S(1)}, u32[]{:S(2)}, u32[]{:S(2)}) collective-permute-start(bf16[48,2048]{1,0:T(8,128)(2,1)S(1)} %slice.105), channel_id=1, source_target_pairs={{0,1},{1,0},{2,3},{3,2},{4,5},{5,4},{6,7},{7,6},{8,9},{9,8},{10,11... | collective-permute-start | bytes 589832 | tf_op jit(solution)/shard_map/ppermute | solution.py:274
  20.8 6.7 %collective-permute-start = (bf16[48,2176]{1,0:T(8,128)(2,1)S(1)}, bf16[48,2176]{1,0:T(8,128)(2,1)S(1)}, u32[]{:S(2)}, u32[]{:S(2)}) collective-permute-start(bf16[48,2176]{1,0:T(8,128)(2,1)S(1)} %get-tuple-element.30), channel_id=1, source_target_pairs={{0,8},{2,10},{4,12},{6,14},{8,0},{10,2},{12,4},{14,6},{16,24},{18,... | collective-permute-start | bytes 626696 | tf_op jit(solution)/shard_map/ppermute | solution.py:265
  23.5 7.0 %collective-permute-start.16 = (bf16[96,1024]{1,0:T(8,128)(2,1)S(1)}, bf16[96,1024]{1,0:T(8,128)(2,1)S(1)}, u32[]{:S(2)}, u32[]{:S(2)}) collective-permute-start(bf16[96,1024]{1,0:T(8,128)(2,1)S(1)} %constant_dynamic-update-slice_fusion.4), channel_id=1, source_target_pairs={{0,4},{2,6},{4,0},{6,2},{8,12},{10,14},{12,8},{14,10},{16,20},{18,... | collective-permute-start | bytes 589832 | tf_op jit(solution)/shard_map/ppermute | solution.py:268
  25.2 7.8 %collective-permute-start.5 = (bf16[96,1024]{1,0:T(8,128)(2,1)S(1)}, bf16[96,1024]{1,0:T(8,128)(2,1)S(1)}, u32[]{:S(2)}, u32[]{:S(2)}) collective-permute-start(bf16[96,1024]{1,0:T(8,128)(2,1)S(1)} %constant_dynamic-update-slice_fusion.4), channel_id=1, source_target_pairs={{0,1},{1,0},{2,3},{3,2},{4,5},{5,4},{6,7},{7,6},{8,9},{9,8},{10,11... | collective-permute-start | bytes 589832 | tf_op jit(solution)/shard_map/ppermute | solution.py:274
  26.9 9.4 %collective-permute-start.10 = (bf16[96,1024]{1,0:T(8,128)(2,1)S(1)}, bf16[96,1024]{1,0:T(8,128)(2,1)S(1)}, u32[]{:S(2)}, u32[]{:S(2)}) collective-permute-start(bf16[96,1024]{1,0:T(8,128)(2,1)S(1)} %pad_maximum_fusion.9), channel_id=1, source_target_pairs={{0,1},{1,0},{2,3},{3,2},{4,5},{5,4},{6,7},{7,6},{8,9},{9,8},{10,11... | collective-permute-start | bytes 589832 | tf_op jit(solution)/shard_map/ppermute | solution.py:274
  27.5 9.5 %collective-permute-start.21 = (bf16[96,1152]{1,0:T(8,128)(2,1)S(1)}, bf16[96,1152]{1,0:T(8,128)(2,1)S(1)}, u32[]{:S(2)}, u32[]{:S(2)}) collective-permute-start(bf16[96,1152]{1,0:T(8,128)(2,1)S(1)} %pad_maximum_fusion.8), channel_id=1, source_target_pairs={{0,4},{2,6},{4,0},{6,2},{8,12},{10,14},{12,8},{14,10},{16,20},{18,... | collective-permute-start | bytes 663560 | tf_op jit(solution)/shard_map/ppermute | solution.py:268
  28.9 9.5 %collective-permute-start.4 = (bf16[48,2048]{1,0:T(8,128)(2,1)S(1)}, bf16[48,2048]{1,0:T(8,128)(2,1)S(1)}, u32[]{:S(2)}, u32[]{:S(2)}) collective-permute-start(bf16[48,2048]{1,0:T(8,128)(2,1)S(1)} %slice.138), channel_id=1, source_target_pairs={{0,1},{1,0},{2,3},{3,2},{4,5},{5,4},{6,7},{7,6},{8,9},{9,8},{10,11... | collective-permute-start | bytes 589832 | tf_op jit(solution)/shard_map/ppermute | solution.py:274
  30.6 13.4 %collective-permute-start.6 = (bf16[192,1024]{1,0:T(8,128)(2,1)S(1)}, bf16[192,1024]{1,0:T(8,128)(2,1)S(1)}, u32[]{:S(2)}, u32[]{:S(2)}) collective-permute-start(bf16[192,1024]{1,0:T(8,128)(2,1)S(1)} %pad_maximum_fusion.2.refs_0_), channel_id=1, source_target_pairs={{0,2},{2,0},{4,6},{6,4},{8,10},{10,8},{12,14},{14,12},{16,18},{18,... | collective-permute-start | bytes 1179656 | tf_op jit(solution)/shard_map/ppermute | solution.py:271
  33.1 14.0 %collective-permute-start.11 = (bf16[192,1152]{1,0:T(8,128)(2,1)S(1)}, bf16[192,1152]{1,0:T(8,128)(2,1)S(1)}, u32[]{:S(2)}, u32[]{:S(2)}) collective-permute-start(bf16[192,1152]{1,0:T(8,128)(2,1)S(1)} %pad_maximum_fusion.refs_1_.refs_0_), channel_id=1, source_target_pairs={{0,2},{2,0},{4,6},{6,4},{8,10},{10,8},{12,14},{14,12},{16,18},{18,... | collective-permute-start | bytes 1327112 | tf_op jit(solution)/shard_map/ppermute | solution.py:271
  36.3 5.9 %collective-permute-start.15 = (bf16[48,2176]{1,0:T(8,128)(2,1)S(1)}, bf16[48,2176]{1,0:T(8,128)(2,1)S(1)}, u32[]{:S(2)}, u32[]{:S(2)}) collective-permute-start(bf16[48,2176]{1,0:T(8,128)(2,1)S(1)} %collective-permute-done), channel_id=1, source_target_pairs={{0,4},{2,6},{4,0},{6,2},{8,12},{10,14},{12,8},{14,10},{16,20},{18,... | collective-permute-start | bytes 626696 | tf_op jit(solution)/shard_map/ppermute | solution.py:268
  38.5 6.1 %collective-permute-start.7 = (bf16[192,1024]{1,0:T(8,128)(2,1)S(1)}, bf16[192,1024]{1,0:T(8,128)(2,1)S(1)}, u32[]{:S(2)}, u32[]{:S(2)}) collective-permute-start(bf16[192,1024]{1,0:T(8,128)(2,1)S(1)} %pad_maximum_fusion.3.refs_1_), channel_id=1, source_target_pairs={{0,2},{2,0},{4,6},{6,4},{8,10},{10,8},{12,14},{14,12},{16,18},{18,... | collective-permute-start | bytes 1179656 | tf_op jit(solution)/shard_map/ppermute | solution.py:271
  38.6 7.5 %copy-start = (bf16[1,2048,256]{2,1,0:T(8,128)(2,1)S(1)}, bf16[1,2048,256]{2,1,0:T(8,128)(2,1)}, u32[]{:S(2)}) copy-start(bf16[1,2048,256]{2,1,0:T(8,128)(2,1)} %param.15) | copy-start | bytes 3145732
  38.6 7.5 %copy-start.1 = (bf16[1,2048,256]{2,1,0:T(8,128)(2,1)S(1)}, bf16[1,2048,256]{2,1,0:T(8,128)(2,1)}, u32[]{:S(2)}) copy-start(bf16[1,2048,256]{2,1,0:T(8,128)(2,1)} %param.16) | copy-start | bytes 3145732
  38.6 8.5 %collective-permute-start.12 = (bf16[192,1024]{1,0:T(8,128)(2,1)S(1)}, bf16[192,1024]{1,0:T(8,128)(2,1)S(1)}, u32[]{:S(2)}, u32[]{:S(2)}) collective-permute-start(bf16[192,1024]{1,0:T(8,128)(2,1)S(1)} %pad_maximum_fusion.4.refs_2_.refs_1_), channel_id=1, source_target_pairs={{0,2},{2,0},{4,6},{6,4},{8,10},{10,8},{12,14},{14,12},{16,18},{18,... | collective-permute-start | bytes 1179656 | tf_op jit(solution)/shard_map/ppermute | solution.py:271
  42.3 7.9 %collective-permute-start.17 = (bf16[96,2048]{1,0:T(8,128)(2,1)S(1)}, bf16[96,2048]{1,0:T(8,128)(2,1)S(1)}, u32[]{:S(2)}, u32[]{:S(2)}) collective-permute-start(bf16[96,2048]{1,0:T(8,128)(2,1)S(1)} %slice_select_fusion), channel_id=1, source_target_pairs={{0,1},{1,0},{2,6},{3,7},{4,5},{5,4},{6,2},{7,3},{8,9},{9,8},{10,14... | collective-permute-start | bytes 1179656 | tf_op jit(solution)/shard_map/ppermute | solution.py:286
  44.0 8.3 %collective-permute-start.18 = (bf16[96,1024]{1,0:T(8,128)(2,1)S(1)}, bf16[96,1024]{1,0:T(8,128)(2,1)S(1)}, u32[]{:S(2)}, u32[]{:S(2)}) collective-permute-start(bf16[96,1024]{1,0:T(8,128)(2,1)S(1)} %broadcast_select_fusion), channel_id=1, source_target_pairs={{0,1},{1,0},{2,6},{3,7},{4,5},{5,4},{6,2},{7,3},{8,9},{9,8},{10,14... | collective-permute-start | bytes 589832 | tf_op jit(solution)/shard_map/ppermute | solution.py:286
  44.5 9.8 %collective-permute-start.22 = (bf16[96,1024]{1,0:T(8,128)(2,1)S(1)}, bf16[96,1024]{1,0:T(8,128)(2,1)S(1)}, u32[]{:S(2)}, u32[]{:S(2)}) collective-permute-start(bf16[96,1024]{1,0:T(8,128)(2,1)S(1)} %slice_select_fusion.1), channel_id=1, source_target_pairs={{0,1},{1,0},{2,6},{3,7},{4,5},{5,4},{6,2},{7,3},{8,9},{9,8},{10,14... | collective-permute-start | bytes 589832 | tf_op jit(solution)/shard_map/ppermute | solution.py:286
  46.1 1.6 %copy-start.2 = (bf16[1,256,2048]{2,1,0:T(8,128)(2,1)S(1)}, bf16[1,256,2048]{2,1,0:T(8,128)(2,1)}, u32[]{:S(2)}) copy-start(bf16[1,256,2048]{2,1,0:T(8,128)(2,1)} %param.17) | copy-start | bytes 3145732
  47.0 8.7 %collective-permute-start.19 = (bf16[192,1024]{1,0:T(8,128)(2,1)S(1)}, bf16[192,1024]{1,0:T(8,128)(2,1)S(1)}, u32[]{:S(2)}, u32[]{:S(2)}) collective-permute-start(bf16[192,1024]{1,0:T(8,128)(2,1)S(1)} %pad_maximum_fusion.5.refs_0_.refs_4_), channel_id=1, source_target_pairs={{0,2},{2,0},{4,6},{6,4},{8,10},{10,8},{12,14},{14,12},{16,18},{18,... | collective-permute-start | bytes 1179656 | tf_op jit(solution)/shard_map/ppermute | solution.py:271
  47.1 9.6 %collective-permute-start.23 = (bf16[192,1152]{1,0:T(8,128)(2,1)S(1)}, bf16[192,1152]{1,0:T(8,128)(2,1)S(1)}, u32[]{:S(2)}, u32[]{:S(2)}) collective-permute-start(bf16[192,1152]{1,0:T(8,128)(2,1)S(1)} %pad_maximum_fusion.1.refs_1_.refs_4_), channel_id=1, source_target_pairs={{0,2},{2,0},{4,6},{6,4},{8,10},{10,8},{12,14},{14,12},{16,18},{18,... | collective-permute-start | bytes 1327112 | tf_op jit(solution)/shard_map/ppermute | solution.py:271
  49.5 4.9 %copy-start.3 = (s32[128]{0:T(128)S(1)}, s32[128]{0:T(128)}, u32[]{:S(2)}) copy-start(s32[128]{0:T(128)} %param.13) | copy-start | bytes 1540
  50.2 4.9 %collective-permute-start.13 = (bf16[192,1024]{1,0:T(8,128)(2,1)S(1)}, bf16[192,1024]{1,0:T(8,128)(2,1)S(1)}, u32[]{:S(2)}, u32[]{:S(2)}) collective-permute-start(bf16[192,1024]{1,0:T(8,128)(2,1)S(1)} %get-tuple-element.37), channel_id=1, source_target_pairs={{0,2},{2,0},{4,6},{6,4},{8,10},{10,8},{12,14},{14,12},{16,18},{18,... | collective-permute-start | bytes 1179656 | tf_op jit(solution)/shard_map/ppermute | solution.py:271
  52.3 3.5 %collective-permute-start.20 = (bf16[192,1024]{1,0:T(8,128)(2,1)S(1)}, bf16[192,1024]{1,0:T(8,128)(2,1)S(1)}, u32[]{:S(2)}, u32[]{:S(2)}) collective-permute-start(bf16[192,1024]{1,0:T(8,128)(2,1)S(1)} %pad_maximum_fusion.6.refs_1_.refs_5_), channel_id=1, source_target_pairs={{0,2},{2,0},{4,6},{6,4},{8,10},{10,8},{12,14},{14,12},{16,18},{18,... | collective-permute-start | bytes 1179656 | tf_op jit(solution)/shard_map/ppermute | solution.py:271
  54.4 2.4 %collective-permute-start.24 = (bf16[192,1024]{1,0:T(8,128)(2,1)S(1)}, bf16[192,1024]{1,0:T(8,128)(2,1)S(1)}, u32[]{:S(2)}, u32[]{:S(2)}) collective-permute-start(bf16[192,1024]{1,0:T(8,128)(2,1)S(1)} %pad_maximum_fusion.7.refs_2_.refs_5_), channel_id=1, source_target_pairs={{0,2},{2,0},{4,6},{6,4},{8,10},{10,8},{12,14},{14,12},{16,18},{18,... | collective-permute-start | bytes 1179656 | tf_op jit(solution)/shard_map/ppermute | solution.py:271
  55.1 4.9 %collective-permute-start.27 = (bf16[192,1152]{1,0:T(8,128)(2,1)S(1)}, bf16[192,1152]{1,0:T(8,128)(2,1)S(1)}, u32[]{:S(2)}, u32[]{:S(2)}) collective-permute-start(bf16[192,1152]{1,0:T(8,128)(2,1)S(1)} %get-tuple-element.42), channel_id=1, source_target_pairs={{0,2},{2,0},{4,6},{6,4},{8,10},{10,8},{12,14},{14,12},{16,18},{18,... | collective-permute-start | bytes 1327112 | tf_op jit(solution)/shard_map/ppermute | solution.py:271
  58.7 3.0 %collective-permute-start.28 = (bf16[192,1152]{1,0:T(8,128)(2,1)S(1)}, bf16[192,1152]{1,0:T(8,128)(2,1)S(1)}, u32[]{:S(2)}, u32[]{:S(2)}) collective-permute-start(bf16[192,1152]{1,0:T(8,128)(2,1)S(1)} %get-tuple-element.44), channel_id=1, source_target_pairs={{0,2},{2,0},{4,6},{6,4},{8,10},{10,8},{12,14},{14,12},{16,18},{18,... | collective-permute-start | bytes 1327112 | tf_op jit(solution)/shard_map/ppermute | solution.py:271
  59.4 3.8 %collective-permute-start.25 = (bf16[192,1024]{1,0:T(8,128)(2,1)S(1)}, bf16[192,1024]{1,0:T(8,128)(2,1)S(1)}, u32[]{:S(2)}, u32[]{:S(2)}) collective-permute-start(bf16[192,1024]{1,0:T(8,128)(2,1)S(1)} %get-tuple-element.40), channel_id=1, source_target_pairs={{0,2},{2,0},{4,6},{6,4},{8,10},{10,8},{12,14},{14,12},{16,18},{18,... | collective-permute-start | bytes 1179656 | tf_op jit(solution)/shard_map/ppermute | solution.py:271
  60.0 1.8 %copy-start.7 = (f32[192,1152]{1,0:T(8,128)}, f32[192,1152]{1,0:T(8,128)S(1)}, u32[]{:S(2)}) copy-start(f32[192,1152]{1,0:T(8,128)S(1)} %convert_add_fusion) | copy-start | bytes 2654212
  60.1 17.7 %collective-permute-start.31 = (bf16[192,640]{1,0:T(8,128)(2,1)S(1)}, bf16[192,640]{1,0:T(8,128)(2,1)S(1)}, u32[]{:S(2)}, u32[]{:S(2)}) collective-permute-start(bf16[192,640]{1,0:T(8,128)(2,1)S(1)} %slice.193), channel_id=1, source_target_pairs={{0,1},{1,0},{2,3},{3,2},{4,5},{5,4},{6,7},{7,6},{8,9},{9,8},{10,11... | collective-permute-start | bytes 737288 | tf_op jit(solution)/shard_map/ppermute | solution.py:274
  61.8 7.8 %collective-permute-start.29 = (bf16[192,512]{1,0:T(8,128)(2,1)S(1)}, bf16[192,512]{1,0:T(8,128)(2,1)S(1)}, u32[]{:S(2)}, u32[]{:S(2)}) collective-permute-start(bf16[192,512]{1,0:T(8,128)(2,1)S(1)} %pad_maximum_fusion.10), channel_id=1, source_target_pairs={{0,4},{2,6},{4,0},{6,2},{8,12},{10,14},{12,8},{14,10},{16,20},{18,... | collective-permute-start | bytes 589832 | tf_op jit(solution)/shard_map/ppermute | solution.py:268
  62.6 7.1 %slice-start = ((f32[192,1152]{1,0:T(8,128)}), f32[192,128]{1,0:T(8,128)S(1)}, s32[]{:S(2)}) async-start(f32[192,1152]{1,0:T(8,128)} %copy-done.7), calls=%async_computation | async-start | bytes 196608 | tf_op jit(solution)/shard_map/slice | solution.py:396
  62.6 7.1 %slice-start.1 = ((f32[192,1152]{1,0:T(8,128)}), f32[192,384]{1,0:T(8,128)S(1)}, s32[]{:S(2)}) async-start(f32[192,1152]{1,0:T(8,128)} %copy-done.7), calls=%async_computation.1 | async-start | bytes 589824 | tf_op jit(solution)/shard_map/slice | solution.py:396
  62.6 11.6 %collective-permute-start.32 = (bf16[192,640]{1,0:T(8,128)(2,1)S(1)}, bf16[192,640]{1,0:T(8,128)(2,1)S(1)}, u32[]{:S(2)}, u32[]{:S(2)}) collective-permute-start(bf16[192,640]{1,0:T(8,128)(2,1)S(1)} %slice.160), channel_id=1, source_target_pairs={{0,1},{1,0},{2,3},{3,2},{4,5},{5,4},{6,7},{7,6},{8,9},{9,8},{10,11... | collective-permute-start | bytes 737288 | tf_op jit(solution)/shard_map/ppermute | solution.py:274
  63.3 14.4 %collective-permute-start.26 = (bf16[192,384]{1,0:T(8,128)(2,1)S(1)}, bf16[192,384]{1,0:T(8,128)(2,1)S(1)}, u32[]{:S(2)}, u32[]{:S(2)}) collective-permute-start(bf16[192,384]{1,0:T(8,128)(2,1)S(1)} %slice.194), channel_id=1, source_target_pairs={{0,4},{2,6},{4,0},{6,2},{8,12},{10,14},{12,8},{14,10},{16,20},{18,... | collective-permute-start | bytes 442376 | tf_op jit(solution)/shard_map/ppermute | solution.py:268
  69.7 7.7 %collective-permute-start.30 = (bf16[192,512]{1,0:T(8,128)(2,1)S(1)}, bf16[192,512]{1,0:T(8,128)(2,1)S(1)}, u32[]{:S(2)}, u32[]{:S(2)}) collective-permute-start(bf16[192,512]{1,0:T(8,128)(2,1)S(1)} %get-tuple-element.52), channel_id=1, source_target_pairs={{0,1},{1,0},{2,3},{3,2},{4,5},{5,4},{6,7},{7,6},{8,9},{9,8},{10,11... | collective-permute-start | bytes 589832 | tf_op jit(solution)/shard_map/ppermute | solution.py:274
  74.3 6.3 %collective-permute-start.33 = (bf16[192,640]{1,0:T(8,128)(2,1)S(1)}, bf16[192,640]{1,0:T(8,128)(2,1)S(1)}, u32[]{:S(2)}, u32[]{:S(2)}) collective-permute-start(bf16[192,640]{1,0:T(8,128)(2,1)S(1)} %fusion.1), channel_id=1, source_target_pairs={{0,4},{2,6},{4,0},{6,2},{8,12},{10,14},{12,8},{14,10},{16,20},{18,... | collective-permute-start | bytes 737288 | tf_op jit(solution)/shard_map/ppermute | solution.py:268
  80.7 10.6 %collective-permute-start.36 = (bf16[48,1152]{1,0:T(8,128)(2,1)S(1)}, bf16[48,1152]{1,0:T(8,128)(2,1)S(1)}, u32[]{:S(2)}, u32[]{:S(2)}) collective-permute-start(bf16[48,1152]{1,0:T(8,128)(2,1)S(1)} %get-tuple-element.54), channel_id=1, source_target_pairs={{0,24},{2,26},{4,28},{6,30},{8,16},{10,18},{12,20},{14,22},{16,8},... | collective-permute-start | bytes 331784 | tf_op jit(solution)/shard_map/ppermute | solution.py:265
  84.3 7.2 %collective-permute-start.35 = (bf16[48,1152]{1,0:T(8,128)(2,1)S(1)}, bf16[48,1152]{1,0:T(8,128)(2,1)S(1)}, u32[]{:S(2)}, u32[]{:S(2)}) collective-permute-start(bf16[48,1152]{1,0:T(8,128)(2,1)S(1)} %get-tuple-element.55), channel_id=1, source_target_pairs={{0,16},{2,18},{4,20},{6,22},{8,24},{10,26},{12,28},{14,30},{16,0},... | collective-permute-start | bytes 331784 | tf_op jit(solution)/shard_map/ppermute | solution.py:265
  84.3 7.2 %collective-permute-start.34 = (bf16[48,1152]{1,0:T(8,128)(2,1)S(1)}, bf16[48,1152]{1,0:T(8,128)(2,1)S(1)}, u32[]{:S(2)}, u32[]{:S(2)}) collective-permute-start(bf16[48,1152]{1,0:T(8,128)(2,1)S(1)} %get-tuple-element.56), channel_id=1, source_target_pairs={{0,8},{2,10},{4,12},{6,14},{8,0},{10,2},{12,4},{14,6},{16,24},{18,... | collective-permute-start | bytes 331784 | tf_op jit(solution)/shard_map/ppermute | solution.py:265
  89.0 2.5 %copy-start.4 = (s32[128,2]{0,1:T(2,128)S(1)}, s32[128,2]{0,1:T(2,128)}, u32[]{:S(2)}) copy-start(s32[128,2]{0,1:T(2,128)} %param.14) | copy-start | bytes 3076
  89.0 2.5 %copy-start.5 = (f32[128,2]{0,1:T(2,128)S(1)}, f32[128,2]{0,1:T(2,128)}, u32[]{:S(2)}) copy-start(f32[128,2]{0,1:T(2,128)} %param.12) | copy-start | bytes 3076
  89.0 2.5 %copy-start.6 = (f32[128]{0:T(128)S(1)}, f32[128]{0:T(128)}, u32[]{:S(2)}) copy-start(f32[128]{0:T(128)} %param.11) | copy-start | bytes 1540

commit v4 on v3

--- a/solution.py
+++ b/solution.py
@@ -137,8 +137,11 @@
         part = stack([tok[c][j][...] for c in range(2)])
         gate = gate + dot(part, gate_w[spans[j], :], COLS_ROWS)
         up = up + dot(part, up_w[spans[j], :], COLS_ROWS)
-    out[:, :cols] = gate
-    out[:, cols:] = up
+    sigma = jax.nn.sigmoid(gate)
+    swish = gate * sigma
+    out[:, :cols] = swish
+    out[:, cols : 2 * cols] = swish * up
+    out[:, 2 * cols :] = up * sigma * (1.0 + gate * (1.0 - sigma))
 
 
 def main_body(lanes, width, *refs):
@@ -151,21 +154,17 @@
     mine = lax.axis_index("ep") % EPG
     spans = spans_of(lanes, width)
     lane = lax.broadcasted_iota(jnp.int32, (2 * rows, LANES), 1)
-    pre_gate = pre[:, :cols]
-    pre_up = pre[:, cols:]
     back = 0.0
     for j in range(lanes):
         part = stack([cot[c][j][:, :width] for c in range(2)])
         back = back + dot(part, down_w[:, spans[j]], ROWS_COLS)
     gates = stack([cot[c][0][:, width:] for c in range(2)]).astype(F32)
     gate = jnp.sum(jnp.where(lane == mine, gates, 0.0), axis=1, keepdims=True)
-    sigma = jax.nn.sigmoid(pre_gate)
-    swish = pre_gate * sigma
-    hidden = swish * pre_up
+    hidden = pre[:, cols : 2 * cols]
     gate_part = jnp.sum(hidden * back, axis=1, keepdims=True)
     scaled = gate * back
-    grad_gate = (scaled * pre_up * sigma * (1.0 + pre_gate * (1.0 - sigma))).astype(BF16)
-    grad_up = (scaled * swish).astype(BF16)
+    grad_gate = (scaled * pre[:, 2 * cols :]).astype(BF16)
+    grad_up = (scaled * pre[:, :cols]).astype(BF16)
     grads[:, :cols] = grad_gate
     grads[:, cols:] = grad_up
     scaled_hidden[...] = (gate * hidden).astype(BF16)
@@ -328,15 +327,34 @@
     def join(head, rest):
         return jnp.concatenate([head, rest], axis=0)
 
-    own_side = along_side(routed[0])
-    own_lane = [along_tp(routed[0][:, : 2 * width], j) for j in range(1, lanes)]
+    def along_mixed(a, flip):
+        pairs = []
+        for e in range(experts):
+            for r in range(lanes):
+                across = (e + flip) % 2
+                there = (e ^ 2) * lanes + r if across else e * lanes + (r + 1) % lanes
+                pairs.append((e * lanes + r, there))
+        return lax.ppermute(a, ("ep", "tp"), pairs)
+
     next_side = along_side(next_sent)
     next_lane = [along_tp(next_sent[:, : 2 * width], j) for j in range(1, lanes)]
+    if lanes == 2:
+        step = along_mixed(routed[0], 1)
+        steps = along_mixed(join(routed[0], step), 0)
+        own_side = jnp.where(core == 0, step, steps[:cap])
+        own_lane = [jnp.where(core == 0, steps[:cap], step)[:, : 2 * width]]
+        own_both = [steps[cap:, : 2 * width]]
+        next_both = along_diagonal(next_side[:, : 2 * width], next_lane)
+    else:
+        own_side = along_side(routed[0])
+        own_lane = [along_tp(routed[0][:, : 2 * width], j) for j in range(1, lanes)]
+        own_both = along_diagonal(own_side[:, : 2 * width], own_lane)
+        next_both = along_diagonal(next_side[:, : 2 * width], next_lane)
     own = join(routed[0], next_sent)
     own_side = join(own_side, next_side)
     own_lane = [join(a, b) for a, b in zip(own_lane, next_lane)]
+    own_both = [join(a, b) for a, b in zip(own_both, next_both)]
     cot_sent = {k: along_groups(routed[groups - 2 + k], k) for k in range(2, groups)}
-    own_both = along_diagonal(own_side[:, : 2 * width], own_lane)
     tok = jnp.concatenate([tok_sent[k] for k in range(2, groups)], axis=0)
     cot = jnp.concatenate([cot_sent[k] for k in range(2, groups)], axis=0)
     cot_bare = jnp.concatenate([cot_sent[k][:, :width] for k in range(2, groups)], axis=0)
@@ -366,7 +384,7 @@
         tok_other += [along_core(a) for a in tok_list[1:]]
         cot_other += [along_core(a) for a in cot_list[1:]]
         pre = call(
-            functools.partial(pre_body, lanes, width), shape((2 * size, 2 * cols), F32), 2 * work
+            functools.partial(pre_body, lanes, width), shape((2 * size, 3 * cols), F32), 2 * work
         )(*tok_list, *tok_other, first, second)
         outs = call(
             functools.partial(main_body, lanes, width),

time: 93 us -> 95.5 us (1.027)
  starting transfers between devices: 36.1 us -> 37.4 us
  waiting for transfers between devices: 37.1 us -> 38.2 us
    ppermute x0 -> x2, waiting for transfers between devices: none -> 4.45 us  [along_mixed(): return lax.ppermute(a, ('ep', 'tp'), pairs)]
    ppermute x7 -> x6, waiting for transfers between devices: 10.8 us -> 7.69 us  [along_side(): return lax.ppermute(a, 'ep', [(e, e ^ 2) for e in range(experts)])]
    ppermute x0 -> x2, starting transfers between devices: none -> 2.91 us  [along_mixed(): return lax.ppermute(a, ('ep', 'tp'), pairs)]
    ppermute x7 -> x6, waiting for transfers between devices: 13.3 us -> 11.4 us  [along_tp(): return lax.ppermute(a, 'tp', [(r, (r + j) % lanes) for r in range(lanes)])]
    ppermute x7 -> x6, starting transfers between devices: 8.18 us -> 6.37 us  [along_tp(): return lax.ppermute(a, 'tp', [(r, (r + j) % lanes) for r in range(lanes)])]
    ppermute x8, waiting for transfers between devices: 9.07 us -> 10.7 us  [along_groups(): return lax.ppermute(a, 'ep', [(e, e ^ k * EPG) for e in range(experts)])]
    ppermute x7 -> x6, starting transfers between devices: 8.04 us -> 8.42 us  [along_side(): return lax.ppermute(a, 'ep', [(e, e ^ 2) for e in range(experts)])]
  transfers between devices with their start and end apart: 37 -> 37, of which waited for: 13 -> 12; matrix products, arithmetic and copies ran while one was open for 2% -> 2% of each run, Pallas kernels for 15% -> 14%
where the time goes in v4:
time: 95.5 us; the launch traced here: 95.3 us
  waiting for transfers between devices  38.2 us (40%)
  starting transfers between devices  37.4 us (39%)
  Pallas kernels  16.7 us (17%)
  other arithmetic  1.33 us (1%)
  between operations  1.2 us (1%)
    pallas_call x14, Pallas kernels, run(): pl.pallas_call(body, out_shape=outs, in_specs=[pl.BlockSpec(memory_space=...  16.7 us
    ppermute x8, starting transfers between devices, along_groups(): return lax.ppermute(a, 'ep', [(e, e ^ k * EPG) for e in range(experts)])  13.1 us
    ppermute x6, waiting for transfers between devices, along_tp(): return lax.ppermute(a, 'tp', [(r, (r + j) % lanes) for r in range(lanes)])  11.4 us
    ppermute x8, waiting for transfers between devices, along_groups(): return lax.ppermute(a, 'ep', [(e, e ^ k * EPG) for e in range(experts)])  10.7 us
    ppermute x6, starting transfers between devices, along_side(): return lax.ppermute(a, 'ep', [(e, e ^ 2) for e in range(experts)])  8.42 us
    ppermute x6, waiting for transfers between devices, along_side(): return lax.ppermute(a, 'ep', [(e, e ^ 2) for e in range(experts)])  7.69 us
    ppermute x6, starting transfers between devices, along_tp(): return lax.ppermute(a, 'tp', [(r, (r + j) % lanes) for r in range(lanes)])  6.37 us
    ppermute x2, waiting for transfers between devices, along_mixed(): return lax.ppermute(a, ('ep', 'tp'), pairs)  4.45 us
  transfers between devices with their start and end apart: 37, of which 12 were waited for; matrix products, arithmetic and copies ran while one was open for 2% of the time, Pallas kernels for 14%

profile of v4, /device:TPU:0, one launch (start us, length us, event | category | flops | bytes accessed | tf_op | source)
XLA Modules:
  0.0 95.3 jit_solution(13373961148993879988)
XLA Ops:
  0.6 1.7 %shard_map.136 = (bf16[48,2176]{1,0:T(8,128)(2,1)S(1)}, bf16[48,2176]{1,0:T(8,128)(2,1)S(1)}, bf16[48,1024]{1,0:T(8,128)(2,1)S(1)}, bf16[48,1024]{1,0:T(8,128)(2...) custom-call(s32[1,128]{1,0:T(1,128)} %bitcast.26, s32[2,128]{1,0:T(2,128)} %bitcast.31, ...), custom_call_target="tpu_custom_call" | custom-call | tf_op jit(solution)/shard_map/pallas_call | solution.py:27
  2.3 4.1 %collective-permute-start.1 = (bf16[48,1024]{1,0:T(8,128)(2,1)S(1)}, bf16[48,1024]{1,0:T(8,128)(2,1)S(1)}, u32[]{:S(2)}, u32[]{:S(2)}) collective-permute-start(bf16[48,1024]{1,0:T(8,128)(2,1)S(1)} %get-tuple-element.31), channel_id=1, source_target_pairs={{0,16},{2,18},{4,20},{6,22},{8,24},{10,26},{12,28},{14,30},{16,0},... | collective-permute-start | bytes 294920 | tf_op jit(solution)/shard_map/ppermute | solution.py:264
  6.5 1.3 %collective-permute-start.2 = (bf16[48,1024]{1,0:T(8,128)(2,1)S(1)}, bf16[48,1024]{1,0:T(8,128)(2,1)S(1)}, u32[]{:S(2)}, u32[]{:S(2)}) collective-permute-start(bf16[48,1024]{1,0:T(8,128)(2,1)S(1)} %get-tuple-element.32), channel_id=1, source_target_pairs={{0,24},{2,26},{4,28},{6,30},{8,16},{10,18},{12,20},{14,22},{16,8},... | collective-permute-start | bytes 294920 | tf_op jit(solution)/shard_map/ppermute | solution.py:264
  7.8 1.7 %collective-permute-start.9 = (bf16[48,1152]{1,0:T(8,128)(2,1)S(1)}, bf16[48,1152]{1,0:T(8,128)(2,1)S(1)}, u32[]{:S(2)}, u32[]{:S(2)}) collective-permute-start(bf16[48,1152]{1,0:T(8,128)(2,1)S(1)} %get-tuple-element.33), channel_id=1, source_target_pairs={{0,16},{2,18},{4,20},{6,22},{8,24},{10,26},{12,28},{14,30},{16,0},... | collective-permute-start | bytes 331784 | tf_op jit(solution)/shard_map/ppermute | solution.py:264
  9.5 0.9 collective-permute-start.10
  10.4 1.5 %collective-permute-start.3 = (bf16[48,2176]{1,0:T(8,128)(2,1)S(1)}, bf16[48,2176]{1,0:T(8,128)(2,1)S(1)}, u32[]{:S(2)}, u32[]{:S(2)}) collective-permute-start(bf16[48,2176]{1,0:T(8,128)(2,1)S(1)} %get-tuple-element.29), channel_id=1, source_target_pairs={{0,4},{1,5},{2,3},{3,2},{4,0},{5,1},{6,7},{7,6},{8,12},{9,13},{10,... | collective-permute-start | bytes 626696 | tf_op jit(solution)/shard_map/ppermute | solution.py:337
  11.9 7.1 %collective-permute-done.1 = bf16[48,1024]{1,0:T(8,128)(2,1)S(1)} collective-permute-done((bf16[48,1024]{1,0:T(8,128)(2,1)S(1)}, bf16[48,1024]{1,0:T(8,128)(2,1)S(1)}, u32[]{:S(2)}, u32[]{:S(2)}) %collective-permute-start.1) | collective-permute-done | bytes 98336 | tf_op jit(solution)/shard_map/ppermute | solution.py:264
  19.1 1.7 %collective-permute-start.16 = (bf16[96,1024]{1,0:T(8,128)(2,1)S(1)}, bf16[96,1024]{1,0:T(8,128)(2,1)S(1)}, u32[]{:S(2)}, u32[]{:S(2)}) collective-permute-start(bf16[96,1024]{1,0:T(8,128)(2,1)S(1)} %constant_dynamic-update-slice_fusion.2), channel_id=1, source_target_pairs={{0,4},{2,6},{4,0},{6,2},{8,12},{10,14},{12,8},{14,10},{16,20},{18,... | collective-permute-start | bytes 589832 | tf_op jit(solution)/shard_map/ppermute | solution.py:267
  20.8 2.7 %collective-permute-done.9 = bf16[48,1152]{1,0:T(8,128)(2,1)S(1)} collective-permute-done((bf16[48,1152]{1,0:T(8,128)(2,1)S(1)}, bf16[48,1152]{1,0:T(8,128)(2,1)S(1)}, u32[]{:S(2)}, u32[]{:S(2)}) %collective-permute-start.9) | collective-permute-done | bytes 110624 | tf_op jit(solution)/shard_map/ppermute | solution.py:264
  23.5 1.7 %collective-permute-start.6 = (bf16[96,1024]{1,0:T(8,128)(2,1)S(1)}, bf16[96,1024]{1,0:T(8,128)(2,1)S(1)}, u32[]{:S(2)}, u32[]{:S(2)}) collective-permute-start(bf16[96,1024]{1,0:T(8,128)(2,1)S(1)} %constant_dynamic-update-slice_fusion.2), channel_id=1, source_target_pairs={{0,1},{1,0},{2,3},{3,2},{4,5},{5,4},{6,7},{7,6},{8,9},{9,8},{10,11... | collective-permute-start | bytes 589832 | tf_op jit(solution)/shard_map/ppermute | solution.py:273
  25.3 0.4 collective-permute-start.11
  25.7 0.9 collective-permute-done
  26.6 1.3 %collective-permute-start.21 = (bf16[96,1152]{1,0:T(8,128)(2,1)S(1)}, bf16[96,1152]{1,0:T(8,128)(2,1)S(1)}, u32[]{:S(2)}, u32[]{:S(2)}) collective-permute-start(bf16[96,1152]{1,0:T(8,128)(2,1)S(1)} %pad_maximum_fusion.9), channel_id=1, source_target_pairs={{0,4},{2,6},{4,0},{6,2},{8,12},{10,14},{12,8},{14,10},{16,20},{18,... | collective-permute-start | bytes 663560 | tf_op jit(solution)/shard_map/ppermute | solution.py:267
  28.0 1.6 %collective-permute-start.5 = (bf16[48,2048]{1,0:T(8,128)(2,1)S(1)}, bf16[48,2048]{1,0:T(8,128)(2,1)S(1)}, u32[]{:S(2)}, u32[]{:S(2)}) collective-permute-start(bf16[48,2048]{1,0:T(8,128)(2,1)S(1)} %slice.150), channel_id=1, source_target_pairs={{0,1},{1,0},{2,3},{3,2},{4,5},{5,4},{6,7},{7,6},{8,9},{9,8},{10,11... | collective-permute-start | bytes 589832 | tf_op jit(solution)/shard_map/ppermute | solution.py:273
  29.8 1.5 %collective-permute-done.6 = bf16[96,1024]{1,0:T(8,128)(2,1)S(1)} collective-permute-done((bf16[96,1024]{1,0:T(8,128)(2,1)S(1)}, bf16[96,1024]{1,0:T(8,128)(2,1)S(1)}, u32[]{:S(2)}, u32[]{:S(2)}) %collective-permute-start.6) | collective-permute-done | bytes 196640 | tf_op jit(solution)/shard_map/ppermute | solution.py:273
  31.3 1.7 %collective-permute-start.15 = (bf16[48,2176]{1,0:T(8,128)(2,1)S(1)}, bf16[48,2176]{1,0:T(8,128)(2,1)S(1)}, u32[]{:S(2)}, u32[]{:S(2)}) collective-permute-start(bf16[48,2176]{1,0:T(8,128)(2,1)S(1)} %collective-permute-done), channel_id=1, source_target_pairs={{0,4},{2,6},{4,0},{6,2},{8,12},{10,14},{12,8},{14,10},{16,20},{18,... | collective-permute-start | bytes 626696 | tf_op jit(solution)/shard_map/ppermute | solution.py:267
  33.0 4.2 %collective-permute-done.5 = bf16[48,2048]{1,0:T(8,128)(2,1)S(1)} collective-permute-done((bf16[48,2048]{1,0:T(8,128)(2,1)S(1)}, bf16[48,2048]{1,0:T(8,128)(2,1)S(1)}, u32[]{:S(2)}, u32[]{:S(2)}) %collective-permute-start.5) | collective-permute-done | bytes 196640 | tf_op jit(solution)/shard_map/ppermute | solution.py:273
  37.2 1.4 %collective-permute-start.4 = (bf16[96,2176]{1,0:T(8,128)(2,1)S(1)}, bf16[96,2176]{1,0:T(8,128)(2,1)S(1)}, u32[]{:S(2)}, u32[]{:S(2)}) collective-permute-start(bf16[96,2176]{1,0:T(8,128)(2,1)S(1)} %pad_maximum_fusion.2), channel_id=1, source_target_pairs={{0,1},{1,0},{2,6},{3,7},{4,5},{5,4},{6,2},{7,3},{8,9},{9,8},{10,14... | collective-permute-start | bytes 1253384 | tf_op jit(solution)/shard_map/ppermute | solution.py:337
  38.6 0.7 collective-permute-start.18
  39.3 1.4 %collective-permute-start.17 = (bf16[48,2048]{1,0:T(8,128)(2,1)S(1)}, bf16[48,2048]{1,0:T(8,128)(2,1)S(1)}, u32[]{:S(2)}, u32[]{:S(2)}) collective-permute-start(bf16[48,2048]{1,0:T(8,128)(2,1)S(1)} %slice_select_fusion.1), channel_id=1, source_target_pairs={{0,1},{1,0},{2,6},{3,7},{4,5},{5,4},{6,2},{7,3},{8,9},{9,8},{10,14... | collective-permute-start | bytes 589832 | tf_op jit(solution)/shard_map/ppermute | solution.py:285
  40.8 4.4 %collective-permute-done.4 = bf16[96,2176]{1,0:T(8,128)(2,1)S(1)} collective-permute-done((bf16[96,2176]{1,0:T(8,128)(2,1)S(1)}, bf16[96,2176]{1,0:T(8,128)(2,1)S(1)}, u32[]{:S(2)}, u32[]{:S(2)}) %collective-permute-start.4) | collective-permute-done | bytes 417824 | tf_op jit(solution)/shard_map/ppermute | solution.py:337
  45.2 1.4 %collective-permute-start.22 = (bf16[96,1024]{1,0:T(8,128)(2,1)S(1)}, bf16[96,1024]{1,0:T(8,128)(2,1)S(1)}, u32[]{:S(2)}, u32[]{:S(2)}) collective-permute-start(bf16[96,1024]{1,0:T(8,128)(2,1)S(1)} %slice_select_fusion), channel_id=1, source_target_pairs={{0,1},{1,0},{2,6},{3,7},{4,5},{5,4},{6,2},{7,3},{8,9},{9,8},{10,14... | collective-permute-start | bytes 589832 | tf_op jit(solution)/shard_map/ppermute | solution.py:285
  46.6 2.8 %collective-permute-done.17 = bf16[48,2048]{1,0:T(8,128)(2,1)S(1)} collective-permute-done((bf16[48,2048]{1,0:T(8,128)(2,1)S(1)}, bf16[48,2048]{1,0:T(8,128)(2,1)S(1)}, u32[]{:S(2)}, u32[]{:S(2)}) %collective-permute-start.17) | collective-permute-done | bytes 196640 | tf_op jit(solution)/shard_map/ppermute | solution.py:285
  49.7 0.6 collective-permute-start.8
  50.4 1.2 %collective-permute-done.22 = bf16[96,1024]{1,0:T(8,128)(2,1)S(1)} collective-permute-done((bf16[96,1024]{1,0:T(8,128)(2,1)S(1)}, bf16[96,1024]{1,0:T(8,128)(2,1)S(1)}, u32[]{:S(2)}, u32[]{:S(2)}) %collective-permute-start.22) | collective-permute-done | bytes 196640 | tf_op jit(solution)/shard_map/ppermute | solution.py:285
  51.6 0.6 collective-permute-start.24
  52.2 0.1 collective-permute-start.19
  52.3 0.4 collective-permute-start.23
  52.7 1.0 %shard_map.137.refs_0_ = f32[384,768]{1,0:T(8,128)S(1)} custom-call(bf16[192,1024]{1,0:T(8,128)(2,1)S(1)} %pad_maximum_fusion.6.refs_0_, bf16[192,1024]{1,0:T(8,128)(2,1)S(1)} %pad_maximum_fusion.7.refs_1_, bf16[192,1024]{1,0:T(8,128)(2,1)S(1)} %collective-permute-done.7.refs_2_, bf16[192,1024]{1,0:T(8,128)(2,1)S(1)} %collective-permute-done.8.refs_3_, ...), custom_call_target="tpu_custom_call" | custom-call | flops 805306368 | tf_op jit(solution)/shard_map/pallas_call | solution.py:27
  53.8 0.2 copy-done.2
  53.9 1.8 %shard_map.138 = (f32[192,1152]{1,0:T(8,128)S(1)}, bf16[192,1152]{1,0:T(8,128)(2,1)S(1)}, bf16[384,512]{1,0:T(8,128)(2,1)S(1)}, bf16[384,256]{1,0:T(8,128)(2,1)S(1)}) custom-call(f32[384,768]{1,0:T(8,128)S(1)} %shard_map.137.refs_0_, bf16[192,1152]{1,0:T(8,128)(2,1)S(1)} %pad_maximum_fusion.1.refs_1_.refs_0_, bf16[192,1024]{1,0:T(8,128)(2,1)S(1)} %fusion.8.refs_2_.refs_1_, ...), custom_call_target="tpu_custom_call" | custom-call | flops 805306368 | tf_op jit(solution)/shard_map/pallas_call | solution.py:27
  55.8 0.6 shard_map.139
  56.4 0.2 collective-permute-start.14
  56.6 0.1 shard_map.146.refs_7_
  56.7 0.1 shard_map.145.refs_6_
  56.9 0.1 shard_map.144.refs_5_
  57.0 0.1 shard_map.143.refs_4_
  57.2 0.5 collective-permute-start.27
  57.7 1.0 %shard_map.140.refs_0_ = f32[384,768]{1,0:T(8,128)S(1)} custom-call(bf16[192,1024]{1,0:T(8,128)(2,1)S(1)} %fusion.7.refs_0_.refs_4_, bf16[192,1024]{1,0:T(8,128)(2,1)S(1)} %pad_maximum_fusion.8.refs_1_.refs_5_, bf16[192,1024]{1,0:T(8,128)(2,1)S(1)} %collective-permute-done.19.refs_2_.refs_6_, bf16[192,1024]{1,0:T(8,128)(2,1)S(1)} %collective-permute-done.20.refs_3_.refs_7_, ...), custom_call_target="tpu_custom_call" | custom-call | flops 805306368 | tf_op jit(solution)/shard_map/pallas_call | solution.py:27
  58.7 1.9 %shard_map.141 = (f32[192,1152]{1,0:T(8,128)S(1)}, bf16[192,1152]{1,0:T(8,128)(2,1)S(1)}, bf16[384,512]{1,0:T(8,128)(2,1)S(1)}, bf16[384,256]{1,0:T(8,128)(2,1)S(1)}) custom-call(f32[384,768]{1,0:T(8,128)S(1)} %shard_map.140.refs_0_, bf16[192,1152]{1,0:T(8,128)(2,1)S(1)} %fusion.5.refs_1_.refs_4_, bf16[192,1024]{1,0:T(8,128)(2,1)S(1)} %fusion.6.refs_2_.refs_5_, ...), custom_call_target="tpu_custom_call" | custom-call | flops 805306368 | tf_op jit(solution)/shard_map/pallas_call | solution.py:27
  60.6 0.2 collective-permute-start.28
  60.7 0.6 shard_map.142
  61.3 0.5 collective-permute-start.25
  61.8 0.1 convert_add_fusion.2
  61.9 0.1 convert_add_fusion
  62.1 1.5 %collective-permute-start.31 = (bf16[192,640]{1,0:T(8,128)(2,1)S(1)}, bf16[192,640]{1,0:T(8,128)(2,1)S(1)}, u32[]{:S(2)}, u32[]{:S(2)}) collective-permute-start(bf16[192,640]{1,0:T(8,128)(2,1)S(1)} %slice.219), channel_id=1, source_target_pairs={{0,1},{1,0},{2,3},{3,2},{4,5},{5,4},{6,7},{7,6},{8,9},{9,8},{10,11... | collective-permute-start | bytes 737288 | tf_op jit(solution)/shard_map/ppermute | solution.py:273
  63.6 0.1 add_convert_fusion
  63.8 1.6 %collective-permute-start.29 = (bf16[192,512]{1,0:T(8,128)(2,1)S(1)}, bf16[192,512]{1,0:T(8,128)(2,1)S(1)}, u32[]{:S(2)}, u32[]{:S(2)}) collective-permute-start(bf16[192,512]{1,0:T(8,128)(2,1)S(1)} %pad_maximum_fusion.11), channel_id=1, source_target_pairs={{0,4},{2,6},{4,0},{6,2},{8,12},{10,14},{12,8},{14,10},{16,20},{18,... | collective-permute-start | bytes 589832 | tf_op jit(solution)/shard_map/ppermute | solution.py:267
  65.3 0.5 collective-permute-start.32
  65.9 0.1 convert_add_fusion.1
  66.0 0.7 collective-permute-start.26
  66.7 5.0 %collective-permute-done.29 = bf16[192,512]{1,0:T(8,128)(2,1)S(1)} collective-permute-done((bf16[192,512]{1,0:T(8,128)(2,1)S(1)}, bf16[192,512]{1,0:T(8,128)(2,1)S(1)}, u32[]{:S(2)}, u32[]{:S(2)}) %collective-permute-start.29) | collective-permute-done | bytes 196640 | tf_op jit(solution)/shard_map/ppermute | solution.py:267
  71.7 0.7 collective-permute-start.30
  72.3 3.9 %collective-permute-done.32 = bf16[192,640]{1,0:T(8,128)(2,1)S(1)} collective-permute-done((bf16[192,640]{1,0:T(8,128)(2,1)S(1)}, bf16[192,640]{1,0:T(8,128)(2,1)S(1)}, u32[]{:S(2)}, u32[]{:S(2)}) %collective-permute-start.32) | collective-permute-done | bytes 245792 | tf_op jit(solution)/shard_map/ppermute | solution.py:273
  76.3 1.5 %collective-permute-start.33 = (bf16[192,640]{1,0:T(8,128)(2,1)S(1)}, bf16[192,640]{1,0:T(8,128)(2,1)S(1)}, u32[]{:S(2)}, u32[]{:S(2)}) collective-permute-start(bf16[192,640]{1,0:T(8,128)(2,1)S(1)} %fusion.1), channel_id=1, source_target_pairs={{0,4},{2,6},{4,0},{6,2},{8,12},{10,14},{12,8},{14,10},{16,20},{18,... | collective-permute-start | bytes 737288 | tf_op jit(solution)/shard_map/ppermute | solution.py:267
  77.8 1.8 %collective-permute-done.30 = bf16[192,512]{1,0:T(8,128)(2,1)S(1)} collective-permute-done((bf16[192,512]{1,0:T(8,128)(2,1)S(1)}, bf16[192,512]{1,0:T(8,128)(2,1)S(1)}, u32[]{:S(2)}, u32[]{:S(2)}) %collective-permute-start.30) | collective-permute-done | bytes 196640 | tf_op jit(solution)/shard_map/ppermute | solution.py:273
  79.7 0.1 fusion.12
  79.9 2.7 %collective-permute-done.33 = bf16[192,640]{1,0:T(8,128)(2,1)S(1)} collective-permute-done((bf16[192,640]{1,0:T(8,128)(2,1)S(1)}, bf16[192,640]{1,0:T(8,128)(2,1)S(1)}, u32[]{:S(2)}, u32[]{:S(2)}) %collective-permute-start.33) | collective-permute-done | bytes 245792 | tf_op jit(solution)/shard_map/ppermute | solution.py:267
  82.6 0.1 fusion.3
  82.8 4.4 %collective-permute-start.36 = (bf16[48,1152]{1,0:T(8,128)(2,1)S(1)}, bf16[48,1152]{1,0:T(8,128)(2,1)S(1)}, u32[]{:S(2)}, u32[]{:S(2)}) collective-permute-start(bf16[48,1152]{1,0:T(8,128)(2,1)S(1)} %get-tuple-element.54), channel_id=1, source_target_pairs={{0,24},{2,26},{4,28},{6,30},{8,16},{10,18},{12,20},{14,22},{16,8},... | collective-permute-start | bytes 331784 | tf_op jit(solution)/shard_map/ppermute | solution.py:264
  87.1 0.6 collective-permute-start.34
  87.8 3.8 %shard_map.148 = (f32[2048,256]{1,0:T(8,128)}, f32[2048,256]{1,0:T(8,128)}) custom-call(bf16[192,1024]{1,0:T(8,128)(2,1)S(1)} %pad_maximum_fusion.6.refs_0_, bf16[192,1024]{1,0:T(8,128)(2,1)S(1)} %pad_maximum_fusion.7.refs_1_, bf16[192,1024]{1,0:T(8,128)(2,1)S(1)} %collective-permute-done.7.refs_2_, bf16[192,1024]{1,0:T(8,128)(2,1)S(1)} %collective-permute-done.8.refs_3_, ...), custom_call_target="tpu_custom_call" | custom-call | flops 1610612736 | tf_op jit(solution)/shard_map/pallas_call | solution.py:27
  91.6 2.3 %shard_map.149 = f32[256,2048]{1,0:T(8,128)} custom-call(bf16[192,1152]{1,0:T(8,128)(2,1)S(1)} %pad_maximum_fusion.1.refs_1_.refs_0_, bf16[192,1024]{1,0:T(8,128)(2,1)S(1)} %fusion.8.refs_2_.refs_1_, bf16[192,1152]{1,0:T(8,128)(2,1)S(1)} %collective-permute-done.12.refs_3_.refs_2_, bf16[192,1024]{1,0:T(8,128)(2,1)S(1)} %collective-permute-done.13.refs_4_.refs_3_, ...), custom_call_target="tpu_custom_call" | custom-call | flops 805306368 | tf_op jit(solution)/shard_map/pallas_call | solution.py:27
  94.0 1.3 %shard_map.147 = (f32[128,1024]{1,0:T(8,128)}, f32[1,128]{1,0:T(1,128)}, f32[2,128]{1,0:T(2,128)}) custom-call(bf16[48,1152]{1,0:T(8,128)(2,1)S(1)} %get-tuple-element.57.refs_0_, bf16[48,1152]{1,0:T(8,128)(2,1)S(1)} %collective-permute-done.34.refs_1_, bf16[48,1152]{1,0:T(8,128)(2,1)S(1)} %collective-permute-done.35.refs_2_, ...), custom_call_target="tpu_custom_call" | custom-call | tf_op jit(solution)/shard_map/pallas_call | solution.py:27
  (91 shorter events, 1.3 us)
Async XLA Ops:
  2.3 16.7 %collective-permute-start.1 = (bf16[48,1024]{1,0:T(8,128)(2,1)S(1)}, bf16[48,1024]{1,0:T(8,128)(2,1)S(1)}, u32[]{:S(2)}, u32[]{:S(2)}) collective-permute-start(bf16[48,1024]{1,0:T(8,128)(2,1)S(1)} %get-tuple-element.31), channel_id=1, source_target_pairs={{0,16},{2,18},{4,20},{6,22},{8,24},{10,26},{12,28},{14,30},{16,0},... | collective-permute-start | bytes 294920 | tf_op jit(solution)/shard_map/ppermute | solution.py:264
  6.5 12.6 %collective-permute-start.2 = (bf16[48,1024]{1,0:T(8,128)(2,1)S(1)}, bf16[48,1024]{1,0:T(8,128)(2,1)S(1)}, u32[]{:S(2)}, u32[]{:S(2)}) collective-permute-start(bf16[48,1024]{1,0:T(8,128)(2,1)S(1)} %get-tuple-element.32), channel_id=1, source_target_pairs={{0,24},{2,26},{4,28},{6,30},{8,16},{10,18},{12,20},{14,22},{16,8},... | collective-permute-start | bytes 294920 | tf_op jit(solution)/shard_map/ppermute | solution.py:264
  7.8 15.7 %collective-permute-start.9 = (bf16[48,1152]{1,0:T(8,128)(2,1)S(1)}, bf16[48,1152]{1,0:T(8,128)(2,1)S(1)}, u32[]{:S(2)}, u32[]{:S(2)}) collective-permute-start(bf16[48,1152]{1,0:T(8,128)(2,1)S(1)} %get-tuple-element.33), channel_id=1, source_target_pairs={{0,16},{2,18},{4,20},{6,22},{8,24},{10,26},{12,28},{14,30},{16,0},... | collective-permute-start | bytes 331784 | tf_op jit(solution)/shard_map/ppermute | solution.py:264
  9.5 15.8 %collective-permute-start.10 = (bf16[48,1152]{1,0:T(8,128)(2,1)S(1)}, bf16[48,1152]{1,0:T(8,128)(2,1)S(1)}, u32[]{:S(2)}, u32[]{:S(2)}) collective-permute-start(bf16[48,1152]{1,0:T(8,128)(2,1)S(1)} %get-tuple-element.34), channel_id=1, source_target_pairs={{0,24},{2,26},{4,28},{6,30},{8,16},{10,18},{12,20},{14,22},{16,8},... | collective-permute-start | bytes 331784 | tf_op jit(solution)/shard_map/ppermute | solution.py:264
  10.4 17.6 %collective-permute-start.3 = (bf16[48,2176]{1,0:T(8,128)(2,1)S(1)}, bf16[48,2176]{1,0:T(8,128)(2,1)S(1)}, u32[]{:S(2)}, u32[]{:S(2)}) collective-permute-start(bf16[48,2176]{1,0:T(8,128)(2,1)S(1)} %get-tuple-element.29), channel_id=1, source_target_pairs={{0,4},{1,5},{2,3},{3,2},{4,0},{5,1},{6,7},{7,6},{8,12},{9,13},{10,... | collective-permute-start | bytes 626696 | tf_op jit(solution)/shard_map/ppermute | solution.py:337
  19.1 7.5 %collective-permute-start = (bf16[48,2176]{1,0:T(8,128)(2,1)S(1)}, bf16[48,2176]{1,0:T(8,128)(2,1)S(1)}, u32[]{:S(2)}, u32[]{:S(2)}) collective-permute-start(bf16[48,2176]{1,0:T(8,128)(2,1)S(1)} %get-tuple-element.30), channel_id=1, source_target_pairs={{0,8},{2,10},{4,12},{6,14},{8,0},{10,2},{12,4},{14,6},{16,24},{18,... | collective-permute-start | bytes 626696 | tf_op jit(solution)/shard_map/ppermute | solution.py:264
  19.1 10.6 %collective-permute-start.16 = (bf16[96,1024]{1,0:T(8,128)(2,1)S(1)}, bf16[96,1024]{1,0:T(8,128)(2,1)S(1)}, u32[]{:S(2)}, u32[]{:S(2)}) collective-permute-start(bf16[96,1024]{1,0:T(8,128)(2,1)S(1)} %constant_dynamic-update-slice_fusion.2), channel_id=1, source_target_pairs={{0,4},{2,6},{4,0},{6,2},{8,12},{10,14},{12,8},{14,10},{16,20},{18,... | collective-permute-start | bytes 589832 | tf_op jit(solution)/shard_map/ppermute | solution.py:267
  23.5 7.8 %collective-permute-start.6 = (bf16[96,1024]{1,0:T(8,128)(2,1)S(1)}, bf16[96,1024]{1,0:T(8,128)(2,1)S(1)}, u32[]{:S(2)}, u32[]{:S(2)}) collective-permute-start(bf16[96,1024]{1,0:T(8,128)(2,1)S(1)} %constant_dynamic-update-slice_fusion.2), channel_id=1, source_target_pairs={{0,1},{1,0},{2,3},{3,2},{4,5},{5,4},{6,7},{7,6},{8,9},{9,8},{10,11... | collective-permute-start | bytes 589832 | tf_op jit(solution)/shard_map/ppermute | solution.py:273
  25.3 13.3 %collective-permute-start.11 = (bf16[96,1024]{1,0:T(8,128)(2,1)S(1)}, bf16[96,1024]{1,0:T(8,128)(2,1)S(1)}, u32[]{:S(2)}, u32[]{:S(2)}) collective-permute-start(bf16[96,1024]{1,0:T(8,128)(2,1)S(1)} %pad_maximum_fusion.10), channel_id=1, source_target_pairs={{0,1},{1,0},{2,3},{3,2},{4,5},{5,4},{6,7},{7,6},{8,9},{9,8},{10,11... | collective-permute-start | bytes 589832 | tf_op jit(solution)/shard_map/ppermute | solution.py:273
  26.6 12.7 %collective-permute-start.21 = (bf16[96,1152]{1,0:T(8,128)(2,1)S(1)}, bf16[96,1152]{1,0:T(8,128)(2,1)S(1)}, u32[]{:S(2)}, u32[]{:S(2)}) collective-permute-start(bf16[96,1152]{1,0:T(8,128)(2,1)S(1)} %pad_maximum_fusion.9), channel_id=1, source_target_pairs={{0,4},{2,6},{4,0},{6,2},{8,12},{10,14},{12,8},{14,10},{16,20},{18,... | collective-permute-start | bytes 663560 | tf_op jit(solution)/shard_map/ppermute | solution.py:267
  28.0 9.2 %collective-permute-start.5 = (bf16[48,2048]{1,0:T(8,128)(2,1)S(1)}, bf16[48,2048]{1,0:T(8,128)(2,1)S(1)}, u32[]{:S(2)}, u32[]{:S(2)}) collective-permute-start(bf16[48,2048]{1,0:T(8,128)(2,1)S(1)} %slice.150), channel_id=1, source_target_pairs={{0,1},{1,0},{2,3},{3,2},{4,5},{5,4},{6,7},{7,6},{8,9},{9,8},{10,11... | collective-permute-start | bytes 589832 | tf_op jit(solution)/shard_map/ppermute | solution.py:273
  29.7 21.9 %collective-permute-start.7 = (bf16[192,1024]{1,0:T(8,128)(2,1)S(1)}, bf16[192,1024]{1,0:T(8,128)(2,1)S(1)}, u32[]{:S(2)}, u32[]{:S(2)}) collective-permute-start(bf16[192,1024]{1,0:T(8,128)(2,1)S(1)} %pad_maximum_fusion.6.refs_0_), channel_id=1, source_target_pairs={{0,2},{2,0},{4,6},{6,4},{8,10},{10,8},{12,14},{14,12},{16,18},{18,... | collective-permute-start | bytes 1179656 | tf_op jit(solution)/shard_map/ppermute | solution.py:270
  31.3 7.3 %collective-permute-start.15 = (bf16[48,2176]{1,0:T(8,128)(2,1)S(1)}, bf16[48,2176]{1,0:T(8,128)(2,1)S(1)}, u32[]{:S(2)}, u32[]{:S(2)}) collective-permute-start(bf16[48,2176]{1,0:T(8,128)(2,1)S(1)} %collective-permute-done), channel_id=1, source_target_pairs={{0,4},{2,6},{4,0},{6,2},{8,12},{10,14},{12,8},{14,10},{16,20},{18,... | collective-permute-start | bytes 626696 | tf_op jit(solution)/shard_map/ppermute | solution.py:267
  37.2 8.0 %collective-permute-start.4 = (bf16[96,2176]{1,0:T(8,128)(2,1)S(1)}, bf16[96,2176]{1,0:T(8,128)(2,1)S(1)}, u32[]{:S(2)}, u32[]{:S(2)}) collective-permute-start(bf16[96,2176]{1,0:T(8,128)(2,1)S(1)} %pad_maximum_fusion.2), channel_id=1, source_target_pairs={{0,1},{1,0},{2,6},{3,7},{4,5},{5,4},{6,2},{7,3},{8,9},{9,8},{10,14... | collective-permute-start | bytes 1253384 | tf_op jit(solution)/shard_map/ppermute | solution.py:337
  38.6 13.6 %collective-permute-start.12 = (bf16[192,1152]{1,0:T(8,128)(2,1)S(1)}, bf16[192,1152]{1,0:T(8,128)(2,1)S(1)}, u32[]{:S(2)}, u32[]{:S(2)}) collective-permute-start(bf16[192,1152]{1,0:T(8,128)(2,1)S(1)} %pad_maximum_fusion.1.refs_1_.refs_0_), channel_id=1, source_target_pairs={{0,2},{2,0},{4,6},{6,4},{8,10},{10,8},{12,14},{14,12},{16,18},{18,... | collective-permute-start | bytes 1327112 | tf_op jit(solution)/shard_map/ppermute | solution.py:270
  38.6 10.8 %collective-permute-start.18 = (bf16[96,1024]{1,0:T(8,128)(2,1)S(1)}, bf16[96,1024]{1,0:T(8,128)(2,1)S(1)}, u32[]{:S(2)}, u32[]{:S(2)}) collective-permute-start(bf16[96,1024]{1,0:T(8,128)(2,1)S(1)} %broadcast_select_fusion.1), channel_id=1, source_target_pairs={{0,1},{1,0},{2,6},{3,7},{4,5},{5,4},{6,2},{7,3},{8,9},{9,8},{10,14... | collective-permute-start | bytes 589832 | tf_op jit(solution)/shard_map/ppermute | solution.py:285
  39.3 10.1 %collective-permute-start.17 = (bf16[48,2048]{1,0:T(8,128)(2,1)S(1)}, bf16[48,2048]{1,0:T(8,128)(2,1)S(1)}, u32[]{:S(2)}, u32[]{:S(2)}) collective-permute-start(bf16[48,2048]{1,0:T(8,128)(2,1)S(1)} %slice_select_fusion.1), channel_id=1, source_target_pairs={{0,1},{1,0},{2,6},{3,7},{4,5},{5,4},{6,2},{7,3},{8,9},{9,8},{10,14... | collective-permute-start | bytes 589832 | tf_op jit(solution)/shard_map/ppermute | solution.py:285
  45.2 6.3 %collective-permute-start.22 = (bf16[96,1024]{1,0:T(8,128)(2,1)S(1)}, bf16[96,1024]{1,0:T(8,128)(2,1)S(1)}, u32[]{:S(2)}, u32[]{:S(2)}) collective-permute-start(bf16[96,1024]{1,0:T(8,128)(2,1)S(1)} %slice_select_fusion), channel_id=1, source_target_pairs={{0,1},{1,0},{2,6},{3,7},{4,5},{5,4},{6,2},{7,3},{8,9},{9,8},{10,14... | collective-permute-start | bytes 589832 | tf_op jit(solution)/shard_map/ppermute | solution.py:285
  49.5 7.7 %collective-permute-start.20 = (bf16[192,1024]{1,0:T(8,128)(2,1)S(1)}, bf16[192,1024]{1,0:T(8,128)(2,1)S(1)}, u32[]{:S(2)}, u32[]{:S(2)}) collective-permute-start(bf16[192,1024]{1,0:T(8,128)(2,1)S(1)} %pad_maximum_fusion.8.refs_1_.refs_5_), channel_id=1, source_target_pairs={{0,2},{2,0},{4,6},{6,4},{8,10},{10,8},{12,14},{14,12},{16,18},{18,... | collective-permute-start | bytes 1179656 | tf_op jit(solution)/shard_map/ppermute | solution.py:270
  49.7 3.0 %copy-start = (bf16[1,2048,256]{2,1,0:T(8,128)(2,1)S(1)}, bf16[1,2048,256]{2,1,0:T(8,128)(2,1)}, u32[]{:S(2)}) copy-start(bf16[1,2048,256]{2,1,0:T(8,128)(2,1)} %param.15) | copy-start | bytes 3145732
  49.7 3.0 %copy-start.1 = (bf16[1,2048,256]{2,1,0:T(8,128)(2,1)S(1)}, bf16[1,2048,256]{2,1,0:T(8,128)(2,1)}, u32[]{:S(2)}) copy-start(bf16[1,2048,256]{2,1,0:T(8,128)(2,1)} %param.16) | copy-start | bytes 3145732
  49.7 2.6 %collective-permute-start.8 = (bf16[192,1024]{1,0:T(8,128)(2,1)S(1)}, bf16[192,1024]{1,0:T(8,128)(2,1)S(1)}, u32[]{:S(2)}, u32[]{:S(2)}) collective-permute-start(bf16[192,1024]{1,0:T(8,128)(2,1)S(1)} %pad_maximum_fusion.7.refs_1_), channel_id=1, source_target_pairs={{0,2},{2,0},{4,6},{6,4},{8,10},{10,8},{12,14},{14,12},{16,18},{18,... | collective-permute-start | bytes 1179656 | tf_op jit(solution)/shard_map/ppermute | solution.py:270
  51.5 2.2 %collective-permute-start.13 = (bf16[192,1024]{1,0:T(8,128)(2,1)S(1)}, bf16[192,1024]{1,0:T(8,128)(2,1)S(1)}, u32[]{:S(2)}, u32[]{:S(2)}) collective-permute-start(bf16[192,1024]{1,0:T(8,128)(2,1)S(1)} %fusion.8.refs_2_.refs_1_), channel_id=1, source_target_pairs={{0,2},{2,0},{4,6},{6,4},{8,10},{10,8},{12,14},{14,12},{16,18},{18,... | collective-permute-start | bytes 1179656 | tf_op jit(solution)/shard_map/ppermute | solution.py:270
  51.6 7.1 %collective-permute-start.24 = (bf16[192,1024]{1,0:T(8,128)(2,1)S(1)}, bf16[192,1024]{1,0:T(8,128)(2,1)S(1)}, u32[]{:S(2)}, u32[]{:S(2)}) collective-permute-start(bf16[192,1024]{1,0:T(8,128)(2,1)S(1)} %fusion.6.refs_2_.refs_5_), channel_id=1, source_target_pairs={{0,2},{2,0},{4,6},{6,4},{8,10},{10,8},{12,14},{14,12},{16,18},{18,... | collective-permute-start | bytes 1179656 | tf_op jit(solution)/shard_map/ppermute | solution.py:270
  52.2 5.5 %collective-permute-start.19 = (bf16[192,1024]{1,0:T(8,128)(2,1)S(1)}, bf16[192,1024]{1,0:T(8,128)(2,1)S(1)}, u32[]{:S(2)}, u32[]{:S(2)}) collective-permute-start(bf16[192,1024]{1,0:T(8,128)(2,1)S(1)} %fusion.7.refs_0_.refs_4_), channel_id=1, source_target_pairs={{0,2},{2,0},{4,6},{6,4},{8,10},{10,8},{12,14},{14,12},{16,18},{18,... | collective-permute-start | bytes 1179656 | tf_op jit(solution)/shard_map/ppermute | solution.py:270
  52.3 6.4 %collective-permute-start.23 = (bf16[192,1152]{1,0:T(8,128)(2,1)S(1)}, bf16[192,1152]{1,0:T(8,128)(2,1)S(1)}, u32[]{:S(2)}, u32[]{:S(2)}) collective-permute-start(bf16[192,1152]{1,0:T(8,128)(2,1)S(1)} %fusion.5.refs_1_.refs_4_), channel_id=1, source_target_pairs={{0,2},{2,0},{4,6},{6,4},{8,10},{10,8},{12,14},{14,12},{16,18},{18,... | collective-permute-start | bytes 1327112 | tf_op jit(solution)/shard_map/ppermute | solution.py:270
  52.7 1.2 %copy-start.2 = (bf16[1,256,2048]{2,1,0:T(8,128)(2,1)S(1)}, bf16[1,256,2048]{2,1,0:T(8,128)(2,1)}, u32[]{:S(2)}) copy-start(bf16[1,256,2048]{2,1,0:T(8,128)(2,1)} %param.17) | copy-start | bytes 3145732
  55.8 0.8 copy-start.3
  56.4 5.4 %collective-permute-start.14 = (bf16[192,1024]{1,0:T(8,128)(2,1)S(1)}, bf16[192,1024]{1,0:T(8,128)(2,1)S(1)}, u32[]{:S(2)}, u32[]{:S(2)}) collective-permute-start(bf16[192,1024]{1,0:T(8,128)(2,1)S(1)} %get-tuple-element.37), channel_id=1, source_target_pairs={{0,2},{2,0},{4,6},{6,4},{8,10},{10,8},{12,14},{14,12},{16,18},{18,... | collective-permute-start | bytes 1179656 | tf_op jit(solution)/shard_map/ppermute | solution.py:270
  57.2 4.8 %collective-permute-start.27 = (bf16[192,1152]{1,0:T(8,128)(2,1)S(1)}, bf16[192,1152]{1,0:T(8,128)(2,1)S(1)}, u32[]{:S(2)}, u32[]{:S(2)}) collective-permute-start(bf16[192,1152]{1,0:T(8,128)(2,1)S(1)} %get-tuple-element.42), channel_id=1, source_target_pairs={{0,2},{2,0},{4,6},{6,4},{8,10},{10,8},{12,14},{14,12},{16,18},{18,... | collective-permute-start | bytes 1327112 | tf_op jit(solution)/shard_map/ppermute | solution.py:270
  60.6 3.0 %collective-permute-start.28 = (bf16[192,1152]{1,0:T(8,128)(2,1)S(1)}, bf16[192,1152]{1,0:T(8,128)(2,1)S(1)}, u32[]{:S(2)}, u32[]{:S(2)}) collective-permute-start(bf16[192,1152]{1,0:T(8,128)(2,1)S(1)} %get-tuple-element.44), channel_id=1, source_target_pairs={{0,2},{2,0},{4,6},{6,4},{8,10},{10,8},{12,14},{14,12},{16,18},{18,... | collective-permute-start | bytes 1327112 | tf_op jit(solution)/shard_map/ppermute | solution.py:270
  61.3 4.5 %collective-permute-start.25 = (bf16[192,1024]{1,0:T(8,128)(2,1)S(1)}, bf16[192,1024]{1,0:T(8,128)(2,1)S(1)}, u32[]{:S(2)}, u32[]{:S(2)}) collective-permute-start(bf16[192,1024]{1,0:T(8,128)(2,1)S(1)} %get-tuple-element.40), channel_id=1, source_target_pairs={{0,2},{2,0},{4,6},{6,4},{8,10},{10,8},{12,14},{14,12},{16,18},{18,... | collective-permute-start | bytes 1179656 | tf_op jit(solution)/shard_map/ppermute | solution.py:270
  62.0 1.7 %copy-start.7 = (f32[192,1152]{1,0:T(8,128)}, f32[192,1152]{1,0:T(8,128)S(1)}, u32[]{:S(2)}) copy-start(f32[192,1152]{1,0:T(8,128)S(1)} %convert_add_fusion) | copy-start | bytes 2654212
  62.1 17.8 %collective-permute-start.31 = (bf16[192,640]{1,0:T(8,128)(2,1)S(1)}, bf16[192,640]{1,0:T(8,128)(2,1)S(1)}, u32[]{:S(2)}, u32[]{:S(2)}) collective-permute-start(bf16[192,640]{1,0:T(8,128)(2,1)S(1)} %slice.219), channel_id=1, source_target_pairs={{0,1},{1,0},{2,3},{3,2},{4,5},{5,4},{6,7},{7,6},{8,9},{9,8},{10,11... | collective-permute-start | bytes 737288 | tf_op jit(solution)/shard_map/ppermute | solution.py:273
  63.8 7.8 %collective-permute-start.29 = (bf16[192,512]{1,0:T(8,128)(2,1)S(1)}, bf16[192,512]{1,0:T(8,128)(2,1)S(1)}, u32[]{:S(2)}, u32[]{:S(2)}) collective-permute-start(bf16[192,512]{1,0:T(8,128)(2,1)S(1)} %pad_maximum_fusion.11), channel_id=1, source_target_pairs={{0,4},{2,6},{4,0},{6,2},{8,12},{10,14},{12,8},{14,10},{16,20},{18,... | collective-permute-start | bytes 589832 | tf_op jit(solution)/shard_map/ppermute | solution.py:267
  65.3 6.3 %slice-start = ((f32[192,1152]{1,0:T(8,128)}), f32[192,128]{1,0:T(8,128)S(1)}, s32[]{:S(2)}) async-start(f32[192,1152]{1,0:T(8,128)} %copy-done.7), calls=%async_computation | async-start | bytes 196608 | tf_op jit(solution)/shard_map/slice | solution.py:414
  65.3 6.3 %slice-start.1 = ((f32[192,1152]{1,0:T(8,128)}), f32[192,384]{1,0:T(8,128)S(1)}, s32[]{:S(2)}) async-start(f32[192,1152]{1,0:T(8,128)} %copy-done.7), calls=%async_computation.1 | async-start | bytes 589824 | tf_op jit(solution)/shard_map/slice | solution.py:414
  65.3 10.9 %collective-permute-start.32 = (bf16[192,640]{1,0:T(8,128)(2,1)S(1)}, bf16[192,640]{1,0:T(8,128)(2,1)S(1)}, u32[]{:S(2)}, u32[]{:S(2)}) collective-permute-start(bf16[192,640]{1,0:T(8,128)(2,1)S(1)} %slice.171), channel_id=1, source_target_pairs={{0,1},{1,0},{2,3},{3,2},{4,5},{5,4},{6,7},{7,6},{8,9},{9,8},{10,11... | collective-permute-start | bytes 737288 | tf_op jit(solution)/shard_map/ppermute | solution.py:273
  66.0 13.8 %collective-permute-start.26 = (bf16[192,384]{1,0:T(8,128)(2,1)S(1)}, bf16[192,384]{1,0:T(8,128)(2,1)S(1)}, u32[]{:S(2)}, u32[]{:S(2)}) collective-permute-start(bf16[192,384]{1,0:T(8,128)(2,1)S(1)} %slice.220), channel_id=1, source_target_pairs={{0,4},{2,6},{4,0},{6,2},{8,12},{10,14},{12,8},{14,10},{16,20},{18,... | collective-permute-start | bytes 442376 | tf_op jit(solution)/shard_map/ppermute | solution.py:267
  71.7 7.9 %collective-permute-start.30 = (bf16[192,512]{1,0:T(8,128)(2,1)S(1)}, bf16[192,512]{1,0:T(8,128)(2,1)S(1)}, u32[]{:S(2)}, u32[]{:S(2)}) collective-permute-start(bf16[192,512]{1,0:T(8,128)(2,1)S(1)} %get-tuple-element.52), channel_id=1, source_target_pairs={{0,1},{1,0},{2,3},{3,2},{4,5},{5,4},{6,7},{7,6},{8,9},{9,8},{10,11... | collective-permute-start | bytes 589832 | tf_op jit(solution)/shard_map/ppermute | solution.py:273
  76.3 6.3 %collective-permute-start.33 = (bf16[192,640]{1,0:T(8,128)(2,1)S(1)}, bf16[192,640]{1,0:T(8,128)(2,1)S(1)}, u32[]{:S(2)}, u32[]{:S(2)}) collective-permute-start(bf16[192,640]{1,0:T(8,128)(2,1)S(1)} %fusion.1), channel_id=1, source_target_pairs={{0,4},{2,6},{4,0},{6,2},{8,12},{10,14},{12,8},{14,10},{16,20},{18,... | collective-permute-start | bytes 737288 | tf_op jit(solution)/shard_map/ppermute | solution.py:267
  82.8 11.2 %collective-permute-start.36 = (bf16[48,1152]{1,0:T(8,128)(2,1)S(1)}, bf16[48,1152]{1,0:T(8,128)(2,1)S(1)}, u32[]{:S(2)}, u32[]{:S(2)}) collective-permute-start(bf16[48,1152]{1,0:T(8,128)(2,1)S(1)} %get-tuple-element.54), channel_id=1, source_target_pairs={{0,24},{2,26},{4,28},{6,30},{8,16},{10,18},{12,20},{14,22},{16,8},... | collective-permute-start | bytes 331784 | tf_op jit(solution)/shard_map/ppermute | solution.py:264
  87.1 6.8 %collective-permute-start.35 = (bf16[48,1152]{1,0:T(8,128)(2,1)S(1)}, bf16[48,1152]{1,0:T(8,128)(2,1)S(1)}, u32[]{:S(2)}, u32[]{:S(2)}) collective-permute-start(bf16[48,1152]{1,0:T(8,128)(2,1)S(1)} %get-tuple-element.55), channel_id=1, source_target_pairs={{0,16},{2,18},{4,20},{6,22},{8,24},{10,26},{12,28},{14,30},{16,0},... | collective-permute-start | bytes 331784 | tf_op jit(solution)/shard_map/ppermute | solution.py:264
  87.1 6.8 %collective-permute-start.34 = (bf16[48,1152]{1,0:T(8,128)(2,1)S(1)}, bf16[48,1152]{1,0:T(8,128)(2,1)S(1)}, u32[]{:S(2)}, u32[]{:S(2)}) collective-permute-start(bf16[48,1152]{1,0:T(8,128)(2,1)S(1)} %get-tuple-element.56), channel_id=1, source_target_pairs={{0,8},{2,10},{4,12},{6,14},{8,0},{10,2},{12,4},{14,6},{16,24},{18,... | collective-permute-start | bytes 331784 | tf_op jit(solution)/shard_map/ppermute | solution.py:264
  91.6 2.3 %copy-start.4 = (s32[128,2]{0,1:T(2,128)S(1)}, s32[128,2]{0,1:T(2,128)}, u32[]{:S(2)}) copy-start(s32[128,2]{0,1:T(2,128)} %param.14) | copy-start | bytes 3076
  91.6 2.4 %copy-start.5 = (f32[128,2]{0,1:T(2,128)S(1)}, f32[128,2]{0,1:T(2,128)}, u32[]{:S(2)}) copy-start(f32[128,2]{0,1:T(2,128)} %param.12) | copy-start | bytes 3076
  91.6 2.4 %copy-start.6 = (f32[128]{0:T(128)S(1)}, f32[128]{0:T(128)}, u32[]{:S(2)}) copy-start(f32[128]{0:T(128)} %param.11) | copy-start | bytes 1540

commit v5 on v4

--- a/solution.py
+++ b/solution.py
@@ -221,19 +221,27 @@
             down_out[:, span] = dot(hidden, part, ROWS_ROWS)
 
 
-def final_body(groups, cap, *refs):
-    back = refs[:groups]
-    pick_refs = refs[groups : groups + 4]
-    local_ref, weight_ref, expert_ref = refs[groups + 4 : groups + 7]
-    tok_out, group_out, expert_out = refs[groups + 7 :]
-    count, width = tok_out.shape
-    picks = [pick_refs[min(k, 3)][pl.ds(max(k - 3, 0) * cap, cap), :] for k in range(groups)]
+def first_body(cap, blocks, *refs):
+    back = refs[: len(blocks)]
+    pick_refs = refs[len(blocks) : len(blocks) + 4]
+    total_out, held_out = refs[len(blocks) + 4 :]
+    count, width = total_out.shape
     total = jnp.zeros((count, width), F32)
     held = jnp.zeros((LANES, count), F32)
-    for k in range(groups):
-        total = total + dot(picks[k], back[k][:, :width], ROWS_ROWS)
-        held = held + dot(back[k][:, width:], picks[k], ROWS_ROWS)
-    tok_out[...] = total
+    for ref, k in zip(back, blocks):
+        pick = pick_refs[min(k, 3)][pl.ds(max(k - 3, 0) * cap, cap), :]
+        total = total + dot(pick, ref[:, :width], ROWS_ROWS)
+        held = held + dot(ref[:, width:], pick, ROWS_ROWS)
+    total_out[...] = total
+    held_out[...] = held
+
+
+def final_body(back, pick_ref, total_ref, held_ref, local_ref, weight_ref, expert_ref, *outs):
+    tok_out, group_out, expert_out = outs
+    count, width = tok_out.shape
+    pick = pick_ref[...]
+    tok_out[...] = total_ref[...] + dot(pick, back[:, :width], ROWS_ROWS)
+    held = held_ref[...] + dot(back[:, width:], pick, ROWS_ROWS)
     lane = lax.broadcasted_iota(jnp.int32, (LANES, count), 0)
     group_sum = jnp.zeros((1, count), F32)
     for k in range(local_ref.shape[0]):
@@ -432,8 +440,15 @@
     held = tail[:, :EPG] + tail[:, EPG : 2 * EPG]
     held = jnp.pad(held, ((0, 0), (0, LANES - EPG)))
     result = jnp.concatenate([body, held], axis=1).astype(BF16)
-    sent = {k: along_groups(result[k * cap : (k + 1) * cap], k) for k in range(groups - 1, 0, -1)}
-    returned = [result[:cap]] + [sent[k] for k in range(1, groups)]
+    blocks = [k for k in range(groups) if k != 2]
+    sent = {k: along_groups(result[k * cap : (k + 1) * cap], k) for k in blocks[:0:-1]}
+    mid = along_groups(result[2 * cap : 3 * cap], 2)
+    returned = [result[:cap]] + [sent[k] for k in blocks[1:]]
+    part = call(
+        functools.partial(first_body, cap, blocks),
+        [shape((count, width), F32), shape((LANES, count), F32)],
+        10**6,
+    )(*returned, *picked)
     grads, scaled_hidden, toks, cots = [near[i] + far[i] for i in range(4)]
     up_work = 2 * 2 * 4 * rows * features * cols
     first_grad, second_grad = call(
@@ -447,9 +462,8 @@
         up_work // 2,
     )(*cots, *scaled_hidden)
     token_grad, group_grad, expert_grad = call(
-        functools.partial(final_body, groups, cap),
-        [shape((count, width), F32), shape((1, count), F32), shape((picks, count), F32)],
-    )(*returned, *picked, local_rows, weight_row, expert_rows)
+        final_body, [shape((count, width), F32), shape((1, count), F32), shape((picks, count), F32)]
+    )(mid, picked[2], *part, local_rows, weight_row, expert_rows)
     return (
         token_grad,
         group_grad.reshape(count),

time: 95.5 us -> 95.7 us (level)
    pallas_call x14 -> x15, Pallas kernels: 16.7 us -> 16.9 us  [run(): pl.pallas_call(body, out_shape=outs, in_specs=[pl.BlockSpec(memory_space=...]
  transfers between devices with their start and end apart: 37 -> 37, of which waited for: 12 -> 13; matrix products, arithmetic and copies ran while one was open for 2% -> 1% of each run, Pallas kernels for 14% -> 15%
where the time goes in v5:
time: 95.7 us; the launch traced here: 95.6 us
  waiting for transfers between devices  38.3 us (40%)
  starting transfers between devices  37.4 us (39%)
  Pallas kernels  16.9 us (18%)
  other arithmetic  1.32 us (1%)
  between operations  1.17 us (1%)
    pallas_call x15, Pallas kernels, run(): pl.pallas_call(body, out_shape=outs, in_specs=[pl.BlockSpec(memory_space=...  16.9 us
    ppermute x8, starting transfers between devices, along_groups(): return lax.ppermute(a, 'ep', [(e, e ^ k * EPG) for e in range(experts)])  13.1 us
    ppermute x6, waiting for transfers between devices, along_tp(): return lax.ppermute(a, 'tp', [(r, (r + j) % lanes) for r in range(lanes)])  11.4 us
    ppermute x8, waiting for transfers between devices, along_groups(): return lax.ppermute(a, 'ep', [(e, e ^ k * EPG) for e in range(experts)])  10.9 us
    ppermute x6, starting transfers between devices, along_side(): return lax.ppermute(a, 'ep', [(e, e ^ 2) for e in range(experts)])  8.42 us
    ppermute x6, waiting for transfers between devices, along_side(): return lax.ppermute(a, 'ep', [(e, e ^ 2) for e in range(experts)])  7.68 us
    ppermute x6, starting transfers between devices, along_tp(): return lax.ppermute(a, 'tp', [(r, (r + j) % lanes) for r in range(lanes)])  6.37 us
    ppermute x2, waiting for transfers between devices, along_mixed(): return lax.ppermute(a, ('ep', 'tp'), pairs)  4.45 us
  transfers between devices with their start and end apart: 37, of which 13 were waited for; matrix products, arithmetic and copies ran while one was open for 1% of the time, Pallas kernels for 15%

profile of v5, /device:TPU:0, one launch (start us, length us, event | category | flops | bytes accessed | tf_op | source)
XLA Modules:
  0.0 95.6 jit_solution(9820047817966624953)
XLA Ops:
  0.6 1.7 %shard_map.136 = (bf16[48,2176]{1,0:T(8,128)(2,1)S(1)}, bf16[48,2176]{1,0:T(8,128)(2,1)S(1)}, bf16[48,1024]{1,0:T(8,128)(2,1)S(1)}, bf16[48,1024]{1,0:T(8,128)(2...) custom-call(s32[1,128]{1,0:T(1,128)} %bitcast.26, s32[2,128]{1,0:T(2,128)} %bitcast.31, ...), custom_call_target="tpu_custom_call" | custom-call | tf_op jit(solution)/shard_map/pallas_call | solution.py:27
  2.3 4.1 %collective-permute-start.1 = (bf16[48,1024]{1,0:T(8,128)(2,1)S(1)}, bf16[48,1024]{1,0:T(8,128)(2,1)S(1)}, u32[]{:S(2)}, u32[]{:S(2)}) collective-permute-start(bf16[48,1024]{1,0:T(8,128)(2,1)S(1)} %get-tuple-element.33), channel_id=1, source_target_pairs={{0,16},{2,18},{4,20},{6,22},{8,24},{10,26},{12,28},{14,30},{16,0},... | collective-permute-start | bytes 294920 | tf_op jit(solution)/shard_map/ppermute | solution.py:272
  6.5 1.3 %collective-permute-start.2 = (bf16[48,1024]{1,0:T(8,128)(2,1)S(1)}, bf16[48,1024]{1,0:T(8,128)(2,1)S(1)}, u32[]{:S(2)}, u32[]{:S(2)}) collective-permute-start(bf16[48,1024]{1,0:T(8,128)(2,1)S(1)} %get-tuple-element.34), channel_id=1, source_target_pairs={{0,24},{2,26},{4,28},{6,30},{8,16},{10,18},{12,20},{14,22},{16,8},... | collective-permute-start | bytes 294920 | tf_op jit(solution)/shard_map/ppermute | solution.py:272
  7.8 1.7 %collective-permute-start.9 = (bf16[48,1152]{1,0:T(8,128)(2,1)S(1)}, bf16[48,1152]{1,0:T(8,128)(2,1)S(1)}, u32[]{:S(2)}, u32[]{:S(2)}) collective-permute-start(bf16[48,1152]{1,0:T(8,128)(2,1)S(1)} %get-tuple-element.35), channel_id=1, source_target_pairs={{0,16},{2,18},{4,20},{6,22},{8,24},{10,26},{12,28},{14,30},{16,0},... | collective-permute-start | bytes 331784 | tf_op jit(solution)/shard_map/ppermute | solution.py:272
  9.5 0.9 collective-permute-start.10
  10.4 1.5 %collective-permute-start.3 = (bf16[48,2176]{1,0:T(8,128)(2,1)S(1)}, bf16[48,2176]{1,0:T(8,128)(2,1)S(1)}, u32[]{:S(2)}, u32[]{:S(2)}) collective-permute-start(bf16[48,2176]{1,0:T(8,128)(2,1)S(1)} %get-tuple-element.31), channel_id=1, source_target_pairs={{0,4},{1,5},{2,3},{3,2},{4,0},{5,1},{6,7},{7,6},{8,12},{9,13},{10,... | collective-permute-start | bytes 626696 | tf_op jit(solution)/shard_map/ppermute | solution.py:345
  11.9 7.1 %collective-permute-done.1 = bf16[48,1024]{1,0:T(8,128)(2,1)S(1)} collective-permute-done((bf16[48,1024]{1,0:T(8,128)(2,1)S(1)}, bf16[48,1024]{1,0:T(8,128)(2,1)S(1)}, u32[]{:S(2)}, u32[]{:S(2)}) %collective-permute-start.1) | collective-permute-done | bytes 98336 | tf_op jit(solution)/shard_map/ppermute | solution.py:272
  19.1 1.7 %collective-permute-start.16 = (bf16[96,1024]{1,0:T(8,128)(2,1)S(1)}, bf16[96,1024]{1,0:T(8,128)(2,1)S(1)}, u32[]{:S(2)}, u32[]{:S(2)}) collective-permute-start(bf16[96,1024]{1,0:T(8,128)(2,1)S(1)} %constant_dynamic-update-slice_fusion.2), channel_id=1, source_target_pairs={{0,4},{2,6},{4,0},{6,2},{8,12},{10,14},{12,8},{14,10},{16,20},{18,... | collective-permute-start | bytes 589832 | tf_op jit(solution)/shard_map/ppermute | solution.py:275
  20.8 2.7 %collective-permute-done.9 = bf16[48,1152]{1,0:T(8,128)(2,1)S(1)} collective-permute-done((bf16[48,1152]{1,0:T(8,128)(2,1)S(1)}, bf16[48,1152]{1,0:T(8,128)(2,1)S(1)}, u32[]{:S(2)}, u32[]{:S(2)}) %collective-permute-start.9) | collective-permute-done | bytes 110624 | tf_op jit(solution)/shard_map/ppermute | solution.py:272
  23.5 1.7 %collective-permute-start.6 = (bf16[96,1024]{1,0:T(8,128)(2,1)S(1)}, bf16[96,1024]{1,0:T(8,128)(2,1)S(1)}, u32[]{:S(2)}, u32[]{:S(2)}) collective-permute-start(bf16[96,1024]{1,0:T(8,128)(2,1)S(1)} %constant_dynamic-update-slice_fusion.2), channel_id=1, source_target_pairs={{0,1},{1,0},{2,3},{3,2},{4,5},{5,4},{6,7},{7,6},{8,9},{9,8},{10,11... | collective-permute-start | bytes 589832 | tf_op jit(solution)/shard_map/ppermute | solution.py:281
  25.3 0.4 collective-permute-start.11
  25.7 0.9 collective-permute-done
  26.6 1.3 %collective-permute-start.21 = (bf16[96,1152]{1,0:T(8,128)(2,1)S(1)}, bf16[96,1152]{1,0:T(8,128)(2,1)S(1)}, u32[]{:S(2)}, u32[]{:S(2)}) collective-permute-start(bf16[96,1152]{1,0:T(8,128)(2,1)S(1)} %pad_maximum_fusion.9), channel_id=1, source_target_pairs={{0,4},{2,6},{4,0},{6,2},{8,12},{10,14},{12,8},{14,10},{16,20},{18,... | collective-permute-start | bytes 663560 | tf_op jit(solution)/shard_map/ppermute | solution.py:275
  28.0 1.6 %collective-permute-start.5 = (bf16[48,2048]{1,0:T(8,128)(2,1)S(1)}, bf16[48,2048]{1,0:T(8,128)(2,1)S(1)}, u32[]{:S(2)}, u32[]{:S(2)}) collective-permute-start(bf16[48,2048]{1,0:T(8,128)(2,1)S(1)} %slice.150), channel_id=1, source_target_pairs={{0,1},{1,0},{2,3},{3,2},{4,5},{5,4},{6,7},{7,6},{8,9},{9,8},{10,11... | collective-permute-start | bytes 589832 | tf_op jit(solution)/shard_map/ppermute | solution.py:281
  29.8 1.5 %collective-permute-done.6 = bf16[96,1024]{1,0:T(8,128)(2,1)S(1)} collective-permute-done((bf16[96,1024]{1,0:T(8,128)(2,1)S(1)}, bf16[96,1024]{1,0:T(8,128)(2,1)S(1)}, u32[]{:S(2)}, u32[]{:S(2)}) %collective-permute-start.6) | collective-permute-done | bytes 196640 | tf_op jit(solution)/shard_map/ppermute | solution.py:281
  31.3 1.7 %collective-permute-start.15 = (bf16[48,2176]{1,0:T(8,128)(2,1)S(1)}, bf16[48,2176]{1,0:T(8,128)(2,1)S(1)}, u32[]{:S(2)}, u32[]{:S(2)}) collective-permute-start(bf16[48,2176]{1,0:T(8,128)(2,1)S(1)} %collective-permute-done), channel_id=1, source_target_pairs={{0,4},{2,6},{4,0},{6,2},{8,12},{10,14},{12,8},{14,10},{16,20},{18,... | collective-permute-start | bytes 626696 | tf_op jit(solution)/shard_map/ppermute | solution.py:275
  33.0 4.2 %collective-permute-done.5 = bf16[48,2048]{1,0:T(8,128)(2,1)S(1)} collective-permute-done((bf16[48,2048]{1,0:T(8,128)(2,1)S(1)}, bf16[48,2048]{1,0:T(8,128)(2,1)S(1)}, u32[]{:S(2)}, u32[]{:S(2)}) %collective-permute-start.5) | collective-permute-done | bytes 196640 | tf_op jit(solution)/shard_map/ppermute | solution.py:281
  37.2 1.4 %collective-permute-start.4 = (bf16[96,2176]{1,0:T(8,128)(2,1)S(1)}, bf16[96,2176]{1,0:T(8,128)(2,1)S(1)}, u32[]{:S(2)}, u32[]{:S(2)}) collective-permute-start(bf16[96,2176]{1,0:T(8,128)(2,1)S(1)} %pad_maximum_fusion.2), channel_id=1, source_target_pairs={{0,1},{1,0},{2,6},{3,7},{4,5},{5,4},{6,2},{7,3},{8,9},{9,8},{10,14... | collective-permute-start | bytes 1253384 | tf_op jit(solution)/shard_map/ppermute | solution.py:345
  38.6 0.7 collective-permute-start.18
  39.3 1.4 %collective-permute-start.17 = (bf16[48,2048]{1,0:T(8,128)(2,1)S(1)}, bf16[48,2048]{1,0:T(8,128)(2,1)S(1)}, u32[]{:S(2)}, u32[]{:S(2)}) collective-permute-start(bf16[48,2048]{1,0:T(8,128)(2,1)S(1)} %slice_select_fusion.1), channel_id=1, source_target_pairs={{0,1},{1,0},{2,6},{3,7},{4,5},{5,4},{6,2},{7,3},{8,9},{9,8},{10,14... | collective-permute-start | bytes 589832 | tf_op jit(solution)/shard_map/ppermute | solution.py:293
  40.8 4.4 %collective-permute-done.4 = bf16[96,2176]{1,0:T(8,128)(2,1)S(1)} collective-permute-done((bf16[96,2176]{1,0:T(8,128)(2,1)S(1)}, bf16[96,2176]{1,0:T(8,128)(2,1)S(1)}, u32[]{:S(2)}, u32[]{:S(2)}) %collective-permute-start.4) | collective-permute-done | bytes 417824 | tf_op jit(solution)/shard_map/ppermute | solution.py:345
  45.2 1.4 %collective-permute-start.22 = (bf16[96,1024]{1,0:T(8,128)(2,1)S(1)}, bf16[96,1024]{1,0:T(8,128)(2,1)S(1)}, u32[]{:S(2)}, u32[]{:S(2)}) collective-permute-start(bf16[96,1024]{1,0:T(8,128)(2,1)S(1)} %slice_select_fusion), channel_id=1, source_target_pairs={{0,1},{1,0},{2,6},{3,7},{4,5},{5,4},{6,2},{7,3},{8,9},{9,8},{10,14... | collective-permute-start | bytes 589832 | tf_op jit(solution)/shard_map/ppermute | solution.py:293
  46.6 2.8 %collective-permute-done.17 = bf16[48,2048]{1,0:T(8,128)(2,1)S(1)} collective-permute-done((bf16[48,2048]{1,0:T(8,128)(2,1)S(1)}, bf16[48,2048]{1,0:T(8,128)(2,1)S(1)}, u32[]{:S(2)}, u32[]{:S(2)}) %collective-permute-start.17) | collective-permute-done | bytes 196640 | tf_op jit(solution)/shard_map/ppermute | solution.py:293
  49.7 0.6 collective-permute-start.8
  50.4 1.2 %collective-permute-done.22 = bf16[96,1024]{1,0:T(8,128)(2,1)S(1)} collective-permute-done((bf16[96,1024]{1,0:T(8,128)(2,1)S(1)}, bf16[96,1024]{1,0:T(8,128)(2,1)S(1)}, u32[]{:S(2)}, u32[]{:S(2)}) %collective-permute-start.22) | collective-permute-done | bytes 196640 | tf_op jit(solution)/shard_map/ppermute | solution.py:293
  51.6 0.6 collective-permute-start.24
  52.2 0.1 collective-permute-start.19
  52.3 0.4 collective-permute-start.23
  52.7 1.0 %shard_map.137.refs_0_ = f32[384,768]{1,0:T(8,128)S(1)} custom-call(bf16[192,1024]{1,0:T(8,128)(2,1)S(1)} %pad_maximum_fusion.6.refs_0_, bf16[192,1024]{1,0:T(8,128)(2,1)S(1)} %pad_maximum_fusion.7.refs_1_, bf16[192,1024]{1,0:T(8,128)(2,1)S(1)} %collective-permute-done.7.refs_2_, bf16[192,1024]{1,0:T(8,128)(2,1)S(1)} %collective-permute-done.8.refs_3_, ...), custom_call_target="tpu_custom_call" | custom-call | flops 805306368 | tf_op jit(solution)/shard_map/pallas_call | solution.py:27
  53.8 0.2 copy-done.2
  53.9 1.8 %shard_map.138 = (f32[192,1152]{1,0:T(8,128)S(1)}, bf16[192,1152]{1,0:T(8,128)(2,1)S(1)}, bf16[384,512]{1,0:T(8,128)(2,1)S(1)}, bf16[384,256]{1,0:T(8,128)(2,1)S(1)}) custom-call(f32[384,768]{1,0:T(8,128)S(1)} %shard_map.137.refs_0_, bf16[192,1152]{1,0:T(8,128)(2,1)S(1)} %pad_maximum_fusion.1.refs_1_.refs_0_, bf16[192,1024]{1,0:T(8,128)(2,1)S(1)} %fusion.8.refs_2_.refs_1_, ...), custom_call_target="tpu_custom_call" | custom-call | flops 805306368 | tf_op jit(solution)/shard_map/pallas_call | solution.py:27
  55.8 0.6 shard_map.139
  56.4 0.2 collective-permute-start.14
  56.6 0.1 shard_map.143.refs_5_.pick_ref
  56.7 0.1 shard_map.146.refs_6_
  56.9 0.1 shard_map.145.refs_4_
  57.0 0.1 shard_map.144.refs_3_
  57.2 0.5 collective-permute-start.27
  57.7 1.0 %shard_map.140.refs_0_ = f32[384,768]{1,0:T(8,128)S(1)} custom-call(bf16[192,1024]{1,0:T(8,128)(2,1)S(1)} %fusion.7.refs_0_.refs_4_, bf16[192,1024]{1,0:T(8,128)(2,1)S(1)} %pad_maximum_fusion.8.refs_1_.refs_5_, bf16[192,1024]{1,0:T(8,128)(2,1)S(1)} %collective-permute-done.19.refs_2_.refs_6_, bf16[192,1024]{1,0:T(8,128)(2,1)S(1)} %collective-permute-done.20.refs_3_.refs_7_, ...), custom_call_target="tpu_custom_call" | custom-call | flops 805306368 | tf_op jit(solution)/shard_map/pallas_call | solution.py:27
  58.7 1.9 %shard_map.141 = (f32[192,1152]{1,0:T(8,128)S(1)}, bf16[192,1152]{1,0:T(8,128)(2,1)S(1)}, bf16[384,512]{1,0:T(8,128)(2,1)S(1)}, bf16[384,256]{1,0:T(8,128)(2,1)S(1)}) custom-call(f32[384,768]{1,0:T(8,128)S(1)} %shard_map.140.refs_0_, bf16[192,1152]{1,0:T(8,128)(2,1)S(1)} %fusion.5.refs_1_.refs_4_, bf16[192,1024]{1,0:T(8,128)(2,1)S(1)} %fusion.6.refs_2_.refs_5_, ...), custom_call_target="tpu_custom_call" | custom-call | flops 805306368 | tf_op jit(solution)/shard_map/pallas_call | solution.py:27
  60.6 0.2 collective-permute-start.28
  60.7 0.6 shard_map.142
  61.3 0.5 collective-permute-start.25
  61.8 0.1 convert_add_fusion.2
  62.1 1.5 %collective-permute-start.31 = (bf16[192,640]{1,0:T(8,128)(2,1)S(1)}, bf16[192,640]{1,0:T(8,128)(2,1)S(1)}, u32[]{:S(2)}, u32[]{:S(2)}) collective-permute-start(bf16[192,640]{1,0:T(8,128)(2,1)S(1)} %slice.219), channel_id=1, source_target_pairs={{0,1},{1,0},{2,3},{3,2},{4,5},{5,4},{6,7},{7,6},{8,9},{9,8},{10,11... | collective-permute-start | bytes 737288 | tf_op jit(solution)/shard_map/ppermute | solution.py:281
  63.8 1.6 %collective-permute-start.29 = (bf16[192,512]{1,0:T(8,128)(2,1)S(1)}, bf16[192,512]{1,0:T(8,128)(2,1)S(1)}, u32[]{:S(2)}, u32[]{:S(2)}) collective-permute-start(bf16[192,512]{1,0:T(8,128)(2,1)S(1)} %pad_maximum_fusion.11), channel_id=1, source_target_pairs={{0,4},{2,6},{4,0},{6,2},{8,12},{10,14},{12,8},{14,10},{16,20},{18,... | collective-permute-start | bytes 589832 | tf_op jit(solution)/shard_map/ppermute | solution.py:275
  65.3 0.5 collective-permute-start.32
  65.9 0.1 convert_add_fusion.1
  66.0 0.7 collective-permute-start.26
  66.6 5.0 %collective-permute-done.29 = bf16[192,512]{1,0:T(8,128)(2,1)S(1)} collective-permute-done((bf16[192,512]{1,0:T(8,128)(2,1)S(1)}, bf16[192,512]{1,0:T(8,128)(2,1)S(1)}, u32[]{:S(2)}, u32[]{:S(2)}) %collective-permute-start.29) | collective-permute-done | bytes 196640 | tf_op jit(solution)/shard_map/ppermute | solution.py:275
  71.7 0.7 collective-permute-start.30
  72.3 3.9 %collective-permute-done.32 = bf16[192,640]{1,0:T(8,128)(2,1)S(1)} collective-permute-done((bf16[192,640]{1,0:T(8,128)(2,1)S(1)}, bf16[192,640]{1,0:T(8,128)(2,1)S(1)}, u32[]{:S(2)}, u32[]{:S(2)}) %collective-permute-start.32) | collective-permute-done | bytes 245792 | tf_op jit(solution)/shard_map/ppermute | solution.py:281
  76.3 1.5 %collective-permute-start.33 = (bf16[192,640]{1,0:T(8,128)(2,1)S(1)}, bf16[192,640]{1,0:T(8,128)(2,1)S(1)}, u32[]{:S(2)}, u32[]{:S(2)}) collective-permute-start(bf16[192,640]{1,0:T(8,128)(2,1)S(1)} %fusion.1), channel_id=1, source_target_pairs={{0,4},{2,6},{4,0},{6,2},{8,12},{10,14},{12,8},{14,10},{16,20},{18,... | collective-permute-start | bytes 737288 | tf_op jit(solution)/shard_map/ppermute | solution.py:275
  77.8 1.8 %collective-permute-done.30 = bf16[192,512]{1,0:T(8,128)(2,1)S(1)} collective-permute-done((bf16[192,512]{1,0:T(8,128)(2,1)S(1)}, bf16[192,512]{1,0:T(8,128)(2,1)S(1)}, u32[]{:S(2)}, u32[]{:S(2)}) %collective-permute-start.30) | collective-permute-done | bytes 196640 | tf_op jit(solution)/shard_map/ppermute | solution.py:281
  79.7 0.1 fusion.12
  79.9 2.7 %collective-permute-done.33 = bf16[192,640]{1,0:T(8,128)(2,1)S(1)} collective-permute-done((bf16[192,640]{1,0:T(8,128)(2,1)S(1)}, bf16[192,640]{1,0:T(8,128)(2,1)S(1)}, u32[]{:S(2)}, u32[]{:S(2)}) %collective-permute-start.33) | collective-permute-done | bytes 245792 | tf_op jit(solution)/shard_map/ppermute | solution.py:275
  82.6 0.1 fusion.3
  82.7 4.4 %collective-permute-start.36 = (bf16[48,1152]{1,0:T(8,128)(2,1)S(1)}, bf16[48,1152]{1,0:T(8,128)(2,1)S(1)}, u32[]{:S(2)}, u32[]{:S(2)}) collective-permute-start(bf16[48,1152]{1,0:T(8,128)(2,1)S(1)} %get-tuple-element.58), channel_id=1, source_target_pairs={{0,24},{2,26},{4,28},{6,30},{8,16},{10,18},{12,20},{14,22},{16,8},... | collective-permute-start | bytes 331784 | tf_op jit(solution)/shard_map/ppermute | solution.py:272
  87.1 0.6 collective-permute-start.34
  87.8 3.8 %shard_map.149 = (f32[2048,256]{1,0:T(8,128)}, f32[2048,256]{1,0:T(8,128)}) custom-call(bf16[192,1024]{1,0:T(8,128)(2,1)S(1)} %pad_maximum_fusion.6.refs_0_, bf16[192,1024]{1,0:T(8,128)(2,1)S(1)} %pad_maximum_fusion.7.refs_1_, bf16[192,1024]{1,0:T(8,128)(2,1)S(1)} %collective-permute-done.7.refs_2_, bf16[192,1024]{1,0:T(8,128)(2,1)S(1)} %collective-permute-done.8.refs_3_, ...), custom_call_target="tpu_custom_call" | custom-call | flops 1610612736 | tf_op jit(solution)/shard_map/pallas_call | solution.py:27
  91.6 2.3 %shard_map.150 = f32[256,2048]{1,0:T(8,128)} custom-call(bf16[192,1152]{1,0:T(8,128)(2,1)S(1)} %pad_maximum_fusion.1.refs_1_.refs_0_, bf16[192,1024]{1,0:T(8,128)(2,1)S(1)} %fusion.8.refs_2_.refs_1_, bf16[192,1152]{1,0:T(8,128)(2,1)S(1)} %collective-permute-done.12.refs_3_.refs_2_, bf16[192,1024]{1,0:T(8,128)(2,1)S(1)} %collective-permute-done.13.refs_4_.refs_3_, ...), custom_call_target="tpu_custom_call" | custom-call | flops 805306368 | tf_op jit(solution)/shard_map/pallas_call | solution.py:27
  94.0 0.4 shard_map.147
  94.4 0.1 collective-permute-done.34.back
  94.5 1.1 %shard_map.148 = (f32[128,1024]{1,0:T(8,128)}, f32[1,128]{1,0:T(1,128)}, f32[2,128]{1,0:T(2,128)}) custom-call(bf16[48,1152]{1,0:T(8,128)(2,1)S(1)} %collective-permute-done.34.back, bf16[48,128]{1,0:T(8,128)(2,1)S(1)} %shard_map.143.refs_5_.pick_ref, f32[128,1024]{1,0:T(8,128)S(1)} %get-tuple-element.47.total_ref, ...), custom_call_target="tpu_custom_call" | custom-call | tf_op jit(solution)/shard_map/pallas_call | solution.py:27
  (92 shorter events, 1.5 us)
Async XLA Ops:
  2.3 16.7 %collective-permute-start.1 = (bf16[48,1024]{1,0:T(8,128)(2,1)S(1)}, bf16[48,1024]{1,0:T(8,128)(2,1)S(1)}, u32[]{:S(2)}, u32[]{:S(2)}) collective-permute-start(bf16[48,1024]{1,0:T(8,128)(2,1)S(1)} %get-tuple-element.33), channel_id=1, source_target_pairs={{0,16},{2,18},{4,20},{6,22},{8,24},{10,26},{12,28},{14,30},{16,0},... | collective-permute-start | bytes 294920 | tf_op jit(solution)/shard_map/ppermute | solution.py:272
  6.5 12.6 %collective-permute-start.2 = (bf16[48,1024]{1,0:T(8,128)(2,1)S(1)}, bf16[48,1024]{1,0:T(8,128)(2,1)S(1)}, u32[]{:S(2)}, u32[]{:S(2)}) collective-permute-start(bf16[48,1024]{1,0:T(8,128)(2,1)S(1)} %get-tuple-element.34), channel_id=1, source_target_pairs={{0,24},{2,26},{4,28},{6,30},{8,16},{10,18},{12,20},{14,22},{16,8},... | collective-permute-start | bytes 294920 | tf_op jit(solution)/shard_map/ppermute | solution.py:272
  7.8 15.7 %collective-permute-start.9 = (bf16[48,1152]{1,0:T(8,128)(2,1)S(1)}, bf16[48,1152]{1,0:T(8,128)(2,1)S(1)}, u32[]{:S(2)}, u32[]{:S(2)}) collective-permute-start(bf16[48,1152]{1,0:T(8,128)(2,1)S(1)} %get-tuple-element.35), channel_id=1, source_target_pairs={{0,16},{2,18},{4,20},{6,22},{8,24},{10,26},{12,28},{14,30},{16,0},... | collective-permute-start | bytes 331784 | tf_op jit(solution)/shard_map/ppermute | solution.py:272
  9.5 15.8 %collective-permute-start.10 = (bf16[48,1152]{1,0:T(8,128)(2,1)S(1)}, bf16[48,1152]{1,0:T(8,128)(2,1)S(1)}, u32[]{:S(2)}, u32[]{:S(2)}) collective-permute-start(bf16[48,1152]{1,0:T(8,128)(2,1)S(1)} %get-tuple-element.36), channel_id=1, source_target_pairs={{0,24},{2,26},{4,28},{6,30},{8,16},{10,18},{12,20},{14,22},{16,8},... | collective-permute-start | bytes 331784 | tf_op jit(solution)/shard_map/ppermute | solution.py:272
  10.4 17.6 %collective-permute-start.3 = (bf16[48,2176]{1,0:T(8,128)(2,1)S(1)}, bf16[48,2176]{1,0:T(8,128)(2,1)S(1)}, u32[]{:S(2)}, u32[]{:S(2)}) collective-permute-start(bf16[48,2176]{1,0:T(8,128)(2,1)S(1)} %get-tuple-element.31), channel_id=1, source_target_pairs={{0,4},{1,5},{2,3},{3,2},{4,0},{5,1},{6,7},{7,6},{8,12},{9,13},{10,... | collective-permute-start | bytes 626696 | tf_op jit(solution)/shard_map/ppermute | solution.py:345
  19.1 7.5 %collective-permute-start = (bf16[48,2176]{1,0:T(8,128)(2,1)S(1)}, bf16[48,2176]{1,0:T(8,128)(2,1)S(1)}, u32[]{:S(2)}, u32[]{:S(2)}) collective-permute-start(bf16[48,2176]{1,0:T(8,128)(2,1)S(1)} %get-tuple-element.32), channel_id=1, source_target_pairs={{0,8},{2,10},{4,12},{6,14},{8,0},{10,2},{12,4},{14,6},{16,24},{18,... | collective-permute-start | bytes 626696 | tf_op jit(solution)/shard_map/ppermute | solution.py:272
  19.1 10.6 %collective-permute-start.16 = (bf16[96,1024]{1,0:T(8,128)(2,1)S(1)}, bf16[96,1024]{1,0:T(8,128)(2,1)S(1)}, u32[]{:S(2)}, u32[]{:S(2)}) collective-permute-start(bf16[96,1024]{1,0:T(8,128)(2,1)S(1)} %constant_dynamic-update-slice_fusion.2), channel_id=1, source_target_pairs={{0,4},{2,6},{4,0},{6,2},{8,12},{10,14},{12,8},{14,10},{16,20},{18,... | collective-permute-start | bytes 589832 | tf_op jit(solution)/shard_map/ppermute | solution.py:275
  23.5 7.8 %collective-permute-start.6 = (bf16[96,1024]{1,0:T(8,128)(2,1)S(1)}, bf16[96,1024]{1,0:T(8,128)(2,1)S(1)}, u32[]{:S(2)}, u32[]{:S(2)}) collective-permute-start(bf16[96,1024]{1,0:T(8,128)(2,1)S(1)} %constant_dynamic-update-slice_fusion.2), channel_id=1, source_target_pairs={{0,1},{1,0},{2,3},{3,2},{4,5},{5,4},{6,7},{7,6},{8,9},{9,8},{10,11... | collective-permute-start | bytes 589832 | tf_op jit(solution)/shard_map/ppermute | solution.py:281
  25.3 13.3 %collective-permute-start.11 = (bf16[96,1024]{1,0:T(8,128)(2,1)S(1)}, bf16[96,1024]{1,0:T(8,128)(2,1)S(1)}, u32[]{:S(2)}, u32[]{:S(2)}) collective-permute-start(bf16[96,1024]{1,0:T(8,128)(2,1)S(1)} %pad_maximum_fusion.10), channel_id=1, source_target_pairs={{0,1},{1,0},{2,3},{3,2},{4,5},{5,4},{6,7},{7,6},{8,9},{9,8},{10,11... | collective-permute-start | bytes 589832 | tf_op jit(solution)/shard_map/ppermute | solution.py:281
  26.6 12.7 %collective-permute-start.21 = (bf16[96,1152]{1,0:T(8,128)(2,1)S(1)}, bf16[96,1152]{1,0:T(8,128)(2,1)S(1)}, u32[]{:S(2)}, u32[]{:S(2)}) collective-permute-start(bf16[96,1152]{1,0:T(8,128)(2,1)S(1)} %pad_maximum_fusion.9), channel_id=1, source_target_pairs={{0,4},{2,6},{4,0},{6,2},{8,12},{10,14},{12,8},{14,10},{16,20},{18,... | collective-permute-start | bytes 663560 | tf_op jit(solution)/shard_map/ppermute | solution.py:275
  28.0 9.2 %collective-permute-start.5 = (bf16[48,2048]{1,0:T(8,128)(2,1)S(1)}, bf16[48,2048]{1,0:T(8,128)(2,1)S(1)}, u32[]{:S(2)}, u32[]{:S(2)}) collective-permute-start(bf16[48,2048]{1,0:T(8,128)(2,1)S(1)} %slice.150), channel_id=1, source_target_pairs={{0,1},{1,0},{2,3},{3,2},{4,5},{5,4},{6,7},{7,6},{8,9},{9,8},{10,11... | collective-permute-start | bytes 589832 | tf_op jit(solution)/shard_map/ppermute | solution.py:281
  29.7 21.9 %collective-permute-start.7 = (bf16[192,1024]{1,0:T(8,128)(2,1)S(1)}, bf16[192,1024]{1,0:T(8,128)(2,1)S(1)}, u32[]{:S(2)}, u32[]{:S(2)}) collective-permute-start(bf16[192,1024]{1,0:T(8,128)(2,1)S(1)} %pad_maximum_fusion.6.refs_0_), channel_id=1, source_target_pairs={{0,2},{2,0},{4,6},{6,4},{8,10},{10,8},{12,14},{14,12},{16,18},{18,... | collective-permute-start | bytes 1179656 | tf_op jit(solution)/shard_map/ppermute | solution.py:278
  31.3 7.3 %collective-permute-start.15 = (bf16[48,2176]{1,0:T(8,128)(2,1)S(1)}, bf16[48,2176]{1,0:T(8,128)(2,1)S(1)}, u32[]{:S(2)}, u32[]{:S(2)}) collective-permute-start(bf16[48,2176]{1,0:T(8,128)(2,1)S(1)} %collective-permute-done), channel_id=1, source_target_pairs={{0,4},{2,6},{4,0},{6,2},{8,12},{10,14},{12,8},{14,10},{16,20},{18,... | collective-permute-start | bytes 626696 | tf_op jit(solution)/shard_map/ppermute | solution.py:275
  37.2 8.0 %collective-permute-start.4 = (bf16[96,2176]{1,0:T(8,128)(2,1)S(1)}, bf16[96,2176]{1,0:T(8,128)(2,1)S(1)}, u32[]{:S(2)}, u32[]{:S(2)}) collective-permute-start(bf16[96,2176]{1,0:T(8,128)(2,1)S(1)} %pad_maximum_fusion.2), channel_id=1, source_target_pairs={{0,1},{1,0},{2,6},{3,7},{4,5},{5,4},{6,2},{7,3},{8,9},{9,8},{10,14... | collective-permute-start | bytes 1253384 | tf_op jit(solution)/shard_map/ppermute | solution.py:345
  38.6 13.6 %collective-permute-start.12 = (bf16[192,1152]{1,0:T(8,128)(2,1)S(1)}, bf16[192,1152]{1,0:T(8,128)(2,1)S(1)}, u32[]{:S(2)}, u32[]{:S(2)}) collective-permute-start(bf16[192,1152]{1,0:T(8,128)(2,1)S(1)} %pad_maximum_fusion.1.refs_1_.refs_0_), channel_id=1, source_target_pairs={{0,2},{2,0},{4,6},{6,4},{8,10},{10,8},{12,14},{14,12},{16,18},{18,... | collective-permute-start | bytes 1327112 | tf_op jit(solution)/shard_map/ppermute | solution.py:278
  38.6 10.8 %collective-permute-start.18 = (bf16[96,1024]{1,0:T(8,128)(2,1)S(1)}, bf16[96,1024]{1,0:T(8,128)(2,1)S(1)}, u32[]{:S(2)}, u32[]{:S(2)}) collective-permute-start(bf16[96,1024]{1,0:T(8,128)(2,1)S(1)} %broadcast_select_fusion.1), channel_id=1, source_target_pairs={{0,1},{1,0},{2,6},{3,7},{4,5},{5,4},{6,2},{7,3},{8,9},{9,8},{10,14... | collective-permute-start | bytes 589832 | tf_op jit(solution)/shard_map/ppermute | solution.py:293
  39.3 10.1 %collective-permute-start.17 = (bf16[48,2048]{1,0:T(8,128)(2,1)S(1)}, bf16[48,2048]{1,0:T(8,128)(2,1)S(1)}, u32[]{:S(2)}, u32[]{:S(2)}) collective-permute-start(bf16[48,2048]{1,0:T(8,128)(2,1)S(1)} %slice_select_fusion.1), channel_id=1, source_target_pairs={{0,1},{1,0},{2,6},{3,7},{4,5},{5,4},{6,2},{7,3},{8,9},{9,8},{10,14... | collective-permute-start | bytes 589832 | tf_op jit(solution)/shard_map/ppermute | solution.py:293
  45.2 6.3 %collective-permute-start.22 = (bf16[96,1024]{1,0:T(8,128)(2,1)S(1)}, bf16[96,1024]{1,0:T(8,128)(2,1)S(1)}, u32[]{:S(2)}, u32[]{:S(2)}) collective-permute-start(bf16[96,1024]{1,0:T(8,128)(2,1)S(1)} %slice_select_fusion), channel_id=1, source_target_pairs={{0,1},{1,0},{2,6},{3,7},{4,5},{5,4},{6,2},{7,3},{8,9},{9,8},{10,14... | collective-permute-start | bytes 589832 | tf_op jit(solution)/shard_map/ppermute | solution.py:293
  49.5 7.7 %collective-permute-start.20 = (bf16[192,1024]{1,0:T(8,128)(2,1)S(1)}, bf16[192,1024]{1,0:T(8,128)(2,1)S(1)}, u32[]{:S(2)}, u32[]{:S(2)}) collective-permute-start(bf16[192,1024]{1,0:T(8,128)(2,1)S(1)} %pad_maximum_fusion.8.refs_1_.refs_5_), channel_id=1, source_target_pairs={{0,2},{2,0},{4,6},{6,4},{8,10},{10,8},{12,14},{14,12},{16,18},{18,... | collective-permute-start | bytes 1179656 | tf_op jit(solution)/shard_map/ppermute | solution.py:278
  49.7 3.0 %copy-start = (bf16[1,2048,256]{2,1,0:T(8,128)(2,1)S(1)}, bf16[1,2048,256]{2,1,0:T(8,128)(2,1)}, u32[]{:S(2)}) copy-start(bf16[1,2048,256]{2,1,0:T(8,128)(2,1)} %param.15) | copy-start | bytes 3145732
  49.7 3.0 %copy-start.1 = (bf16[1,2048,256]{2,1,0:T(8,128)(2,1)S(1)}, bf16[1,2048,256]{2,1,0:T(8,128)(2,1)}, u32[]{:S(2)}) copy-start(bf16[1,2048,256]{2,1,0:T(8,128)(2,1)} %param.16) | copy-start | bytes 3145732
  49.7 2.6 %collective-permute-start.8 = (bf16[192,1024]{1,0:T(8,128)(2,1)S(1)}, bf16[192,1024]{1,0:T(8,128)(2,1)S(1)}, u32[]{:S(2)}, u32[]{:S(2)}) collective-permute-start(bf16[192,1024]{1,0:T(8,128)(2,1)S(1)} %pad_maximum_fusion.7.refs_1_), channel_id=1, source_target_pairs={{0,2},{2,0},{4,6},{6,4},{8,10},{10,8},{12,14},{14,12},{16,18},{18,... | collective-permute-start | bytes 1179656 | tf_op jit(solution)/shard_map/ppermute | solution.py:278
  51.5 2.2 %collective-permute-start.13 = (bf16[192,1024]{1,0:T(8,128)(2,1)S(1)}, bf16[192,1024]{1,0:T(8,128)(2,1)S(1)}, u32[]{:S(2)}, u32[]{:S(2)}) collective-permute-start(bf16[192,1024]{1,0:T(8,128)(2,1)S(1)} %fusion.8.refs_2_.refs_1_), channel_id=1, source_target_pairs={{0,2},{2,0},{4,6},{6,4},{8,10},{10,8},{12,14},{14,12},{16,18},{18,... | collective-permute-start | bytes 1179656 | tf_op jit(solution)/shard_map/ppermute | solution.py:278
  51.6 7.1 %collective-permute-start.24 = (bf16[192,1024]{1,0:T(8,128)(2,1)S(1)}, bf16[192,1024]{1,0:T(8,128)(2,1)S(1)}, u32[]{:S(2)}, u32[]{:S(2)}) collective-permute-start(bf16[192,1024]{1,0:T(8,128)(2,1)S(1)} %fusion.6.refs_2_.refs_5_), channel_id=1, source_target_pairs={{0,2},{2,0},{4,6},{6,4},{8,10},{10,8},{12,14},{14,12},{16,18},{18,... | collective-permute-start | bytes 1179656 | tf_op jit(solution)/shard_map/ppermute | solution.py:278
  52.2 5.5 %collective-permute-start.19 = (bf16[192,1024]{1,0:T(8,128)(2,1)S(1)}, bf16[192,1024]{1,0:T(8,128)(2,1)S(1)}, u32[]{:S(2)}, u32[]{:S(2)}) collective-permute-start(bf16[192,1024]{1,0:T(8,128)(2,1)S(1)} %fusion.7.refs_0_.refs_4_), channel_id=1, source_target_pairs={{0,2},{2,0},{4,6},{6,4},{8,10},{10,8},{12,14},{14,12},{16,18},{18,... | collective-permute-start | bytes 1179656 | tf_op jit(solution)/shard_map/ppermute | solution.py:278
  52.3 6.4 %collective-permute-start.23 = (bf16[192,1152]{1,0:T(8,128)(2,1)S(1)}, bf16[192,1152]{1,0:T(8,128)(2,1)S(1)}, u32[]{:S(2)}, u32[]{:S(2)}) collective-permute-start(bf16[192,1152]{1,0:T(8,128)(2,1)S(1)} %fusion.5.refs_1_.refs_4_), channel_id=1, source_target_pairs={{0,2},{2,0},{4,6},{6,4},{8,10},{10,8},{12,14},{14,12},{16,18},{18,... | collective-permute-start | bytes 1327112 | tf_op jit(solution)/shard_map/ppermute | solution.py:278
  52.7 1.2 %copy-start.2 = (bf16[1,256,2048]{2,1,0:T(8,128)(2,1)S(1)}, bf16[1,256,2048]{2,1,0:T(8,128)(2,1)}, u32[]{:S(2)}) copy-start(bf16[1,256,2048]{2,1,0:T(8,128)(2,1)} %param.17) | copy-start | bytes 3145732
  55.8 0.8 copy-start.3
  56.4 5.4 %collective-permute-start.14 = (bf16[192,1024]{1,0:T(8,128)(2,1)S(1)}, bf16[192,1024]{1,0:T(8,128)(2,1)S(1)}, u32[]{:S(2)}, u32[]{:S(2)}) collective-permute-start(bf16[192,1024]{1,0:T(8,128)(2,1)S(1)} %get-tuple-element.39), channel_id=1, source_target_pairs={{0,2},{2,0},{4,6},{6,4},{8,10},{10,8},{12,14},{14,12},{16,18},{18,... | collective-permute-start | bytes 1179656 | tf_op jit(solution)/shard_map/ppermute | solution.py:278
  57.2 4.8 %collective-permute-start.27 = (bf16[192,1152]{1,0:T(8,128)(2,1)S(1)}, bf16[192,1152]{1,0:T(8,128)(2,1)S(1)}, u32[]{:S(2)}, u32[]{:S(2)}) collective-permute-start(bf16[192,1152]{1,0:T(8,128)(2,1)S(1)} %get-tuple-element.44), channel_id=1, source_target_pairs={{0,2},{2,0},{4,6},{6,4},{8,10},{10,8},{12,14},{14,12},{16,18},{18,... | collective-permute-start | bytes 1327112 | tf_op jit(solution)/shard_map/ppermute | solution.py:278
  60.6 3.0 %collective-permute-start.28 = (bf16[192,1152]{1,0:T(8,128)(2,1)S(1)}, bf16[192,1152]{1,0:T(8,128)(2,1)S(1)}, u32[]{:S(2)}, u32[]{:S(2)}) collective-permute-start(bf16[192,1152]{1,0:T(8,128)(2,1)S(1)} %get-tuple-element.46), channel_id=1, source_target_pairs={{0,2},{2,0},{4,6},{6,4},{8,10},{10,8},{12,14},{14,12},{16,18},{18,... | collective-permute-start | bytes 1327112 | tf_op jit(solution)/shard_map/ppermute | solution.py:278
  61.3 4.5 %collective-permute-start.25 = (bf16[192,1024]{1,0:T(8,128)(2,1)S(1)}, bf16[192,1024]{1,0:T(8,128)(2,1)S(1)}, u32[]{:S(2)}, u32[]{:S(2)}) collective-permute-start(bf16[192,1024]{1,0:T(8,128)(2,1)S(1)} %get-tuple-element.42), channel_id=1, source_target_pairs={{0,2},{2,0},{4,6},{6,4},{8,10},{10,8},{12,14},{14,12},{16,18},{18,... | collective-permute-start | bytes 1179656 | tf_op jit(solution)/shard_map/ppermute | solution.py:278
  62.0 1.7 %copy-start.7 = (f32[192,1152]{1,0:T(8,128)}, f32[192,1152]{1,0:T(8,128)S(1)}, u32[]{:S(2)}) copy-start(f32[192,1152]{1,0:T(8,128)S(1)} %convert_add_fusion) | copy-start | bytes 2654212
  62.1 17.8 %collective-permute-start.31 = (bf16[192,640]{1,0:T(8,128)(2,1)S(1)}, bf16[192,640]{1,0:T(8,128)(2,1)S(1)}, u32[]{:S(2)}, u32[]{:S(2)}) collective-permute-start(bf16[192,640]{1,0:T(8,128)(2,1)S(1)} %slice.219), channel_id=1, source_target_pairs={{0,1},{1,0},{2,3},{3,2},{4,5},{5,4},{6,7},{7,6},{8,9},{9,8},{10,11... | collective-permute-start | bytes 737288 | tf_op jit(solution)/shard_map/ppermute | solution.py:281
  63.8 7.8 %collective-permute-start.29 = (bf16[192,512]{1,0:T(8,128)(2,1)S(1)}, bf16[192,512]{1,0:T(8,128)(2,1)S(1)}, u32[]{:S(2)}, u32[]{:S(2)}) collective-permute-start(bf16[192,512]{1,0:T(8,128)(2,1)S(1)} %pad_maximum_fusion.11), channel_id=1, source_target_pairs={{0,4},{2,6},{4,0},{6,2},{8,12},{10,14},{12,8},{14,10},{16,20},{18,... | collective-permute-start | bytes 589832 | tf_op jit(solution)/shard_map/ppermute | solution.py:275
  65.3 6.3 %slice-start = ((f32[192,1152]{1,0:T(8,128)}), f32[192,128]{1,0:T(8,128)S(1)}, s32[]{:S(2)}) async-start(f32[192,1152]{1,0:T(8,128)} %copy-done.7), calls=%async_computation | async-start | bytes 196608 | tf_op jit(solution)/shard_map/slice | solution.py:422
  65.3 6.3 %slice-start.1 = ((f32[192,1152]{1,0:T(8,128)}), f32[192,384]{1,0:T(8,128)S(1)}, s32[]{:S(2)}) async-start(f32[192,1152]{1,0:T(8,128)} %copy-done.7), calls=%async_computation.1 | async-start | bytes 589824 | tf_op jit(solution)/shard_map/slice | solution.py:422
  65.3 10.9 %collective-permute-start.32 = (bf16[192,640]{1,0:T(8,128)(2,1)S(1)}, bf16[192,640]{1,0:T(8,128)(2,1)S(1)}, u32[]{:S(2)}, u32[]{:S(2)}) collective-permute-start(bf16[192,640]{1,0:T(8,128)(2,1)S(1)} %slice.171), channel_id=1, source_target_pairs={{0,1},{1,0},{2,3},{3,2},{4,5},{5,4},{6,7},{7,6},{8,9},{9,8},{10,11... | collective-permute-start | bytes 737288 | tf_op jit(solution)/shard_map/ppermute | solution.py:281
  66.0 13.8 %collective-permute-start.26 = (bf16[192,384]{1,0:T(8,128)(2,1)S(1)}, bf16[192,384]{1,0:T(8,128)(2,1)S(1)}, u32[]{:S(2)}, u32[]{:S(2)}) collective-permute-start(bf16[192,384]{1,0:T(8,128)(2,1)S(1)} %slice.220), channel_id=1, source_target_pairs={{0,4},{2,6},{4,0},{6,2},{8,12},{10,14},{12,8},{14,10},{16,20},{18,... | collective-permute-start | bytes 442376 | tf_op jit(solution)/shard_map/ppermute | solution.py:275
  71.7 7.9 %collective-permute-start.30 = (bf16[192,512]{1,0:T(8,128)(2,1)S(1)}, bf16[192,512]{1,0:T(8,128)(2,1)S(1)}, u32[]{:S(2)}, u32[]{:S(2)}) collective-permute-start(bf16[192,512]{1,0:T(8,128)(2,1)S(1)} %get-tuple-element.56), channel_id=1, source_target_pairs={{0,1},{1,0},{2,3},{3,2},{4,5},{5,4},{6,7},{7,6},{8,9},{9,8},{10,11... | collective-permute-start | bytes 589832 | tf_op jit(solution)/shard_map/ppermute | solution.py:281
  76.3 6.3 %collective-permute-start.33 = (bf16[192,640]{1,0:T(8,128)(2,1)S(1)}, bf16[192,640]{1,0:T(8,128)(2,1)S(1)}, u32[]{:S(2)}, u32[]{:S(2)}) collective-permute-start(bf16[192,640]{1,0:T(8,128)(2,1)S(1)} %fusion.1), channel_id=1, source_target_pairs={{0,4},{2,6},{4,0},{6,2},{8,12},{10,14},{12,8},{14,10},{16,20},{18,... | collective-permute-start | bytes 737288 | tf_op jit(solution)/shard_map/ppermute | solution.py:275
  82.7 11.2 %collective-permute-start.36 = (bf16[48,1152]{1,0:T(8,128)(2,1)S(1)}, bf16[48,1152]{1,0:T(8,128)(2,1)S(1)}, u32[]{:S(2)}, u32[]{:S(2)}) collective-permute-start(bf16[48,1152]{1,0:T(8,128)(2,1)S(1)} %get-tuple-element.58), channel_id=1, source_target_pairs={{0,24},{2,26},{4,28},{6,30},{8,16},{10,18},{12,20},{14,22},{16,8},... | collective-permute-start | bytes 331784 | tf_op jit(solution)/shard_map/ppermute | solution.py:272
  87.1 6.8 %collective-permute-start.35 = (bf16[48,1152]{1,0:T(8,128)(2,1)S(1)}, bf16[48,1152]{1,0:T(8,128)(2,1)S(1)}, u32[]{:S(2)}, u32[]{:S(2)}) collective-permute-start(bf16[48,1152]{1,0:T(8,128)(2,1)S(1)} %get-tuple-element.59), channel_id=1, source_target_pairs={{0,8},{2,10},{4,12},{6,14},{8,0},{10,2},{12,4},{14,6},{16,24},{18,... | collective-permute-start | bytes 331784 | tf_op jit(solution)/shard_map/ppermute | solution.py:272
  87.1 7.3 %collective-permute-start.34 = (bf16[48,1152]{1,0:T(8,128)(2,1)S(1)}, bf16[48,1152]{1,0:T(8,128)(2,1)S(1)}, u32[]{:S(2)}, u32[]{:S(2)}) collective-permute-start(bf16[48,1152]{1,0:T(8,128)(2,1)S(1)} %get-tuple-element.61), channel_id=1, source_target_pairs={{0,16},{2,18},{4,20},{6,22},{8,24},{10,26},{12,28},{14,30},{16,0},... | collective-permute-start | bytes 331784 | tf_op jit(solution)/shard_map/ppermute | solution.py:272
  91.6 2.9 %copy-start.4 = (s32[128,2]{0,1:T(2,128)S(1)}, s32[128,2]{0,1:T(2,128)}, u32[]{:S(2)}) copy-start(s32[128,2]{0,1:T(2,128)} %param.14) | copy-start | bytes 3076
  91.6 2.9 %copy-start.5 = (f32[128,2]{0,1:T(2,128)S(1)}, f32[128,2]{0,1:T(2,128)}, u32[]{:S(2)}) copy-start(f32[128,2]{0,1:T(2,128)} %param.12) | copy-start | bytes 3076
  91.6 2.9 %copy-start.6 = (f32[128]{0:T(128)S(1)}, f32[128]{0:T(128)}, u32[]{:S(2)}) copy-start(f32[128]{0:T(128)} %param.11) | copy-start | bytes 1540
